TPU v7x, 256 devices: a whole 4x4x8 slice. The times are simulated.
256 devices in a mesh: rep: 2 (over z_hi), fs: 16 (over z_lo, y), tp: 8 (over x, core).
Axes of the slice: x: 4, y: 4, z: 8 (z_hi: 2, z_lo: 4; z = z_hi * 4 + z_lo), core: 2. Of those that a mesh axis runs over, the one named last changes fastest.
Arguments:
- stream: bfloat16 [32, 1024, 2048], P(('rep', 'fs'), None, 'tp'), may hold values from -6 to 6
- norm_gain: float32 [2048], replicated, may hold values from 0.1 to 1.9
- w_in: float32 [2048, 512], P('fs', 'tp'), may hold values from -0.125 to 0.125
- s_in: float32 [512], P(('tp', 'fs')), may hold values from 0.1 to 1.9
- pool_w: bfloat16 [4, 128, 128], replicated, may hold values from -0.5 to 0.5
- w_out: float32 [512, 2048], P('fs', 'tp'), may hold values from -0.25 to 0.25
- s_out: float32 [2048], P(('tp', 'fs')), may hold values from 0.1 to 1.9
- ffn_gain: float32 [2048], replicated, may hold values from 0.1 to 1.9
- w_up: float32 [2048, 8192], P('fs', 'tp'), may hold values from -0.125 to 0.125
- s_up: float32 [8192], P(('tp', 'fs')), may hold values from 0.1 to 1.9
- w_down: float32 [8192, 2048], P('tp', 'fs'), may hold values from -0.0625 to 0.0625
- s_down: float32 [2048], P('fs'), may hold values from 0.1 to 1.9
Outputs:
- result: bfloat16 [32, 1024, 2048], P(('rep', 'fs'), None, 'tp')
All inputs are finite; a program needn't handle non-finite values.
Results may differ from a plain program's by a relative error of at most 0.012.
Values may be sent and summed in bfloat16 or wider, within the bound.
No kernel may reach another device: no remote copies, remote signals or barrier semaphores. Data moves between devices by JAX's collectives and lax.ppermute only.
A program may use at most 64 MiB of HBM per device.

v0:
```python
import functools

import jax
import jax.numpy as jnp
from jax import lax
from jax.experimental import pallas as pl
from jax.experimental.pallas import tpu as pltpu
from jax.sharding import Mesh
from jax.sharding import PartitionSpec as P


BF = jnp.bfloat16
F32 = jnp.float32
EPS = 0.25
SEQ = 1024
FS = ("z", "y")
TP = ("x", "c")
VMEM = pl.BlockSpec(memory_space=pltpu.VMEM)


def send(array, axes, shift):
    count = lax.axis_size(axes)
    return lax.ppermute(array, axes, [(i, (i + shift) % count) for i in range(count)])


def swapped(array):
    return send(array, "c", 1)


def two_parts(values):
    high = values.astype(BF).astype(F32)
    return high, values - high


def dot(a, b):
    return jnp.dot(a, b, preferred_element_type=F32)


def dot_t(a, b):
    return lax.dot_general(a, b, (((1,), (1,)), ((), ())), preferred_element_type=F32)


def around(at):
    return [at] + [lax.rem(at + step, 4) for step in (3, 1, 2)]


def owners():
    x, c = lax.axis_index("x"), lax.axis_index("c")
    return [2 * chip + c for chip in around(x)] + [2 * chip + 1 - c for chip in around(x)]


def call(kernel, out_shape, scratch, limit_mb, flops, *args, in_hbm=0):
    moved = sum(a.size * a.dtype.itemsize for a in args)
    return pl.pallas_call(
        kernel,
        out_shape=out_shape,
        in_specs=[VMEM] * (len(args) - in_hbm) + [pl.BlockSpec(memory_space=pltpu.HBM)] * in_hbm,
        out_specs=jax.tree.map(lambda _: VMEM, out_shape),
        scratch_shapes=scratch,
        compiler_params=pltpu.CompilerParams(vmem_limit_bytes=limit_mb << 20),
        cost_estimate=pl.CostEstimate(flops=flops, bytes_accessed=moved, transcendentals=0),
    )(*args)


def column_of(row):
    return jnp.broadcast_to(row, (128, 128)).T


def prep_kernel(
    w_in, w_in_other, norm_gain_at, w_out_at, s_out_at, ffn_gain_at, w_up_at, s_up_at, w_down_at, s_down_at,
    up, packet, top, bottom, small, norm_gain, w_out, s_out, ffn_gain, w_up, s_up, w_down, s_down, done,
):
    sources = (w_up_at, ffn_gain_at, w_down_at, s_down_at, norm_gain_at, w_out_at, s_out_at, s_up_at)
    targets = (w_up, ffn_gain, w_down, s_down, norm_gain, w_out, s_out, s_up)
    copies = [pltpu.make_async_copy(a, b, done.at[k]) for k, (a, b) in enumerate(zip(sources, targets))]
    for copy in copies:
        copy.start()
    for copy in copies:
        copy.wait()
    c = lax.axis_index("c")
    f = 4 * lax.axis_index("z") + lax.axis_index("y")
    gain = column_of(ffn_gain[pl.ds(f, 1), :])
    for j in range(8):
        lanes = slice(j * 128, j * 128 + 128)
        up[:, lanes] = (w_up[:, lanes] * gain).astype(BF)
        packet[:128, lanes] = (w_down[lanes, :] * s_down[...]).T.astype(BF)
    gain = column_of(norm_gain[pl.ds(f, 1), :])
    mine, other = w_in[:128], w_in_other[:128]
    pair = jnp.concatenate(
        [jnp.where(c == 0, mine, other), jnp.where(c == 0, other, mine)], axis=1
    )
    pair = pair * gain
    for j in range(8):
        small[0:16, j * 128 : j * 128 + 128] = pair[j * 16 : j * 16 + 16]
    for j in range(4):
        small[16:24, j * 256 : j * 256 + 256] = w_out[j * 8 : j * 8 + 8, :]
    small[24:32] = jnp.zeros((8, 1024), F32)
    mine, other = w_in[128:129, :4], w_in_other[128:129, :4]
    rows = (
        (s_out[...], 0),
        (jnp.where(c == 0, mine, other), 256),
        (jnp.where(c == 0, other, mine), 512),
        (s_up[...], 768),
    )
    for row, at in rows:
        high, low = two_parts(row)
        small[24:25, at : at + row.shape[1]] = high
        small[24:25, at + 128 : at + 128 + row.shape[1]] = low
    packet[128:] = small[...].astype(BF)
    top[...] = packet[:80]
    bottom[...] = packet[80:]


def unpack_kernel(m0, m1, m2, m3, w_in, w_out, s_in, s_up):
    ys, zs = around(lax.axis_index("y")), around(lax.axis_index("z"))
    w_out[512:] = jnp.zeros((16, 256), BF)
    lane = lax.broadcasted_iota(jnp.int32, (16, 128), 1)
    at = lax.broadcasted_iota(jnp.int32, (16, 128), 0)
    firsts = [jnp.zeros((16, 128), F32) for _ in range(8)]
    for m, yy in zip((m0, m1, m2, m3), ys):
        for k, zz in enumerate(zs):
            f = 4 * zz + yy
            block = m[k]
            for j in range(8):
                w_in[pl.ds(pl.multiple_of(f * 128 + j * 16, 16), 16), :] = block[:16, j * 128 : j * 128 + 128]
            low = block[16:32].astype(F32)
            rows = jnp.concatenate([low[:8, j * 256 : j * 256 + 256] for j in range(4)], axis=0)
            w_out[pl.ds(pl.multiple_of(f * 32, 32), 32), :] = rows.astype(BF)
            for j in range(8):
                row = jnp.broadcast_to(low[8:9, j * 128 : j * 128 + 128], (16, 128))
                firsts[j] = jnp.where(at == f, row, firsts[j])

    def flat(rows, width):
        pieces = []
        for group in range(16 * width // 128):
            total = jnp.zeros((1, 128), F32)
            for i in range(128 // width):
                source = group * (128 // width) + i
                row = jnp.where(lane[:1] < width, rows[source : source + 1], 0.0)
                total += pltpu.roll(row, i * width, 1) if i else row
            pieces.append(total)
        return jnp.concatenate(pieces, axis=1) if len(pieces) > 1 else pieces[0]

    w_out[512:528] = jnp.concatenate(
        [flat(firsts[0], 16), flat(firsts[1], 16), jnp.zeros((14, 256), F32)], axis=0
    ).astype(BF)
    both = [firsts[2] + firsts[3], firsts[4] + firsts[5]]
    both = jnp.where(lane < 4, both[0], 0.0) + pltpu.roll(jnp.where(lane < 4, both[1], 0.0), 64, 1)
    total = jnp.zeros((1, 128), F32)
    for i in range(16):
        row = both[i : i + 1]
        total += pltpu.roll(row, 4 * i, 1) if i else row
    s_in[...] = total
    s_up[...] = flat(firsts[6] + firsts[7], 64)


def piece_refs(refs):
    return list(refs[:5]) + [refs[5].at[k] for k in range(3)]


def pool_kernel(*refs):
    pieces, (w_in, s_in, pool_w, out, mine, padded) = piece_refs(refs), refs[6:]
    x, whose = lax.axis_index("x"), owners()
    first = pl.ds(pl.multiple_of(lax.axis_index("c") * 512, 512), 512)
    padded[0:128] = jnp.zeros((128, 128), BF)
    padded[128 + SEQ :] = jnp.zeros((128, 128), BF)

    @pl.loop(0, 4)
    def _(block):
        rows = pl.ds(pl.multiple_of(block * 256, 256), 256)
        total = jnp.zeros((256, 128), F32)
        squares = jnp.zeros((256, 128), F32)
        for k, piece in enumerate(pieces):
            values = piece[rows, :]
            total += dot(values, w_in[pl.ds(pl.multiple_of(whose[k] * 256, 256), 256), :])
            wide = values.astype(F32)
            wide = wide * wide
            squares += wide[:, :128] + wide[:, 128:]
        scale = lax.rsqrt(jnp.sum(squares, axis=1, keepdims=True) / 2048 + EPS)
        padded[pl.ds(pl.multiple_of(128 + block * 256, 128), 256), :] = (total * scale * s_in[...]).astype(BF)

    half = jnp.left_shift(1, x)
    row = lax.broadcasted_iota(jnp.int32, (256, 512), 0)
    source = lax.broadcasted_iota(jnp.int32, (256, 512), 1) - 128
    band = jnp.where((source >= row - half) & (source < row + half), 1.0, 0.0).astype(BF)
    own = pool_w[x]

    @pl.loop(0, 4)
    def _(block):
        sums = dot(band, padded[pl.ds(pl.multiple_of(block * 256, 256), 512), :])
        at = lax.broadcasted_iota(jnp.int32, (256, 128), 0) + block * 256
        counts = jnp.minimum(at + half, SEQ) - jnp.maximum(at - half, 0)
        here = padded[pl.ds(pl.multiple_of(128 + block * 256, 128), 256), :].astype(F32)
        pooled = (sums / counts.astype(F32) - here).astype(BF)
        out[pl.ds(pl.multiple_of(block * 256, 256), 256), :] = dot(pooled, own).astype(BF)

    mine[...] = out[first, :]


def mix_kernel(*refs):
    pieces, grouped, near, across = piece_refs(refs), refs[6], refs[7:10], refs[10]
    weights = list(refs[11:15]) + [refs[15].at[k] for k in range(4)]
    mixed, own, factor = refs[16:]
    chips, whose = around(lax.axis_index("x")), owners()
    c = lax.axis_index("c")

    @pl.loop(0, 2)
    def _(block):
        rows = pl.ds(pl.multiple_of(block * 512, 512), 512)
        squares = jnp.zeros((512, 128), F32)
        left = jnp.concatenate(
            [grouped[rows, :]] + [jnp.where(block == c, a[...], across[k]) for k, a in enumerate(near)],
            axis=1,
        )
        for k in range(8):
            weight = jnp.concatenate(
                [weights[k][pl.ds(pl.multiple_of(chips[j] * 128, 128), 128), :] for j in range(4)],
                axis=0,
            )
            scale = weights[k][512:513, :].astype(F32) + weights[k][513:514, :].astype(F32)
            value = (pieces[k][rows, :].astype(F32) + dot(left, weight) * scale).astype(BF)
            mixed[rows, pl.ds(pl.multiple_of(whose[k] * 256, 256), 256)] = value
            if k == 0:
                own[rows, :] = value
            wide = value.astype(F32)
            wide = wide * wide
            squares += wide[:, :128] + wide[:, 128:]
        mean = jnp.sum(squares, axis=1, keepdims=True) / 2048
        factor[rows, :] = jnp.broadcast_to(lax.rsqrt(mean + EPS), (512, 128))


def up_kernel(mixed, factor, s_up, b0, b1, b2, b3, b4, hidden):
    ys, zs = around(lax.axis_index("y")), around(lax.axis_index("z"))
    parts = [b.at[pl.ds(2 * k, 2)] for b in (b0, b1, b2) for k in range(2)] + [b3, b4]

    @pl.loop(0, 8)
    def _(step):
        rows = pl.ds(pl.multiple_of(lax.rem(step, 2) * 512, 512), 512)
        cols = pl.ds(pl.multiple_of(lax.div(step, 2) * 256, 256), 256)
        total = jnp.zeros((512, 256), F32)
        for k in range(8):
            left = [
                mixed[rows, pl.ds(pl.multiple_of((4 * zs[k // 2] + ys[2 * (k % 2) + i]) * 128, 128), 128)]
                for i in range(2)
            ]
            total += dot(jnp.concatenate(left, axis=1), parts[k][:, :, cols].reshape(256, 256))
        scale = jnp.concatenate([factor[rows, :]] * 2, axis=1) * s_up[:, cols]
        value = jnp.maximum(total * scale, 0.0)
        hidden[rows, cols] = (value * value).astype(BF)


def down_kernel(steps, hidden, b0, b1, b2, b3, b4, own, other):
    x, y, z = (lax.axis_index(name) for name in ("x", "y", "z"))
    core = lax.shift_right_logical(y, 1)
    y_is_own = core == lax.axis_index("c")
    low_is_own = y_is_own == (jnp.bitwise_and(y, 1) == 1)
    side = jnp.bitwise_and(y, 1)

    @pl.loop(0, 2 * len(steps))
    def _(step):
        rows = pl.ds(pl.multiple_of(lax.rem(step, 2) * 512, 512), 512)
        k = lax.div(step, 2)
        chip = lax.rem(x + (lax.rem(2 * k + 1, 5) if len(steps) > 1 else steps[0]), 4)
        away = lax.rem(chip - z + 4, 4)
        place = jnp.where(away == 0, 0, jnp.where(away == 1, 2, jnp.where(away == 2, 3, 1)))
        inner = jnp.bitwise_and(place, 1)
        far = jnp.where(place < 2, b3[inner], b4[inner])
        for first, second, first_is_own, lane in (
            (b0[place], far, y_is_own, side),
            (b1[place], b2[place], low_is_own, 1 - side),
        ):
            weight = jnp.concatenate(
                [jnp.where(first_is_own, second, first), jnp.where(first_is_own, first, second)], axis=0
            )
            value = dot_t(hidden[rows, :], weight).astype(BF)
            lanes = pl.ds(pl.multiple_of(lane * 128, 128), 128)
            other[k, rows, lanes] = value[:, :128]
            own[k, rows, lanes] = value[:, 128:]


def along(bundle, axes):
    low, high = send(bundle, axes, 1), send(bundle, axes, -1)
    return [bundle, low, high, send(low[:2], axes, 1), send(high[2:], axes, -1)]


def near_three(array):
    far = send(array, "x", 2)
    return [send(array, "x", 1), send(array, "x", -1), far]


def bf(*shape):
    return jax.ShapeDtypeStruct(shape, BF)


def f32(*shape):
    return jax.ShapeDtypeStruct(shape, F32)


def layer(
    stream, norm_gain, w_in, s_in, pool_w, w_out, s_out, ffn_gain, w_up, s_up, w_down, s_down
):
    ring_z = ("rep", "z")
    tokens = stream[0]

    near = near_three(tokens)
    pieces = [tokens] + near
    both_in = jnp.concatenate([w_in, jnp.pad(s_in[None], ((0, 7), (0, 60)))], axis=0)
    other_in = swapped(both_in)
    pieces.append(swapped(tokens))
    pieces.append(swapped(jnp.stack(near)))

    arrays = (
        both_in,
        other_in,
        norm_gain.reshape(16, 128),
        w_out,
        s_out[None],
        ffn_gain.reshape(16, 128),
        w_up,
        s_up[None],
        w_down,
        s_down[None],
    )
    up, packet, top, bottom = call(
        prep_kernel,
        (bf(128, 1024), bf(160, 1024), bf(80, 1024), bf(80, 1024)),
        [pltpu.VMEM((32, 1024), F32)]
        + [pltpu.VMEM(a.shape, F32) for a in arrays[2:]]
        + [pltpu.SemaphoreType.DMA((8,))],
        60,
        1_000_000,
        *arrays,
        in_hbm=8,
    )
    low, high = send(packet, ring_z, 1), send(packet, ring_z, -1)
    far_top, far_bottom = send(top, ring_z, 2), send(bottom, ring_z, -2)
    up_far, up_low, up_high = send(up, "y", 2), send(up, "y", 1), send(up, "y", -1)

    mixer = jnp.stack([packet[128:], low[128:], high[128:], far_bottom[48:]])
    far = send(mixer, "y", 2)
    mixers = [mixer, send(mixer, "y", 1), send(mixer, "y", -1), far]
    w_in_all, out_own, s_in_row, s_up_row = call(
        unpack_kernel,
        (bf(2048, 128), bf(528, 256), f32(1, 128), f32(1, 1024)),
        [],
        8,
        1_000_000,
        *mixers,
    )
    up_parts = along(jnp.stack([up, up_low, up_high, up_far]), ring_z)
    down_parts = along(
        jnp.stack(
            [
                packet[:128],
                low[:128],
                high[:128],
                jnp.concatenate([far_top, far_bottom[:48]], axis=0),
            ]
        ),
        "y",
    )

    grouped, mine = call(
        pool_kernel,
        (bf(SEQ, 128), bf(512, 128)),
        [pltpu.VMEM((SEQ + 256, 128), BF)],
        16,
        800_000_000,
        *pieces,
        w_in_all,
        s_in_row,
        pool_w,
    )
    near = near_three(mine)
    across = swapped(jnp.stack(near))
    outs = [out_own] + near_three(out_own)
    outs.append(swapped(jnp.stack(outs)))
    mixed, mixed_own, factor = call(
        mix_kernel,
        (bf(SEQ, 2048), bf(SEQ, 256), f32(SEQ, 128)),
        [],
        32,
        2_200_000_000,
        *pieces,
        grouped,
        *near,
        across,
        *outs,
    )

    hidden = call(
        up_kernel, bf(SEQ, 1024), [], 32, 4_300_000_000, mixed, factor, s_up_row, *up_parts
    )
    chips = []
    for steps in ((2,), (1, 3, 0)):
        count = len(steps)
        own, other = call(
            functools.partial(down_kernel, steps),
            (bf(count, SEQ, 256), bf(count, SEQ, 256)),
            [],
            32,
            1_075_000_000 * count,
            hidden,
            *down_parts,
        )
        crossed = swapped(other)
        chips += [own[k].astype(F32) + crossed[k].astype(F32) for k in range(count)]
    total = mixed_own.astype(F32) + chips[3]
    for k, shift in enumerate((2, 1, -1)):
        total = total + send(chips[k].astype(BF), "x", shift).astype(F32)
    return total.astype(BF)[None]


def solution(mesh):
    finer = Mesh(
        mesh.devices.reshape(mesh.shape["rep"], 4, 4, 4, 2),
        ("rep", "z", "y", "x", "c"),
    )
    rows = ("rep", "z", "y")
    both = ("x", "c", "z", "y")
    return jax.shard_map(
        layer,
        mesh=finer,
        in_specs=(
            P(rows, None, TP),
            P(),
            P(FS, TP),
            P(both),
            P(),
            P(FS, TP),
            P(both),
            P(),
            P(FS, TP),
            P(both),
            P(TP, FS),
            P(FS),
        ),
        out_specs=P(rows, None, TP),
        check_vma=False,
    )
```

profile of v0, /device:TPU:1, one launch (start us, length us, event | category | flops | bytes accessed | tf_op | source)
XLA Modules:
  0.0 173.5 jit_solution(7887251105566371671)
XLA Ops:
  0.0 2.0 %collective-permute-start = (bf16[1024,256]{1,0:T(8,128)(2,1)}, bf16[1024,256]{1,0:T(8,128)(2,1)S(1)}, u32[]{:S(2)}, u32[]{:S(2)}) collective-permute-start(bf16[1024,256]{1,0:T(8,128)(2,1)} %bitcast.60), channel_id=1, source_target_pairs={{0,2},{2,4},{4,6},{6,0},{1,3},{3,5},{5,7},{7,1},{8,10},{10,12},{12... | collective-permute-start | bytes 1572872 | tf_op jit(solution)/shard_map/ppermute | solution.py:23
  2.0 1.3 collective-permute-start.1
  3.3 1.7 collective-permute-start.2
  6.6 1.6 collective-permute-start.5
  9.7 3.3 %shard_map.118 = (bf16[128,1024]{1,0:T(8,128)(2,1)}, bf16[160,1024]{1,0:T(8,128)(2,1)}, bf16[80,1024]{1,0:T(8,128)(2,1)}, bf16[80,1024]{1,0:T(8,128)(2,1)}) custom-call(f32[136,64]{1,0:T(8,128)} %copy-done.2, f32[136,64]{1,0:T(8,128)} %copy-done.4, f32[16,128]{1,0:T(8,128)} %bitcast.77, f32[32,256]{1,0:T(8,128)} %w_out_at.1, f32[1,16]{1,0:T(1,128)} %bitcast.80, ...), custom_call_target="tpu_custom_call" | custom-call | flops 1000000 | bytes 1168192 | tf_op jit(solution)/shard_map/pallas_call | solution.py:54
  13.0 6.1 %collective-permute-start.8 = (bf16[80,1024]{1,0:T(8,128)(2,1)}, bf16[80,1024]{1,0:T(8,128)(2,1)S(1)}, u32[]{:S(2)}, u32[]{:S(2)}) collective-permute-start(bf16[80,1024]{1,0:T(8,128)(2,1)} %get-tuple-element.23), channel_id=1, source_target_pairs={{0,192},{32,224},{64,0},{96,32},{128,64},{160,96},{192,128},{224,1... | collective-permute-start | bytes 491528 | tf_op jit(solution)/shard_map/ppermute | solution.py:23
  19.1 1.0 slice_bitcast_fusion.2
  20.1 0.8 slice_bitcast_fusion.6
  20.9 3.1 %collective-permute-done.8 = bf16[80,1024]{1,0:T(8,128)(2,1)S(1)} collective-permute-done((bf16[80,1024]{1,0:T(8,128)(2,1)}, bf16[80,1024]{1,0:T(8,128)(2,1)S(1)}, u32[]{:S(2)}, u32[]{:S(2)}) %collective-permute-start.8) | collective-permute-done | bytes 163872 | tf_op jit(solution)/shard_map/ppermute | solution.py:23
  24.1 4.8 %collective-permute-start.7 = (bf16[160,1024]{1,0:T(8,128)(2,1)}, bf16[160,1024]{1,0:T(8,128)(2,1)S(1)}, u32[]{:S(2)}, u32[]{:S(2)}) collective-permute-start(bf16[160,1024]{1,0:T(8,128)(2,1)} %get-tuple-element.22), channel_id=1, source_target_pairs={{0,224},{32,0},{64,32},{96,64},{128,96},{160,128},{192,160},{224,1... | collective-permute-start | bytes 983048 | tf_op jit(solution)/shard_map/ppermute | solution.py:23
  30.0 1.9 %collective-permute-start.4 = (bf16[3,1024,256]{2,1,0:T(8,128)(2,1)S(1)}, bf16[3,1024,256]{2,1,0:T(8,128)(2,1)S(1)}, u32[]{:S(2)}, u32[]{:S(2)}) collective-permute-start(bf16[3,1024,256]{2,1,0:T(8,128)(2,1)S(1)} %pad_maximum_fusion), channel_id=1, source_target_pairs={{0,1},{1,0},{2,3},{3,2},{4,5},{5,4},{6,7},{7,6},{8,9},{9,8},{10,11... | collective-permute-start | bytes 4718600 | tf_op jit(solution)/shard_map/ppermute | solution.py:23
  31.8 11.9 %collective-permute-done.27 = bf16[80,1024]{1,0:T(8,128)(2,1)S(1)} collective-permute-done((bf16[80,1024]{1,0:T(8,128)(2,1)}, bf16[80,1024]{1,0:T(8,128)(2,1)S(1)}, u32[]{:S(2)}, u32[]{:S(2)}) %collective-permute-start.27) | collective-permute-done | bytes 163872 | tf_op jit(solution)/shard_map/ppermute | solution.py:23
  43.7 1.3 collective-permute-start.20
  45.1 1.5 collective-permute-start.21
  46.6 1.7 collective-permute-start.22
  48.4 1.9 %collective-permute-done.20 = bf16[128,1024]{1,0:T(8,128)(2,1)S(1)} collective-permute-done((bf16[128,1024]{1,0:T(8,128)(2,1)S(1)}, bf16[128,1024]{1,0:T(8,128)(2,1)S(1)}, u32[]{:S(2)}, u32[]{:S(2)}) %collective-permute-start.20) | collective-permute-done | bytes 262176 | tf_op jit(solution)/shard_map/ppermute | solution.py:23
  50.2 1.5 collective-permute-start.10
  51.7 1.3 collective-permute-start.11
  53.0 2.1 %collective-permute-done.22 = bf16[128,1024]{1,0:T(8,128)(2,1)S(1)} collective-permute-done((bf16[128,1024]{1,0:T(8,128)(2,1)S(1)}, bf16[128,1024]{1,0:T(8,128)(2,1)S(1)}, u32[]{:S(2)}, u32[]{:S(2)}) %collective-permute-start.22) | collective-permute-done | bytes 262176 | tf_op jit(solution)/shard_map/ppermute | solution.py:23
  55.1 1.5 collective-permute-start.9
  56.7 3.0 %collective-permute-done.10.m2 = bf16[4,32,1024]{2,1,0:T(8,128)(2,1)S(1)} collective-permute-done((bf16[4,32,1024]{2,1,0:T(8,128)(2,1)S(1)}, bf16[4,32,1024]{2,1,0:T(8,128)(2,1)S(1)}, u32[]{:S(2)}, u32[]{:S(2)}) %collective-permute-start.10) | collective-permute-done | bytes 262176 | tf_op jit(solution)/shard_map/ppermute | solution.py:23
  59.7 2.7 %collective-permute-start.23 = (bf16[4,128,1024]{2,1,0:T(8,128)(2,1)S(1)}, bf16[4,128,1024]{2,1,0:T(8,128)(2,1)S(1)}, u32[]{:S(2)}, u32[]{:S(2)}) collective-permute-start(bf16[4,128,1024]{2,1,0:T(8,128)(2,1)S(1)} %pad_maximum_fusion.2.b0), channel_id=1, source_target_pairs={{0,32},{32,64},{64,96},{96,128},{128,160},{160,192},{192,224},{224... | collective-permute-start | bytes 3145736 | tf_op jit(solution)/shard_map/ppermute | solution.py:23
  62.4 4.7 %collective-permute-done.9.m1 = bf16[4,32,1024]{2,1,0:T(8,128)(2,1)S(1)} collective-permute-done((bf16[4,32,1024]{2,1,0:T(8,128)(2,1)S(1)}, bf16[4,32,1024]{2,1,0:T(8,128)(2,1)S(1)}, u32[]{:S(2)}, u32[]{:S(2)}) %collective-permute-start.9) | collective-permute-done | bytes 262176 | tf_op jit(solution)/shard_map/ppermute | solution.py:23
  68.0 2.4 %collective-permute-start.17 = (bf16[528,256]{1,0:T(8,128)(2,1)S(1)}, bf16[528,256]{1,0:T(8,128)(2,1)S(1)}, u32[]{:S(2)}, u32[]{:S(2)}) collective-permute-start(bf16[528,256]{1,0:T(8,128)(2,1)S(1)} %get-tuple-element.28.refs_11_), channel_id=1, source_target_pairs={{0,6},{2,0},{4,2},{6,4},{1,7},{3,1},{5,3},{7,5},{8,14},{10,8},{12,... | collective-permute-start | bytes 811016 | tf_op jit(solution)/shard_map/ppermute | solution.py:23
  70.4 3.1 %collective-permute-start.18 = (bf16[528,256]{1,0:T(8,128)(2,1)S(1)}, bf16[528,256]{1,0:T(8,128)(2,1)S(1)}, u32[]{:S(2)}, u32[]{:S(2)}) collective-permute-start(bf16[528,256]{1,0:T(8,128)(2,1)S(1)} %get-tuple-element.28.refs_11_), channel_id=1, source_target_pairs={{0,4},{2,6},{4,0},{6,2},{1,5},{3,7},{5,1},{7,3},{8,12},{10,14},{12... | collective-permute-start | bytes 811016 | tf_op jit(solution)/shard_map/ppermute | solution.py:23
  75.2 3.4 %shard_map.120 = (bf16[1024,128]{1,0:T(8,128)(2,1)S(1)}, bf16[512,128]{1,0:T(8,128)(2,1)S(1)}) custom-call(bf16[1024,256]{1,0:T(8,128)(2,1)S(1)} %bitcast.64, bf16[1024,256]{1,0:T(8,128)(2,1)S(1)} %collective-permute-done.refs_1_, bf16[1024,256]{1,0:T(8,128)(2,1)S(1)} %collective-permute-done.1.refs_2_, ...), custom_call_target="tpu_custom_call" | custom-call | flops 800000000 | bytes 4850176 | tf_op jit(solution)/shard_map/pallas_call | solution.py:54
  78.8 2.3 %collective-permute-done.18.refs_14_ = bf16[528,256]{1,0:T(8,128)(2,1)S(1)} collective-permute-done((bf16[528,256]{1,0:T(8,128)(2,1)S(1)}, bf16[528,256]{1,0:T(8,128)(2,1)S(1)}, u32[]{:S(2)}, u32[]{:S(2)}) %collective-permute-start.18) | collective-permute-done | bytes 270368 | tf_op jit(solution)/shard_map/ppermute | solution.py:23
  81.0 1.7 collective-permute-start.13
  82.8 3.7 %collective-permute-done.12.refs_7_ = bf16[512,128]{1,0:T(8,128)(2,1)S(1)} collective-permute-done((bf16[512,128]{1,0:T(8,128)(2,1)S(1)}, bf16[512,128]{1,0:T(8,128)(2,1)S(1)}, u32[]{:S(2)}, u32[]{:S(2)}) %collective-permute-start.12) | collective-permute-done | bytes 131104 | tf_op jit(solution)/shard_map/ppermute | solution.py:23
  86.5 1.5 collective-permute-start.14
  88.2 7.6 %collective-permute-start.19 = (bf16[4,528,256]{2,1,0:T(8,128)(2,1)S(1)}, bf16[4,528,256]{2,1,0:T(8,128)(2,1)S(1)}, u32[]{:S(2)}, u32[]{:S(2)}) collective-permute-start(bf16[4,528,256]{2,1,0:T(8,128)(2,1)S(1)} %pad_maximum_fusion.1), channel_id=1, source_target_pairs={{0,1},{1,0},{2,3},{3,2},{4,5},{5,4},{6,7},{7,6},{8,9},{9,8},{10,11... | collective-permute-start | bytes 3244040 | tf_op jit(solution)/shard_map/ppermute | solution.py:23
  95.7 2.8 %collective-permute-start.29 = (bf16[4,128,1024]{2,1,0:T(8,128)(2,1)S(1)}, bf16[4,128,1024]{2,1,0:T(8,128)(2,1)S(1)}, u32[]{:S(2)}, u32[]{:S(2)}) collective-permute-start(bf16[4,128,1024]{2,1,0:T(8,128)(2,1)S(1)} %pad_maximum_fusion.3.b0), channel_id=1, source_target_pairs={{0,24},{8,0},{16,8},{24,16},{1,25},{9,1},{17,9},{25,17},{2,26},{10... | collective-permute-start | bytes 3145736 | tf_op jit(solution)/shard_map/ppermute | solution.py:23
  98.6 4.6 %collective-permute-start.15 = (bf16[3,512,128]{2,1,0:T(8,128)(2,1)S(1)}, bf16[3,512,128]{2,1,0:T(8,128)(2,1)S(1)}, u32[]{:S(2)}, u32[]{:S(2)}) collective-permute-start(bf16[3,512,128]{2,1,0:T(8,128)(2,1)S(1)} %pad_maximum_fusion.4), channel_id=1, source_target_pairs={{0,1},{1,0},{2,3},{3,2},{4,5},{5,4},{6,7},{7,6},{8,9},{9,8},{10,11... | collective-permute-start | bytes 1179656 | tf_op jit(solution)/shard_map/ppermute | solution.py:23
  103.3 1.8 %collective-permute-start.25 = (bf16[2,128,1024]{2,1,0:T(8,128)(2,1)S(1)}, bf16[2,128,1024]{2,1,0:T(8,128)(2,1)S(1)}, u32[]{:S(2)}, u32[]{:S(2)}) collective-permute-start(bf16[2,128,1024]{2,1,0:T(8,128)(2,1)S(1)} %slice.75), channel_id=1, source_target_pairs={{0,32},{32,64},{64,96},{96,128},{128,160},{160,192},{192,224},{224... | collective-permute-start | bytes 1572872 | tf_op jit(solution)/shard_map/ppermute | solution.py:23
  105.1 1.0 collective-permute-start.26
  106.2 10.6 %collective-permute-done.29.b2 = bf16[4,128,1024]{2,1,0:T(8,128)(2,1)S(1)} collective-permute-done((bf16[4,128,1024]{2,1,0:T(8,128)(2,1)S(1)}, bf16[4,128,1024]{2,1,0:T(8,128)(2,1)S(1)}, u32[]{:S(2)}, u32[]{:S(2)}) %collective-permute-start.29) | collective-permute-done | bytes 1048608 | tf_op jit(solution)/shard_map/ppermute | solution.py:23
  116.8 3.1 %collective-permute-start.30 = (bf16[2,128,1024]{2,1,0:T(8,128)(2,1)S(1)}, bf16[2,128,1024]{2,1,0:T(8,128)(2,1)S(1)}, u32[]{:S(2)}, u32[]{:S(2)}) collective-permute-start(bf16[2,128,1024]{2,1,0:T(8,128)(2,1)S(1)} %slice.80), channel_id=1, source_target_pairs={{0,8},{8,16},{16,24},{24,0},{1,9},{9,17},{17,25},{25,1},{2,10},{10... | collective-permute-start | bytes 1572872 | tf_op jit(solution)/shard_map/ppermute | solution.py:23
  120.6 3.4 %shard_map.121 = (bf16[1024,2048]{1,0:T(8,128)(2,1)S(1)}, bf16[1024,256]{1,0:T(8,128)(2,1)S(1)}, f32[1024,128]{1,0:T(8,128)S(1)}) custom-call(bf16[1024,256]{1,0:T(8,128)(2,1)S(1)} %bitcast.65, bf16[1024,256]{1,0:T(8,128)(2,1)S(1)} %collective-permute-done.refs_1_, bf16[1024,256]{1,0:T(8,128)(2,1)S(1)} %collective-permute-done.1.refs_2_, ...), custom_call_target="tpu_custom_call" | custom-call | flops 2200000000 | bytes 7405568 | tf_op jit(solution)/shard_map/pallas_call | solution.py:54
  124.0 6.5 %shard_map.122.hidden = bf16[1024,1024]{1,0:T(8,128)(2,1)S(1)} custom-call(bf16[1024,2048]{1,0:T(8,128)(2,1)S(1)} %get-tuple-element.30.mixed, f32[1024,128]{1,0:T(8,128)S(1)} %get-tuple-element.31.factor, f32[1,1024]{1,0:T(1,128)S(1)} %get-tuple-element.32.s_up, bf16[4,128,1024]{2,1,0:T(8,128)(2,1)S(1)} %pad_maximum_fusion.2.b0, ...), custom_call_target="tpu_custom_call" | custom-call | flops 4300000256 | bytes 8916992 | tf_op jit(solution)/shard_map/pallas_call | solution.py:54
  130.5 5.3 %shard_map.123 = (bf16[3,1024,256]{2,1,0:T(8,128)(2,1)S(1)}, bf16[3,1024,256]{2,1,0:T(8,128)(2,1)S(1)}) custom-call(bf16[1024,1024]{1,0:T(8,128)(2,1)S(1)} %shard_map.122.hidden, bf16[4,128,1024]{2,1,0:T(8,128)(2,1)S(1)} %pad_maximum_fusion.3.b0, bf16[4,128,1024]{2,1,0:T(8,128)(2,1)S(1)} %collective-permute-done.28.b1, ...), custom_call_target="tpu_custom_call" | custom-call | flops 3224999936 | bytes 6291456 | tf_op jit(solution)/shard_map/pallas_call | solution.py:54
  135.8 5.9 %collective-permute-start.32 = (bf16[3,1024,256]{2,1,0:T(8,128)(2,1)S(1)}, bf16[3,1024,256]{2,1,0:T(8,128)(2,1)S(1)}, u32[]{:S(2)}, u32[]{:S(2)}) collective-permute-start(bf16[3,1024,256]{2,1,0:T(8,128)(2,1)S(1)} %get-tuple-element.36), channel_id=1, source_target_pairs={{0,1},{1,0},{2,3},{3,2},{4,5},{5,4},{6,7},{7,6},{8,9},{9,8},{10,11... | collective-permute-start | bytes 4718600 | tf_op jit(solution)/shard_map/ppermute | solution.py:23
  141.7 1.6 shard_map.124
  143.5 2.0 %collective-permute-done.33 = bf16[1,1024,256]{2,1,0:T(8,128)(2,1)S(1)} collective-permute-done((bf16[1,1024,256]{2,1,0:T(8,128)(2,1)S(1)}, bf16[1,1024,256]{2,1,0:T(8,128)(2,1)S(1)}, u32[]{:S(2)}, u32[]{:S(2)}) %collective-permute-start.33) | collective-permute-done | bytes 524320 | tf_op jit(solution)/shard_map/ppermute | solution.py:23
  145.6 1.9 %collective-permute-start.34 = (bf16[1024,256]{1,0:T(8,128)(2,1)S(1)}, bf16[1024,256]{1,0:T(8,128)(2,1)S(1)}, u32[]{:S(2)}, u32[]{:S(2)}) collective-permute-start(bf16[1024,256]{1,0:T(8,128)(2,1)S(1)} %fusion.4), channel_id=1, source_target_pairs={{0,4},{2,6},{4,0},{6,2},{1,5},{3,7},{5,1},{7,3},{8,12},{10,14},{12... | collective-permute-start | bytes 1572872 | tf_op jit(solution)/shard_map/ppermute | solution.py:23
  147.9 2.7 %collective-permute-start.36 = (bf16[1024,256]{1,0:T(8,128)(2,1)S(1)}, bf16[1024,256]{1,0:T(8,128)(2,1)S(1)}, u32[]{:S(2)}, u32[]{:S(2)}) collective-permute-start(bf16[1024,256]{1,0:T(8,128)(2,1)S(1)} %get-tuple-element.40), channel_id=1, source_target_pairs={{0,6},{2,0},{4,2},{6,4},{1,7},{3,1},{5,3},{7,5},{8,14},{10,8},{12,... | collective-permute-start | bytes 1572872 | tf_op jit(solution)/shard_map/ppermute | solution.py:23
  150.6 9.8 %collective-permute-done.34 = bf16[1024,256]{1,0:T(8,128)(2,1)S(1)} collective-permute-done((bf16[1024,256]{1,0:T(8,128)(2,1)S(1)}, bf16[1024,256]{1,0:T(8,128)(2,1)S(1)}, u32[]{:S(2)}, u32[]{:S(2)}) %collective-permute-start.34) | collective-permute-done | bytes 524320 | tf_op jit(solution)/shard_map/ppermute | solution.py:23
  160.4 11.9 %collective-permute-done.35 = bf16[1024,256]{1,0:T(8,128)(2,1)S(1)} collective-permute-done((bf16[1024,256]{1,0:T(8,128)(2,1)S(1)}, bf16[1024,256]{1,0:T(8,128)(2,1)S(1)}, u32[]{:S(2)}, u32[]{:S(2)}) %collective-permute-start.35) | collective-permute-done | bytes 524320 | tf_op jit(solution)/shard_map/ppermute | solution.py:23
  172.3 1.2 fusion.7
  (67 shorter events, 8.5 us)
Async XLA Ops:
  0.0 28.9 %collective-permute-start = (bf16[1024,256]{1,0:T(8,128)(2,1)}, bf16[1024,256]{1,0:T(8,128)(2,1)S(1)}, u32[]{:S(2)}, u32[]{:S(2)}) collective-permute-start(bf16[1024,256]{1,0:T(8,128)(2,1)} %bitcast.60), channel_id=1, source_target_pairs={{0,2},{2,4},{4,6},{6,0},{1,3},{3,5},{5,7},{7,1},{8,10},{10,12},{12... | collective-permute-start | bytes 1572872 | tf_op jit(solution)/shard_map/ppermute | solution.py:23
  2.0 27.0 %collective-permute-start.1 = (bf16[1024,256]{1,0:T(8,128)(2,1)}, bf16[1024,256]{1,0:T(8,128)(2,1)S(1)}, u32[]{:S(2)}, u32[]{:S(2)}) collective-permute-start(bf16[1024,256]{1,0:T(8,128)(2,1)} %bitcast.61), channel_id=1, source_target_pairs={{0,6},{2,0},{4,2},{6,4},{1,7},{3,1},{5,3},{7,5},{8,14},{10,8},{12,... | collective-permute-start | bytes 1572872 | tf_op jit(solution)/shard_map/ppermute | solution.py:23
  3.3 26.5 %collective-permute-start.2 = (bf16[1024,256]{1,0:T(8,128)(2,1)}, bf16[1024,256]{1,0:T(8,128)(2,1)S(1)}, u32[]{:S(2)}, u32[]{:S(2)}) collective-permute-start(bf16[1024,256]{1,0:T(8,128)(2,1)} %bitcast.62), channel_id=1, source_target_pairs={{0,4},{2,6},{4,0},{6,2},{1,5},{3,7},{5,1},{7,3},{8,12},{10,14},{12... | collective-permute-start | bytes 1572872 | tf_op jit(solution)/shard_map/ppermute | solution.py:23
  6.6 2.5 %copy-start.2 = (f32[136,64]{1,0:T(8,128)}, f32[136,64]{1,0:T(8,128)S(1)}, u32[]{:S(2)}) copy-start(f32[136,64]{1,0:T(8,128)S(1)} %select_maximum_fusion.w_in) | copy-start | bytes 104452
  6.6 2.5 %collective-permute-start.5 = (f32[136,64]{1,0:T(8,128)S(1)}, f32[136,64]{1,0:T(8,128)S(1)}, u32[]{:S(2)}, u32[]{:S(2)}) collective-permute-start(f32[136,64]{1,0:T(8,128)S(1)} %select_maximum_fusion.w_in), channel_id=1, source_target_pairs={{0,1},{1,0},{2,3},{3,2},{4,5},{5,4},{6,7},{7,6},{8,9},{9,8},{10,11... | collective-permute-start | bytes 104456 | tf_op jit(solution)/shard_map/ppermute | solution.py:23
  8.2 62.2 %collective-permute-start.3 = (bf16[1024,256]{1,0:T(8,128)(2,1)}, bf16[1024,256]{1,0:T(8,128)(2,1)S(1)}, u32[]{:S(2)}, u32[]{:S(2)}) collective-permute-start(bf16[1024,256]{1,0:T(8,128)(2,1)} %bitcast.63), channel_id=1, source_target_pairs={{0,1},{1,0},{2,3},{3,2},{4,5},{5,4},{6,7},{7,6},{8,9},{9,8},{10,11... | collective-permute-start | bytes 1572872 | tf_op jit(solution)/shard_map/ppermute | solution.py:23
  9.1 0.6 copy-start.4
  13.0 11.1 %collective-permute-start.8 = (bf16[80,1024]{1,0:T(8,128)(2,1)}, bf16[80,1024]{1,0:T(8,128)(2,1)S(1)}, u32[]{:S(2)}, u32[]{:S(2)}) collective-permute-start(bf16[80,1024]{1,0:T(8,128)(2,1)} %get-tuple-element.23), channel_id=1, source_target_pairs={{0,192},{32,224},{64,0},{96,32},{128,64},{160,96},{192,128},{224,1... | collective-permute-start | bytes 491528 | tf_op jit(solution)/shard_map/ppermute | solution.py:23
  24.1 21.0 %collective-permute-start.7 = (bf16[160,1024]{1,0:T(8,128)(2,1)}, bf16[160,1024]{1,0:T(8,128)(2,1)S(1)}, u32[]{:S(2)}, u32[]{:S(2)}) collective-permute-start(bf16[160,1024]{1,0:T(8,128)(2,1)} %get-tuple-element.22), channel_id=1, source_target_pairs={{0,224},{32,0},{64,32},{96,64},{128,96},{160,128},{192,160},{224,1... | collective-permute-start | bytes 983048 | tf_op jit(solution)/shard_map/ppermute | solution.py:23
  28.9 17.7 %collective-permute-start.6 = (bf16[160,1024]{1,0:T(8,128)(2,1)}, bf16[160,1024]{1,0:T(8,128)(2,1)S(1)}, u32[]{:S(2)}, u32[]{:S(2)}) collective-permute-start(bf16[160,1024]{1,0:T(8,128)(2,1)} %get-tuple-element.22), channel_id=1, source_target_pairs={{0,32},{32,64},{64,96},{96,128},{128,160},{160,192},{192,224},{224... | collective-permute-start | bytes 983048 | tf_op jit(solution)/shard_map/ppermute | solution.py:23
  29.0 14.7 %collective-permute-start.27 = (bf16[80,1024]{1,0:T(8,128)(2,1)}, bf16[80,1024]{1,0:T(8,128)(2,1)S(1)}, u32[]{:S(2)}, u32[]{:S(2)}) collective-permute-start(bf16[80,1024]{1,0:T(8,128)(2,1)} %get-tuple-element.34), channel_id=1, source_target_pairs={{0,64},{32,96},{64,128},{96,160},{128,192},{160,224},{192,0},{224,... | collective-permute-start | bytes 491528 | tf_op jit(solution)/shard_map/ppermute | solution.py:23
  29.8 13.9 %copy-start.3 = (bf16[128,1024]{1,0:T(8,128)(2,1)S(1)}, bf16[128,1024]{1,0:T(8,128)(2,1)}, u32[]{:S(2)}) copy-start(bf16[128,1024]{1,0:T(8,128)(2,1)} %get-tuple-element.33) | copy-start | bytes 786436
  30.0 44.6 %collective-permute-start.4 = (bf16[3,1024,256]{2,1,0:T(8,128)(2,1)S(1)}, bf16[3,1024,256]{2,1,0:T(8,128)(2,1)S(1)}, u32[]{:S(2)}, u32[]{:S(2)}) collective-permute-start(bf16[3,1024,256]{2,1,0:T(8,128)(2,1)S(1)} %pad_maximum_fusion), channel_id=1, source_target_pairs={{0,1},{1,0},{2,3},{3,2},{4,5},{5,4},{6,7},{7,6},{8,9},{9,8},{10,11... | collective-permute-start | bytes 4718600 | tf_op jit(solution)/shard_map/ppermute | solution.py:23
  43.7 6.5 %collective-permute-start.20 = (bf16[128,1024]{1,0:T(8,128)(2,1)S(1)}, bf16[128,1024]{1,0:T(8,128)(2,1)S(1)}, u32[]{:S(2)}, u32[]{:S(2)}) collective-permute-start(bf16[128,1024]{1,0:T(8,128)(2,1)S(1)} %copy-done.3), channel_id=1, source_target_pairs={{0,8},{8,16},{16,24},{24,0},{1,9},{9,17},{17,25},{25,1},{2,10},{10... | collective-permute-start | bytes 786440 | tf_op jit(solution)/shard_map/ppermute | solution.py:23
  45.1 6.6 %collective-permute-start.21 = (bf16[128,1024]{1,0:T(8,128)(2,1)S(1)}, bf16[128,1024]{1,0:T(8,128)(2,1)S(1)}, u32[]{:S(2)}, u32[]{:S(2)}) collective-permute-start(bf16[128,1024]{1,0:T(8,128)(2,1)S(1)} %copy-done.3), channel_id=1, source_target_pairs={{0,24},{8,0},{16,8},{24,16},{1,25},{9,1},{17,9},{25,17},{2,26},{10... | collective-permute-start | bytes 786440 | tf_op jit(solution)/shard_map/ppermute | solution.py:23
  46.6 8.5 %collective-permute-start.22 = (bf16[128,1024]{1,0:T(8,128)(2,1)S(1)}, bf16[128,1024]{1,0:T(8,128)(2,1)S(1)}, u32[]{:S(2)}, u32[]{:S(2)}) collective-permute-start(bf16[128,1024]{1,0:T(8,128)(2,1)S(1)} %copy-done.3), channel_id=1, source_target_pairs={{0,16},{8,24},{16,0},{24,8},{1,17},{9,25},{17,1},{25,9},{2,18},{10... | collective-permute-start | bytes 786440 | tf_op jit(solution)/shard_map/ppermute | solution.py:23
  50.2 9.5 %collective-permute-start.10 = (bf16[4,32,1024]{2,1,0:T(8,128)(2,1)S(1)}, bf16[4,32,1024]{2,1,0:T(8,128)(2,1)S(1)}, u32[]{:S(2)}, u32[]{:S(2)}) collective-permute-start(bf16[4,32,1024]{2,1,0:T(8,128)(2,1)S(1)} %pad_maximum_fusion.5.m0), channel_id=1, source_target_pairs={{0,24},{8,0},{16,8},{24,16},{1,25},{9,1},{17,9},{25,17},{2,26},{10... | collective-permute-start | bytes 786440 | tf_op jit(solution)/shard_map/ppermute | solution.py:23
  51.7 10.7 %collective-permute-start.11 = (bf16[4,32,1024]{2,1,0:T(8,128)(2,1)S(1)}, bf16[4,32,1024]{2,1,0:T(8,128)(2,1)S(1)}, u32[]{:S(2)}, u32[]{:S(2)}) collective-permute-start(bf16[4,32,1024]{2,1,0:T(8,128)(2,1)S(1)} %pad_maximum_fusion.5.m0), channel_id=1, source_target_pairs={{0,16},{8,24},{16,0},{24,8},{1,17},{9,25},{17,1},{25,9},{2,18},{10... | collective-permute-start | bytes 786440 | tf_op jit(solution)/shard_map/ppermute | solution.py:23
  55.1 12.1 %collective-permute-start.9 = (bf16[4,32,1024]{2,1,0:T(8,128)(2,1)S(1)}, bf16[4,32,1024]{2,1,0:T(8,128)(2,1)S(1)}, u32[]{:S(2)}, u32[]{:S(2)}) collective-permute-start(bf16[4,32,1024]{2,1,0:T(8,128)(2,1)S(1)} %pad_maximum_fusion.5.m0), channel_id=1, source_target_pairs={{0,8},{8,16},{16,24},{24,0},{1,9},{9,17},{17,25},{25,1},{2,10},{10... | collective-permute-start | bytes 786440 | tf_op jit(solution)/shard_map/ppermute | solution.py:23
  59.7 38.8 %collective-permute-start.23 = (bf16[4,128,1024]{2,1,0:T(8,128)(2,1)S(1)}, bf16[4,128,1024]{2,1,0:T(8,128)(2,1)S(1)}, u32[]{:S(2)}, u32[]{:S(2)}) collective-permute-start(bf16[4,128,1024]{2,1,0:T(8,128)(2,1)S(1)} %pad_maximum_fusion.2.b0), channel_id=1, source_target_pairs={{0,32},{32,64},{64,96},{96,128},{128,160},{160,192},{192,224},{224... | collective-permute-start | bytes 3145736 | tf_op jit(solution)/shard_map/ppermute | solution.py:23
  67.5 7.7 %copy-start = (bf16[1,1024,256]{2,1,0:T(8,128)(2,1)S(1)}, bf16[1,1024,256]{2,1,0:T(8,128)(2,1)}, u32[]{:S(2)}) copy-start(bf16[1,1024,256]{2,1,0:T(8,128)(2,1)} %param.12) | copy-start | bytes 1572868
  67.6 7.7 %copy-start.1 = (bf16[4,128,128]{2,1,0:T(8,128)(2,1)S(1)}, bf16[4,128,128]{2,1,0:T(8,128)(2,1)}, u32[]{:S(2)}) copy-start(bf16[4,128,128]{2,1,0:T(8,128)(2,1)} %refs_8_.1) | copy-start | bytes 393220
  67.6 6.9 %collective-permute-start.16 = (bf16[528,256]{1,0:T(8,128)(2,1)S(1)}, bf16[528,256]{1,0:T(8,128)(2,1)S(1)}, u32[]{:S(2)}, u32[]{:S(2)}) collective-permute-start(bf16[528,256]{1,0:T(8,128)(2,1)S(1)} %get-tuple-element.28.refs_11_), channel_id=1, source_target_pairs={{0,2},{2,4},{4,6},{6,0},{1,3},{3,5},{5,7},{7,1},{8,10},{10,12},{12... | collective-permute-start | bytes 811016 | tf_op jit(solution)/shard_map/ppermute | solution.py:23
  68.0 10.7 %collective-permute-start.17 = (bf16[528,256]{1,0:T(8,128)(2,1)S(1)}, bf16[528,256]{1,0:T(8,128)(2,1)S(1)}, u32[]{:S(2)}, u32[]{:S(2)}) collective-permute-start(bf16[528,256]{1,0:T(8,128)(2,1)S(1)} %get-tuple-element.28.refs_11_), channel_id=1, source_target_pairs={{0,6},{2,0},{4,2},{6,4},{1,7},{3,1},{5,3},{7,5},{8,14},{10,8},{12,... | collective-permute-start | bytes 811016 | tf_op jit(solution)/shard_map/ppermute | solution.py:23
  70.4 10.7 %collective-permute-start.18 = (bf16[528,256]{1,0:T(8,128)(2,1)S(1)}, bf16[528,256]{1,0:T(8,128)(2,1)S(1)}, u32[]{:S(2)}, u32[]{:S(2)}) collective-permute-start(bf16[528,256]{1,0:T(8,128)(2,1)S(1)} %get-tuple-element.28.refs_11_), channel_id=1, source_target_pairs={{0,4},{2,6},{4,0},{6,2},{1,5},{3,7},{5,1},{7,3},{8,12},{10,14},{12... | collective-permute-start | bytes 811016 | tf_op jit(solution)/shard_map/ppermute | solution.py:23
  74.5 28.8 %collective-permute-start.24 = (bf16[4,128,1024]{2,1,0:T(8,128)(2,1)S(1)}, bf16[4,128,1024]{2,1,0:T(8,128)(2,1)S(1)}, u32[]{:S(2)}, u32[]{:S(2)}) collective-permute-start(bf16[4,128,1024]{2,1,0:T(8,128)(2,1)S(1)} %pad_maximum_fusion.2.b0), channel_id=1, source_target_pairs={{0,224},{32,0},{64,32},{96,64},{128,96},{160,128},{192,160},{224,1... | collective-permute-start | bytes 3145736 | tf_op jit(solution)/shard_map/ppermute | solution.py:23
  74.6 30.5 %collective-permute-start.28 = (bf16[4,128,1024]{2,1,0:T(8,128)(2,1)S(1)}, bf16[4,128,1024]{2,1,0:T(8,128)(2,1)S(1)}, u32[]{:S(2)}, u32[]{:S(2)}) collective-permute-start(bf16[4,128,1024]{2,1,0:T(8,128)(2,1)S(1)} %pad_maximum_fusion.3.b0), channel_id=1, source_target_pairs={{0,8},{8,16},{16,24},{24,0},{1,9},{9,17},{17,25},{25,1},{2,10},{10... | collective-permute-start | bytes 3145736 | tf_op jit(solution)/shard_map/ppermute | solution.py:23
  78.7 7.8 %collective-permute-start.12 = (bf16[512,128]{1,0:T(8,128)(2,1)S(1)}, bf16[512,128]{1,0:T(8,128)(2,1)S(1)}, u32[]{:S(2)}, u32[]{:S(2)}) collective-permute-start(bf16[512,128]{1,0:T(8,128)(2,1)S(1)} %get-tuple-element.27), channel_id=1, source_target_pairs={{0,2},{2,4},{4,6},{6,0},{1,3},{3,5},{5,7},{7,1},{8,10},{10,12},{12... | collective-permute-start | bytes 393224 | tf_op jit(solution)/shard_map/ppermute | solution.py:23
  81.0 7.1 %collective-permute-start.13 = (bf16[512,128]{1,0:T(8,128)(2,1)S(1)}, bf16[512,128]{1,0:T(8,128)(2,1)S(1)}, u32[]{:S(2)}, u32[]{:S(2)}) collective-permute-start(bf16[512,128]{1,0:T(8,128)(2,1)S(1)} %get-tuple-element.27), channel_id=1, source_target_pairs={{0,6},{2,0},{4,2},{6,4},{1,7},{3,1},{5,3},{7,5},{8,14},{10,8},{12,... | collective-permute-start | bytes 393224 | tf_op jit(solution)/shard_map/ppermute | solution.py:23
  86.5 9.2 %collective-permute-start.14 = (bf16[512,128]{1,0:T(8,128)(2,1)S(1)}, bf16[512,128]{1,0:T(8,128)(2,1)S(1)}, u32[]{:S(2)}, u32[]{:S(2)}) collective-permute-start(bf16[512,128]{1,0:T(8,128)(2,1)S(1)} %get-tuple-element.27), channel_id=1, source_target_pairs={{0,4},{2,6},{4,0},{6,2},{1,5},{3,7},{5,1},{7,3},{8,12},{10,14},{12... | collective-permute-start | bytes 393224 | tf_op jit(solution)/shard_map/ppermute | solution.py:23
  88.2 31.8 %collective-permute-start.19 = (bf16[4,528,256]{2,1,0:T(8,128)(2,1)S(1)}, bf16[4,528,256]{2,1,0:T(8,128)(2,1)S(1)}, u32[]{:S(2)}, u32[]{:S(2)}) collective-permute-start(bf16[4,528,256]{2,1,0:T(8,128)(2,1)S(1)} %pad_maximum_fusion.1), channel_id=1, source_target_pairs={{0,1},{1,0},{2,3},{3,2},{4,5},{5,4},{6,7},{7,6},{8,9},{9,8},{10,11... | collective-permute-start | bytes 3244040 | tf_op jit(solution)/shard_map/ppermute | solution.py:23
  95.7 21.1 %collective-permute-start.29 = (bf16[4,128,1024]{2,1,0:T(8,128)(2,1)S(1)}, bf16[4,128,1024]{2,1,0:T(8,128)(2,1)S(1)}, u32[]{:S(2)}, u32[]{:S(2)}) collective-permute-start(bf16[4,128,1024]{2,1,0:T(8,128)(2,1)S(1)} %pad_maximum_fusion.3.b0), channel_id=1, source_target_pairs={{0,24},{8,0},{16,8},{24,16},{1,25},{9,1},{17,9},{25,17},{2,26},{10... | collective-permute-start | bytes 3145736 | tf_op jit(solution)/shard_map/ppermute | solution.py:23
  98.6 22.0 %collective-permute-start.15 = (bf16[3,512,128]{2,1,0:T(8,128)(2,1)S(1)}, bf16[3,512,128]{2,1,0:T(8,128)(2,1)S(1)}, u32[]{:S(2)}, u32[]{:S(2)}) collective-permute-start(bf16[3,512,128]{2,1,0:T(8,128)(2,1)S(1)} %pad_maximum_fusion.4), channel_id=1, source_target_pairs={{0,1},{1,0},{2,3},{3,2},{4,5},{5,4},{6,7},{7,6},{8,9},{9,8},{10,11... | collective-permute-start | bytes 1179656 | tf_op jit(solution)/shard_map/ppermute | solution.py:23
  103.3 20.7 %collective-permute-start.25 = (bf16[2,128,1024]{2,1,0:T(8,128)(2,1)S(1)}, bf16[2,128,1024]{2,1,0:T(8,128)(2,1)S(1)}, u32[]{:S(2)}, u32[]{:S(2)}) collective-permute-start(bf16[2,128,1024]{2,1,0:T(8,128)(2,1)S(1)} %slice.75), channel_id=1, source_target_pairs={{0,32},{32,64},{64,96},{96,128},{128,160},{160,192},{192,224},{224... | collective-permute-start | bytes 1572872 | tf_op jit(solution)/shard_map/ppermute | solution.py:23
  105.1 18.8 %collective-permute-start.26 = (bf16[2,128,1024]{2,1,0:T(8,128)(2,1)S(1)}, bf16[2,128,1024]{2,1,0:T(8,128)(2,1)S(1)}, u32[]{:S(2)}, u32[]{:S(2)}) collective-permute-start(bf16[2,128,1024]{2,1,0:T(8,128)(2,1)S(1)} %slice.76), channel_id=1, source_target_pairs={{0,224},{32,0},{64,32},{96,64},{128,96},{160,128},{192,160},{224,1... | collective-permute-start | bytes 1572872 | tf_op jit(solution)/shard_map/ppermute | solution.py:23
  116.8 13.7 %collective-permute-start.30 = (bf16[2,128,1024]{2,1,0:T(8,128)(2,1)S(1)}, bf16[2,128,1024]{2,1,0:T(8,128)(2,1)S(1)}, u32[]{:S(2)}, u32[]{:S(2)}) collective-permute-start(bf16[2,128,1024]{2,1,0:T(8,128)(2,1)S(1)} %slice.80), channel_id=1, source_target_pairs={{0,8},{8,16},{16,24},{24,0},{1,9},{9,17},{17,25},{25,1},{2,10},{10... | collective-permute-start | bytes 1572872 | tf_op jit(solution)/shard_map/ppermute | solution.py:23
  119.9 10.6 %collective-permute-start.31 = (bf16[2,128,1024]{2,1,0:T(8,128)(2,1)S(1)}, bf16[2,128,1024]{2,1,0:T(8,128)(2,1)S(1)}, u32[]{:S(2)}, u32[]{:S(2)}) collective-permute-start(bf16[2,128,1024]{2,1,0:T(8,128)(2,1)S(1)} %slice.81), channel_id=1, source_target_pairs={{0,24},{8,0},{16,8},{24,16},{1,25},{9,1},{17,9},{25,17},{2,26},{10... | collective-permute-start | bytes 1572872 | tf_op jit(solution)/shard_map/ppermute | solution.py:23
  135.8 11.8 %collective-permute-start.32 = (bf16[3,1024,256]{2,1,0:T(8,128)(2,1)S(1)}, bf16[3,1024,256]{2,1,0:T(8,128)(2,1)S(1)}, u32[]{:S(2)}, u32[]{:S(2)}) collective-permute-start(bf16[3,1024,256]{2,1,0:T(8,128)(2,1)S(1)} %get-tuple-element.36), channel_id=1, source_target_pairs={{0,1},{1,0},{2,3},{3,2},{4,5},{5,4},{6,7},{7,6},{8,9},{9,8},{10,11... | collective-permute-start | bytes 4718600 | tf_op jit(solution)/shard_map/ppermute | solution.py:23
  143.3 2.2 %collective-permute-start.33 = (bf16[1,1024,256]{2,1,0:T(8,128)(2,1)S(1)}, bf16[1,1024,256]{2,1,0:T(8,128)(2,1)S(1)}, u32[]{:S(2)}, u32[]{:S(2)}) collective-permute-start(bf16[1,1024,256]{2,1,0:T(8,128)(2,1)S(1)} %get-tuple-element.38), channel_id=1, source_target_pairs={{0,1},{1,0},{2,3},{3,2},{4,5},{5,4},{6,7},{7,6},{8,9},{9,8},{10,11... | collective-permute-start | bytes 1572872 | tf_op jit(solution)/shard_map/ppermute | solution.py:23
  145.6 14.7 %collective-permute-start.34 = (bf16[1024,256]{1,0:T(8,128)(2,1)S(1)}, bf16[1024,256]{1,0:T(8,128)(2,1)S(1)}, u32[]{:S(2)}, u32[]{:S(2)}) collective-permute-start(bf16[1024,256]{1,0:T(8,128)(2,1)S(1)} %fusion.4), channel_id=1, source_target_pairs={{0,4},{2,6},{4,0},{6,2},{1,5},{3,7},{5,1},{7,3},{8,12},{10,14},{12... | collective-permute-start | bytes 1572872 | tf_op jit(solution)/shard_map/ppermute | solution.py:23
  147.8 24.5 %collective-permute-start.35 = (bf16[1024,256]{1,0:T(8,128)(2,1)S(1)}, bf16[1024,256]{1,0:T(8,128)(2,1)S(1)}, u32[]{:S(2)}, u32[]{:S(2)}) collective-permute-start(bf16[1024,256]{1,0:T(8,128)(2,1)S(1)} %get-tuple-element.39), channel_id=1, source_target_pairs={{0,2},{2,4},{4,6},{6,0},{1,3},{3,5},{5,7},{7,1},{8,10},{10,12},{12... | collective-permute-start | bytes 1572872 | tf_op jit(solution)/shard_map/ppermute | solution.py:23
  147.9 24.4 %collective-permute-start.36 = (bf16[1024,256]{1,0:T(8,128)(2,1)S(1)}, bf16[1024,256]{1,0:T(8,128)(2,1)S(1)}, u32[]{:S(2)}, u32[]{:S(2)}) collective-permute-start(bf16[1024,256]{1,0:T(8,128)(2,1)S(1)} %get-tuple-element.40), channel_id=1, source_target_pairs={{0,6},{2,0},{4,2},{6,4},{1,7},{3,1},{5,3},{7,5},{8,14},{10,8},{12,... | collective-permute-start | bytes 1572872 | tf_op jit(solution)/shard_map/ppermute | solution.py:23
where the time goes:
time: 174 us
  starting transfers between devices  74.1 us (43%)
  waiting for transfers between devices  68.8 us (40%)
  Pallas kernels  23.9 us (14%)
  local copies, waits for them, and re-layouts  3.5 us (2%)
  other arithmetic  2.91 us (2%)
    ppermute x37, starting transfers between devices, send(): lax.ppermute(array, axes, [(i, (i + shift) % count) for i in range(count)])  74.1 us
    ppermute x37, waiting for transfers between devices, send(): lax.ppermute(array, axes, [(i, (i + shift) % count) for i in range(count)])  68.8 us
    pallas_call x7, Pallas kernels, call(): pl.pallas_call(kernel, out_shape=out_shape, in_specs=[VMEM] * (len(args)...  23.9 us
  transfers between devices with their start and end apart: 37, of which 14 were waited for; matrix products, arithmetic and copies ran while one was open for 3% of the time, Pallas kernels for 11%

commit v1 on v0

--- a/solution.py
+++ b/solution.py
@@ -67,101 +67,106 @@
 
 
 def prep_kernel(
-    w_in, w_in_other, norm_gain_at, w_out_at, s_out_at, ffn_gain_at, w_up_at, s_up_at, w_down_at, s_down_at,
-    up, packet, top, bottom, small, norm_gain, w_out, s_out, ffn_gain, w_up, s_up, w_down, s_down, done,
+    norm_gain_at, w_in_at, s_in_at, w_out_at, s_out_at, ffn_gain_at, w_up_at, s_up_at, w_down_at, s_down_at,
+    mixer, up, down, small, norm_gain, w_in, s_in, w_out, s_out, ffn_gain, w_up, s_up, w_down, s_down, done,
 ):
-    sources = (w_up_at, ffn_gain_at, w_down_at, s_down_at, norm_gain_at, w_out_at, s_out_at, s_up_at)
-    targets = (w_up, ffn_gain, w_down, s_down, norm_gain, w_out, s_out, s_up)
+    sources = (norm_gain_at, w_in_at, s_in_at, w_out_at, s_out_at, s_up_at, ffn_gain_at, w_up_at, w_down_at, s_down_at)
+    targets = (norm_gain, w_in, s_in, w_out, s_out, s_up, ffn_gain, w_up, w_down, s_down)
     copies = [pltpu.make_async_copy(a, b, done.at[k]) for k, (a, b) in enumerate(zip(sources, targets))]
     for copy in copies:
         copy.start()
-    for copy in copies:
+    for copy in copies[:6]:
         copy.wait()
-    c = lax.axis_index("c")
     f = 4 * lax.axis_index("z") + lax.axis_index("y")
+    own = jnp.concatenate([w_in[...]] * 2, axis=0).T * column_of(norm_gain[pl.ds(f, 1), :])
+    low_lanes = lax.broadcasted_iota(jnp.int32, (8, 128), 1) < 64
+    for j in range(8):
+        lanes = slice(j * 128, j * 128 + 128)
+        small[0:8, lanes] = jnp.where(low_lanes, own[j * 16 : j * 16 + 8], own[j * 16 + 8 : j * 16 + 16])
+    for j in range(4):
+        small[8:16, j * 256 : j * 256 + 256] = w_out[j * 8 : j * 8 + 8, :]
+    small[16:24] = jnp.zeros((8, 1024), F32)
+    for row, at in ((s_out[...], 0), (s_in[...], 256), (s_up[...], 512)):
+        high, low = two_parts(row)
+        small[16:17, at : at + row.shape[1]] = high
+        small[16:17, at + 128 : at + 128 + row.shape[1]] = low
+    mixer[...] = small[...].astype(BF)
+    for copy in copies[6:]:
+        copy.wait()
     gain = column_of(ffn_gain[pl.ds(f, 1), :])
     for j in range(8):
         lanes = slice(j * 128, j * 128 + 128)
         up[:, lanes] = (w_up[:, lanes] * gain).astype(BF)
-        packet[:128, lanes] = (w_down[lanes, :] * s_down[...]).T.astype(BF)
-    gain = column_of(norm_gain[pl.ds(f, 1), :])
-    mine, other = w_in[:128], w_in_other[:128]
-    pair = jnp.concatenate(
-        [jnp.where(c == 0, mine, other), jnp.where(c == 0, other, mine)], axis=1
-    )
-    pair = pair * gain
-    for j in range(8):
-        small[0:16, j * 128 : j * 128 + 128] = pair[j * 16 : j * 16 + 16]
-    for j in range(4):
-        small[16:24, j * 256 : j * 256 + 256] = w_out[j * 8 : j * 8 + 8, :]
-    small[24:32] = jnp.zeros((8, 1024), F32)
-    mine, other = w_in[128:129, :4], w_in_other[128:129, :4]
-    rows = (
-        (s_out[...], 0),
-        (jnp.where(c == 0, mine, other), 256),
-        (jnp.where(c == 0, other, mine), 512),
-        (s_up[...], 768),
-    )
-    for row, at in rows:
-        high, low = two_parts(row)
-        small[24:25, at : at + row.shape[1]] = high
-        small[24:25, at + 128 : at + 128 + row.shape[1]] = low
-    packet[128:] = small[...].astype(BF)
-    top[...] = packet[:80]
-    bottom[...] = packet[80:]
-
-
-def unpack_kernel(m0, m1, m2, m3, w_in, w_out, s_in, s_up):
+        down[:, lanes] = (w_down[lanes, :] * s_down[...]).T.astype(BF)
+
+
+def unpack_kernel(m0, m1, m2, m3, w_in, w_out, s_up):
     ys, zs = around(lax.axis_index("y")), around(lax.axis_index("z"))
-    w_out[512:] = jnp.zeros((16, 256), BF)
     lane = lax.broadcasted_iota(jnp.int32, (16, 128), 1)
     at = lax.broadcasted_iota(jnp.int32, (16, 128), 0)
-    firsts = [jnp.zeros((16, 128), F32) for _ in range(8)]
+    low_lanes = lane[:8] < 64
+    firsts = [jnp.zeros((16, 128), F32) for _ in range(6)]
     for m, yy in zip((m0, m1, m2, m3), ys):
         for k, zz in enumerate(zs):
             f = 4 * zz + yy
-            block = m[k]
+            block = m[k].astype(F32)
             for j in range(8):
-                w_in[pl.ds(pl.multiple_of(f * 128 + j * 16, 16), 16), :] = block[:16, j * 128 : j * 128 + 128]
-            low = block[16:32].astype(F32)
-            rows = jnp.concatenate([low[:8, j * 256 : j * 256 + 256] for j in range(4)], axis=0)
+                part = block[:8, j * 128 : j * 128 + 128]
+                turned = pltpu.roll(part, 64, 1)
+                rows = jnp.concatenate(
+                    [jnp.where(low_lanes, part, turned), jnp.where(low_lanes, turned, part)], axis=0
+                )
+                w_in[pl.ds(pl.multiple_of(f * 128 + j * 16, 16), 16), :] = rows.astype(BF)
+            rows = jnp.concatenate([block[8:16, j * 256 : j * 256 + 256] for j in range(4)], axis=0)
             w_out[pl.ds(pl.multiple_of(f * 32, 32), 32), :] = rows.astype(BF)
-            for j in range(8):
-                row = jnp.broadcast_to(low[8:9, j * 128 : j * 128 + 128], (16, 128))
+            for j in range(6):
+                row = jnp.broadcast_to(block[16:17, j * 128 : j * 128 + 128], (16, 128))
                 firsts[j] = jnp.where(at == f, row, firsts[j])
 
-    def flat(rows, width):
+    def flat(rows, width, copies=1):
         pieces = []
-        for group in range(16 * width // 128):
+        count = min(16, 128 // width)
+        for group in range(16 // count):
             total = jnp.zeros((1, 128), F32)
-            for i in range(128 // width):
-                source = group * (128 // width) + i
+            for i in range(count):
+                source = group * count + i
                 row = jnp.where(lane[:1] < width, rows[source : source + 1], 0.0)
-                total += pltpu.roll(row, i * width, 1) if i else row
+                for again in range(copies):
+                    shift = i * width + 64 * again
+                    total += pltpu.roll(row, shift, 1) if shift else row
             pieces.append(total)
         return jnp.concatenate(pieces, axis=1) if len(pieces) > 1 else pieces[0]
 
     w_out[512:528] = jnp.concatenate(
         [flat(firsts[0], 16), flat(firsts[1], 16), jnp.zeros((14, 256), F32)], axis=0
     ).astype(BF)
-    both = [firsts[2] + firsts[3], firsts[4] + firsts[5]]
-    both = jnp.where(lane < 4, both[0], 0.0) + pltpu.roll(jnp.where(lane < 4, both[1], 0.0), 64, 1)
-    total = jnp.zeros((1, 128), F32)
-    for i in range(16):
-        row = both[i : i + 1]
-        total += pltpu.roll(row, 4 * i, 1) if i else row
-    s_in[...] = total
-    s_up[...] = flat(firsts[6] + firsts[7], 64)
+    w_in[2048:2064] = jnp.concatenate(
+        [flat(firsts[2], 4, 2), flat(firsts[3], 4, 2), jnp.zeros((14, 128), F32)], axis=0
+    ).astype(BF)
+    s_up[...] = flat(firsts[4] + firsts[5], 64)
 
 
 def piece_refs(refs):
-    return list(refs[:5]) + [refs[5].at[k] for k in range(3)]
+    return list(refs[:4]) + [refs[4].at[k] for k in range(4)]
 
 
 def pool_kernel(*refs):
-    pieces, (w_in, s_in, pool_w, out, mine, padded) = piece_refs(refs), refs[6:]
-    x, whose = lax.axis_index("x"), owners()
-    first = pl.ds(pl.multiple_of(lax.axis_index("c") * 512, 512), 512)
+    pieces, (w_own, w_other, pool_w, out, mine, padded, w_in) = piece_refs(refs), refs[5:]
+    x, c, whose = lax.axis_index("x"), lax.axis_index("c"), owners()
+    first = pl.ds(pl.multiple_of(c * 512, 512), 512)
+
+    @pl.when(c == 0)
+    def _():
+        w_in[:, :64] = w_own[:, :64]
+        w_in[:, 64:] = w_other[:, 64:]
+
+    @pl.when(c == 1)
+    def _():
+        w_in[:, :64] = w_other[:, :64]
+        w_in[:, 64:] = w_own[:, 64:]
+
+    tail = w_in[2048:2064].astype(F32)
+    s_in = tail[0:1] + tail[1:2]
     padded[0:128] = jnp.zeros((128, 128), BF)
     padded[128 + SEQ :] = jnp.zeros((128, 128), BF)
 
@@ -177,7 +182,7 @@
             wide = wide * wide
             squares += wide[:, :128] + wide[:, 128:]
         scale = lax.rsqrt(jnp.sum(squares, axis=1, keepdims=True) / 2048 + EPS)
-        padded[pl.ds(pl.multiple_of(128 + block * 256, 128), 256), :] = (total * scale * s_in[...]).astype(BF)
+        padded[pl.ds(pl.multiple_of(128 + block * 256, 128), 256), :] = (total * scale * s_in).astype(BF)
 
     half = jnp.left_shift(1, x)
     row = lax.broadcasted_iota(jnp.int32, (256, 512), 0)
@@ -198,9 +203,9 @@
 
 
 def mix_kernel(*refs):
-    pieces, grouped, near, across = piece_refs(refs), refs[6], refs[7:10], refs[10]
-    weights = list(refs[11:15]) + [refs[15].at[k] for k in range(4)]
-    mixed, own, factor = refs[16:]
+    pieces, grouped, near, across = piece_refs(refs), refs[5], refs[6:9], refs[9]
+    weights = list(refs[10:14]) + [refs[14].at[k] for k in range(4)]
+    mixed, own, factor = refs[15:]
     chips, whose = around(lax.axis_index("x")), owners()
     c = lax.axis_index("c")
 
@@ -260,7 +265,7 @@
     def _(step):
         rows = pl.ds(pl.multiple_of(lax.rem(step, 2) * 512, 512), 512)
         k = lax.div(step, 2)
-        chip = lax.rem(x + (lax.rem(2 * k + 1, 5) if len(steps) > 1 else steps[0]), 4)
+        chip = lax.rem(x + ((2 * k + 1) if len(steps) > 1 else steps[0]), 4)
         away = lax.rem(chip - z + 4, 4)
         place = jnp.where(away == 0, 0, jnp.where(away == 1, 2, jnp.where(away == 2, 3, 1)))
         inner = jnp.bitwise_and(place, 1)
@@ -283,9 +288,13 @@
     return [bundle, low, high, send(low[:2], axes, 1), send(high[2:], axes, -1)]
 
 
+def three(array, axes):
+    far = send(array, axes, 2)
+    return [send(array, axes, 1), send(array, axes, -1), far]
+
+
 def near_three(array):
-    far = send(array, "x", 2)
-    return [send(array, "x", 1), send(array, "x", -1), far]
+    return three(array, "x")
 
 
 def bf(*shape):
@@ -304,15 +313,12 @@
 
     near = near_three(tokens)
     pieces = [tokens] + near
-    both_in = jnp.concatenate([w_in, jnp.pad(s_in[None], ((0, 7), (0, 60)))], axis=0)
-    other_in = swapped(both_in)
-    pieces.append(swapped(tokens))
-    pieces.append(swapped(jnp.stack(near)))
+    pieces.append(swapped(jnp.stack(pieces)))
 
     arrays = (
-        both_in,
-        other_in,
         norm_gain.reshape(16, 128),
+        w_in.T,
+        s_in[None],
         w_out,
         s_out[None],
         ffn_gain.reshape(16, 128),
@@ -321,54 +327,37 @@
         w_down,
         s_down[None],
     )
-    up, packet, top, bottom = call(
+    packet, up, down = call(
         prep_kernel,
-        (bf(128, 1024), bf(160, 1024), bf(80, 1024), bf(80, 1024)),
-        [pltpu.VMEM((32, 1024), F32)]
-        + [pltpu.VMEM(a.shape, F32) for a in arrays[2:]]
-        + [pltpu.SemaphoreType.DMA((8,))],
+        (bf(24, 1024), bf(128, 1024), bf(128, 1024)),
+        [pltpu.VMEM((24, 1024), F32)]
+        + [pltpu.VMEM(a.shape, F32) for a in arrays]
+        + [pltpu.SemaphoreType.DMA((10,))],
         60,
         1_000_000,
         *arrays,
-        in_hbm=8,
-    )
-    low, high = send(packet, ring_z, 1), send(packet, ring_z, -1)
-    far_top, far_bottom = send(top, ring_z, 2), send(bottom, ring_z, -2)
-    up_far, up_low, up_high = send(up, "y", 2), send(up, "y", 1), send(up, "y", -1)
-
-    mixer = jnp.stack([packet[128:], low[128:], high[128:], far_bottom[48:]])
-    far = send(mixer, "y", 2)
-    mixers = [mixer, send(mixer, "y", 1), send(mixer, "y", -1), far]
-    w_in_all, out_own, s_in_row, s_up_row = call(
-        unpack_kernel,
-        (bf(2048, 128), bf(528, 256), f32(1, 128), f32(1, 1024)),
-        [],
-        8,
-        1_000_000,
-        *mixers,
-    )
-    up_parts = along(jnp.stack([up, up_low, up_high, up_far]), ring_z)
-    down_parts = along(
-        jnp.stack(
-            [
-                packet[:128],
-                low[:128],
-                high[:128],
-                jnp.concatenate([far_top, far_bottom[:48]], axis=0),
-            ]
-        ),
-        "y",
-    )
-
+        in_hbm=10,
+    )
+    mixer = jnp.stack([packet] + three(packet, ring_z))
+    up_bundle = [up] + three(up, "y")
+    down_bundle = [down] + three(down, ring_z)
+    mixers = [mixer] + three(mixer, "y")
+    up_parts = along(jnp.stack(up_bundle), ring_z)
+    down_parts = along(jnp.stack(down_bundle), "y")
+    w_in_own, out_own, s_up_row = call(
+        unpack_kernel, (bf(2064, 128), bf(528, 256), f32(1, 1024)), [], 8, 1_000_000, *mixers
+    )
+
+    w_in_other = swapped(w_in_own)
     grouped, mine = call(
         pool_kernel,
         (bf(SEQ, 128), bf(512, 128)),
-        [pltpu.VMEM((SEQ + 256, 128), BF)],
+        [pltpu.VMEM((SEQ + 256, 128), BF), pltpu.VMEM((2064, 128), BF)],
         16,
         800_000_000,
         *pieces,
-        w_in_all,
-        s_in_row,
+        w_in_own,
+        w_in_other,
         pool_w,
     )
     near = near_three(mine)
@@ -391,8 +380,8 @@
     hidden = call(
         up_kernel, bf(SEQ, 1024), [], 32, 4_300_000_000, mixed, factor, s_up_row, *up_parts
     )
-    chips = []
-    for steps in ((2,), (1, 3, 0)):
+
+    def block_sums(steps):
         count = len(steps)
         own, other = call(
             functools.partial(down_kernel, steps),
@@ -404,10 +393,16 @@
             *down_parts,
         )
         crossed = swapped(other)
-        chips += [own[k].astype(F32) + crossed[k].astype(F32) for k in range(count)]
-    total = mixed_own.astype(F32) + chips[3]
-    for k, shift in enumerate((2, 1, -1)):
-        total = total + send(chips[k].astype(BF), "x", shift).astype(F32)
+        return [own[k].astype(F32) + crossed[k].astype(F32) for k in range(count)]
+
+    (far,) = block_sums((2,))
+    from_low, from_high = send(far[:512].astype(BF), "x", 1), send(far[512:].astype(BF), "x", -1)
+    after, before = block_sums((1, 3))
+    (here,) = block_sums((0,))
+    after = jnp.concatenate([after[:512] + from_low.astype(F32), after[512:]], axis=0)
+    before = jnp.concatenate([before[:512], before[512:] + from_high.astype(F32)], axis=0)
+    low, high = send(after.astype(BF), "x", 1), send(before.astype(BF), "x", -1)
+    total = mixed_own.astype(F32) + here + low.astype(F32) + high.astype(F32)
     return total.astype(BF)[None]
 
 

time: 174 us -> 179 us (1.029)
  waiting for transfers between devices: 68.8 us -> 86.7 us
  starting transfers between devices: 74.1 us -> 60.6 us
  other arithmetic: 2.91 us -> 6.75 us
  local copies, waits for them, and re-layouts: 3.5 us -> 0.24 us
    ppermute x37 -> x40, waiting for transfers between devices: 68.8 us -> 86.7 us  [send(): lax.ppermute(array, axes, [(i, (i + shift) % count) for i in range(count)])]
    ppermute x37 -> x40, starting transfers between devices: 74.1 us -> 60.6 us  [send(): lax.ppermute(array, axes, [(i, (i + shift) % count) for i in range(count)])]
    another operation x5 -> x7, other arithmetic: 0.49 us -> 5.05 us  [the longest x1 2.64 us: layer(): pieces.append(swapped(jnp.stack(pieces)))]
    another operation x7 -> x0, local copies, waits for them, and re-layouts: 1.87 us -> none  [the longest x3 1 us: layer(): jnp.stack([packet[:128], low[:128], high[:128], jnp.concatenate([far_top,...]
    pallas_call x7 -> x8, Pallas kernels: 23.9 us -> 22.8 us  [call(): pl.pallas_call(kernel, out_shape=out_shape, in_specs=[VMEM] * (len(args)...]
  transfers between devices with their start and end apart: 37 -> 40, of which waited for: 14 -> 17; matrix products, arithmetic and copies ran while one was open for 3% -> 2% of each run, Pallas kernels for 11% -> 11%
where the time goes in v1:
time: 179 us; the launch traced here: 177 us
  waiting for transfers between devices  86.7 us (48%)
  starting transfers between devices  60.6 us (34%)
  Pallas kernels  22.8 us (13%)
  other arithmetic  6.75 us (4%)
    ppermute x40, waiting for transfers between devices, send(): lax.ppermute(array, axes, [(i, (i + shift) % count) for i in range(count)])  86.7 us
    ppermute x40, starting transfers between devices, send(): lax.ppermute(array, axes, [(i, (i + shift) % count) for i in range(count)])  60.6 us
    pallas_call x8, Pallas kernels, call(): pl.pallas_call(kernel, out_shape=out_shape, in_specs=[VMEM] * (len(args)...  22.8 us
  transfers between devices with their start and end apart: 40, of which 17 were waited for; matrix products, arithmetic and copies ran while one was open for 2% of the time, Pallas kernels for 11%

profile of v1, /device:TPU:1, one launch (start us, length us, event | category | flops | bytes accessed | tf_op | source)
XLA Modules:
  0.0 177.5 jit_solution(7778786560871655533)
XLA Ops:
  0.0 2.0 %collective-permute-start = (bf16[1024,256]{1,0:T(8,128)(2,1)}, bf16[1024,256]{1,0:T(8,128)(2,1)S(1)}, u32[]{:S(2)}, u32[]{:S(2)}) collective-permute-start(bf16[1024,256]{1,0:T(8,128)(2,1)} %bitcast.62), channel_id=1, source_target_pairs={{0,2},{2,4},{4,6},{6,0},{1,3},{3,5},{5,7},{7,1},{8,10},{10,12},{12... | collective-permute-start | bytes 1572872 | tf_op jit(solution)/shard_map/ppermute | solution.py:23
  2.0 1.3 collective-permute-start.1
  3.3 1.7 collective-permute-start.2
  5.0 7.9 %collective-permute-done.refs_1_ = bf16[1024,256]{1,0:T(8,128)(2,1)S(1)} collective-permute-done((bf16[1024,256]{1,0:T(8,128)(2,1)}, bf16[1024,256]{1,0:T(8,128)(2,1)S(1)}, u32[]{:S(2)}, u32[]{:S(2)}) %collective-permute-start) | collective-permute-done | bytes 524320 | tf_op jit(solution)/shard_map/ppermute | solution.py:23
  12.9 1.6 collective-permute-done.1.refs_2_
  14.6 12.7 %collective-permute-done.2.refs_3_ = bf16[1024,256]{1,0:T(8,128)(2,1)S(1)} collective-permute-done((bf16[1024,256]{1,0:T(8,128)(2,1)}, bf16[1024,256]{1,0:T(8,128)(2,1)S(1)}, u32[]{:S(2)}, u32[]{:S(2)}) %collective-permute-start.2) | collective-permute-done | bytes 524320 | tf_op jit(solution)/shard_map/ppermute | solution.py:23
  27.3 2.6 %pad_maximum_fusion = bf16[4,1024,256]{2,1,0:T(8,128)(2,1)} fusion(bf16[1,1024,256]{2,1,0:T(8,128)(2,1)S(1)} %bitcast.69, bf16[1,1024,256]{2,1,0:T(8,128)(2,1)S(1)} %bitcast.68, bf16[1,1024,256]{2,1,0:T(8,128)(2,1)S(1)} %bitcast.67, bf16[1,1024,256]{2,1,0:T(8,128)(2,1)} %param.12), kind=kLoop, calls=%fused_computation | loop fusion | flops 3145728 | bytes 4194304 | tf_op jit(solution)/shard_map/stack | solution.py:316
  29.9 1.5 collective-permute-start.3
  31.4 2.3 %shard_map.118 = (bf16[24,1024]{1,0:T(8,128)(2,1)}, bf16[128,1024]{1,0:T(8,128)(2,1)}, bf16[128,1024]{1,0:T(8,128)(2,1)}) custom-call(f32[16,128]{1,0:T(8,128)} %bitcast.90, f32[64,128]{1,0:T(8,128)} %bitcast.89, f32[1,4]{1,0:T(1,128)} %bitcast.92, f32[32,256]{1,0:T(8,128)} %w_out_at.1, f32[1,16]{1,0:T(1,128)} %bitcast.93, f32[16,128]{1,0:T(8,128)} %bitcast.91, ...), custom_call_target="tpu_custom_call" | custom-call | flops 1000000 | bytes 1131344 | tf_op jit(solution)/shard_map/pallas_call | solution.py:54
  33.8 1.7 collective-permute-start.4
  35.5 4.0 %collective-permute-start.5 = (bf16[24,1024]{1,0:T(8,128)(2,1)}, bf16[24,1024]{1,0:T(8,128)(2,1)S(1)}, u32[]{:S(2)}, u32[]{:S(2)}) collective-permute-start(bf16[24,1024]{1,0:T(8,128)(2,1)} %get-tuple-element.22), channel_id=1, source_target_pairs={{0,224},{32,0},{64,32},{96,64},{128,96},{160,128},{192,160},{224,1... | collective-permute-start | bytes 147464 | tf_op jit(solution)/shard_map/ppermute | solution.py:23
  39.5 2.2 %collective-permute-done.4 = bf16[24,1024]{1,0:T(8,128)(2,1)S(1)} collective-permute-done((bf16[24,1024]{1,0:T(8,128)(2,1)}, bf16[24,1024]{1,0:T(8,128)(2,1)S(1)}, u32[]{:S(2)}, u32[]{:S(2)}) %collective-permute-start.4) | collective-permute-done | bytes 49184 | tf_op jit(solution)/shard_map/ppermute | solution.py:23
  41.8 4.3 %collective-permute-done.6 = bf16[24,1024]{1,0:T(8,128)(2,1)S(1)} collective-permute-done((bf16[24,1024]{1,0:T(8,128)(2,1)}, bf16[24,1024]{1,0:T(8,128)(2,1)S(1)}, u32[]{:S(2)}, u32[]{:S(2)}) %collective-permute-start.6) | collective-permute-done | bytes 49184 | tf_op jit(solution)/shard_map/ppermute | solution.py:23
  46.9 1.4 collective-permute-start.7
  48.3 1.5 collective-permute-start.8
  49.8 1.6 collective-permute-start.9
  51.8 2.3 %collective-permute-done.7.m1 = bf16[4,24,1024]{2,1,0:T(8,128)(2,1)S(1)} collective-permute-done((bf16[4,24,1024]{2,1,0:T(8,128)(2,1)S(1)}, bf16[4,24,1024]{2,1,0:T(8,128)(2,1)S(1)}, u32[]{:S(2)}, u32[]{:S(2)}) %collective-permute-start.7) | collective-permute-done | bytes 196640 | tf_op jit(solution)/shard_map/ppermute | solution.py:23
  54.1 1.4 collective-permute-start.20
  56.4 3.1 %collective-permute-done.9.m3 = bf16[4,24,1024]{2,1,0:T(8,128)(2,1)S(1)} collective-permute-done((bf16[4,24,1024]{2,1,0:T(8,128)(2,1)S(1)}, bf16[4,24,1024]{2,1,0:T(8,128)(2,1)S(1)}, u32[]{:S(2)}, u32[]{:S(2)}) %collective-permute-start.9) | collective-permute-done | bytes 196640 | tf_op jit(solution)/shard_map/ppermute | solution.py:23
  59.5 4.7 %collective-permute-done.19 = bf16[128,1024]{1,0:T(8,128)(2,1)S(1)} collective-permute-done((bf16[128,1024]{1,0:T(8,128)(2,1)}, bf16[128,1024]{1,0:T(8,128)(2,1)S(1)}, u32[]{:S(2)}, u32[]{:S(2)}) %collective-permute-start.19) | collective-permute-done | bytes 262176 | tf_op jit(solution)/shard_map/ppermute | solution.py:23
  64.6 6.0 %collective-permute-start.10 = (bf16[2064,128]{1,0:T(8,128)(2,1)S(1)}, bf16[2064,128]{1,0:T(8,128)(2,1)S(1)}, u32[]{:S(2)}, u32[]{:S(2)}) collective-permute-start(bf16[2064,128]{1,0:T(8,128)(2,1)S(1)} %get-tuple-element.23.refs_5_), channel_id=1, source_target_pairs={{0,1},{1,0},{2,3},{3,2},{4,5},{5,4},{6,7},{7,6},{8,9},{9,8},{10,11... | collective-permute-start | bytes 1585160 | tf_op jit(solution)/shard_map/ppermute | solution.py:23
  71.6 1.9 %collective-permute-start.16 = (bf16[528,256]{1,0:T(8,128)(2,1)S(1)}, bf16[528,256]{1,0:T(8,128)(2,1)S(1)}, u32[]{:S(2)}, u32[]{:S(2)}) collective-permute-start(bf16[528,256]{1,0:T(8,128)(2,1)S(1)} %get-tuple-element.26.refs_10_), channel_id=1, source_target_pairs={{0,6},{2,0},{4,2},{6,4},{1,7},{3,1},{5,3},{7,5},{8,14},{10,8},{12,... | collective-permute-start | bytes 811016 | tf_op jit(solution)/shard_map/ppermute | solution.py:23
  74.6 10.7 %collective-permute-done.28 = bf16[128,1024]{1,0:T(8,128)(2,1)S(1)} collective-permute-done((bf16[128,1024]{1,0:T(8,128)(2,1)}, bf16[128,1024]{1,0:T(8,128)(2,1)S(1)}, u32[]{:S(2)}, u32[]{:S(2)}) %collective-permute-start.28) | collective-permute-done | bytes 262176 | tf_op jit(solution)/shard_map/ppermute | solution.py:23
  85.3 2.0 %collective-permute-start.17 = (bf16[528,256]{1,0:T(8,128)(2,1)S(1)}, bf16[528,256]{1,0:T(8,128)(2,1)S(1)}, u32[]{:S(2)}, u32[]{:S(2)}) collective-permute-start(bf16[528,256]{1,0:T(8,128)(2,1)S(1)} %get-tuple-element.26.refs_10_), channel_id=1, source_target_pairs={{0,4},{2,6},{4,0},{6,2},{1,5},{3,7},{5,1},{7,3},{8,12},{10,14},{12... | collective-permute-start | bytes 811016 | tf_op jit(solution)/shard_map/ppermute | solution.py:23
  87.5 2.7 %collective-permute-start.23 = (bf16[4,128,1024]{2,1,0:T(8,128)(2,1)S(1)}, bf16[4,128,1024]{2,1,0:T(8,128)(2,1)S(1)}, u32[]{:S(2)}, u32[]{:S(2)}) collective-permute-start(bf16[4,128,1024]{2,1,0:T(8,128)(2,1)S(1)} %pad_maximum_fusion.2.b0), channel_id=1, source_target_pairs={{0,224},{32,0},{64,32},{96,64},{128,96},{160,128},{192,160},{224,1... | collective-permute-start | bytes 3145736 | tf_op jit(solution)/shard_map/ppermute | solution.py:23
  90.2 3.6 %shard_map.120 = (bf16[1024,128]{1,0:T(8,128)(2,1)S(1)}, bf16[512,128]{1,0:T(8,128)(2,1)S(1)}) custom-call(bf16[1024,256]{1,0:T(8,128)(2,1)S(1)} %bitcast.65, bf16[1024,256]{1,0:T(8,128)(2,1)S(1)} %collective-permute-done.refs_1_, bf16[1024,256]{1,0:T(8,128)(2,1)S(1)} %collective-permute-done.1.refs_2_, ...), custom_call_target="tpu_custom_call" | custom-call | flops 800000000 | bytes 5382144 | tf_op jit(solution)/shard_map/pallas_call | solution.py:54
  94.3 2.3 %collective-permute-start.12 = (bf16[512,128]{1,0:T(8,128)(2,1)S(1)}, bf16[512,128]{1,0:T(8,128)(2,1)S(1)}, u32[]{:S(2)}, u32[]{:S(2)}) collective-permute-start(bf16[512,128]{1,0:T(8,128)(2,1)S(1)} %get-tuple-element.25), channel_id=1, source_target_pairs={{0,6},{2,0},{4,2},{6,4},{1,7},{3,1},{5,3},{7,5},{8,14},{10,8},{12,... | collective-permute-start | bytes 393224 | tf_op jit(solution)/shard_map/ppermute | solution.py:23
  96.6 2.6 %collective-permute-done.11.refs_6_ = bf16[512,128]{1,0:T(8,128)(2,1)S(1)} collective-permute-done((bf16[512,128]{1,0:T(8,128)(2,1)S(1)}, bf16[512,128]{1,0:T(8,128)(2,1)S(1)}, u32[]{:S(2)}, u32[]{:S(2)}) %collective-permute-start.11) | collective-permute-done | bytes 131104 | tf_op jit(solution)/shard_map/ppermute | solution.py:23
  99.4 3.4 %collective-permute-start.18 = (bf16[4,528,256]{2,1,0:T(8,128)(2,1)S(1)}, bf16[4,528,256]{2,1,0:T(8,128)(2,1)S(1)}, u32[]{:S(2)}, u32[]{:S(2)}) collective-permute-start(bf16[4,528,256]{2,1,0:T(8,128)(2,1)S(1)} %pad_maximum_fusion.1), channel_id=1, source_target_pairs={{0,1},{1,0},{2,3},{3,2},{4,5},{5,4},{6,7},{7,6},{8,9},{9,8},{10,11... | collective-permute-start | bytes 3244040 | tf_op jit(solution)/shard_map/ppermute | solution.py:23
  102.8 1.7 collective-permute-done.13.refs_8_
  104.6 3.2 %collective-permute-start.30 = (bf16[4,128,1024]{2,1,0:T(8,128)(2,1)S(1)}, bf16[4,128,1024]{2,1,0:T(8,128)(2,1)S(1)}, u32[]{:S(2)}, u32[]{:S(2)}) collective-permute-start(bf16[4,128,1024]{2,1,0:T(8,128)(2,1)S(1)} %pad_maximum_fusion.3.b0), channel_id=1, source_target_pairs={{0,24},{8,0},{16,8},{24,16},{1,25},{9,1},{17,9},{25,17},{2,26},{10... | collective-permute-start | bytes 3145736 | tf_op jit(solution)/shard_map/ppermute | solution.py:23
  107.8 4.0 %collective-permute-done.22.b1 = bf16[4,128,1024]{2,1,0:T(8,128)(2,1)S(1)} collective-permute-done((bf16[4,128,1024]{2,1,0:T(8,128)(2,1)S(1)}, bf16[4,128,1024]{2,1,0:T(8,128)(2,1)S(1)}, u32[]{:S(2)}, u32[]{:S(2)}) %collective-permute-start.22) | collective-permute-done | bytes 1048608 | tf_op jit(solution)/shard_map/ppermute | solution.py:23
  111.8 2.3 %collective-permute-start.14 = (bf16[3,512,128]{2,1,0:T(8,128)(2,1)S(1)}, bf16[3,512,128]{2,1,0:T(8,128)(2,1)S(1)}, u32[]{:S(2)}, u32[]{:S(2)}) collective-permute-start(bf16[3,512,128]{2,1,0:T(8,128)(2,1)S(1)} %pad_maximum_fusion.6), channel_id=1, source_target_pairs={{0,1},{1,0},{2,3},{3,2},{4,5},{5,4},{6,7},{7,6},{8,9},{9,8},{10,11... | collective-permute-start | bytes 1179656 | tf_op jit(solution)/shard_map/ppermute | solution.py:23
  114.9 2.1 %collective-permute-start.25 = (bf16[2,128,1024]{2,1,0:T(8,128)(2,1)S(1)}, bf16[2,128,1024]{2,1,0:T(8,128)(2,1)S(1)}, u32[]{:S(2)}, u32[]{:S(2)}) collective-permute-start(bf16[2,128,1024]{2,1,0:T(8,128)(2,1)S(1)} %slice.79), channel_id=1, source_target_pairs={{0,224},{32,0},{64,32},{96,64},{128,96},{160,128},{192,160},{224,1... | collective-permute-start | bytes 1572872 | tf_op jit(solution)/shard_map/ppermute | solution.py:23
  117.1 11.0 %collective-permute-done.30.b2 = bf16[4,128,1024]{2,1,0:T(8,128)(2,1)S(1)} collective-permute-done((bf16[4,128,1024]{2,1,0:T(8,128)(2,1)S(1)}, bf16[4,128,1024]{2,1,0:T(8,128)(2,1)S(1)}, u32[]{:S(2)}, u32[]{:S(2)}) %collective-permute-start.30) | collective-permute-done | bytes 1048608 | tf_op jit(solution)/shard_map/ppermute | solution.py:23
  128.1 1.2 collective-permute-start.31
  129.3 1.6 collective-permute-start.32
  130.9 3.4 %shard_map.121 = (bf16[1024,2048]{1,0:T(8,128)(2,1)S(1)}, bf16[1024,256]{1,0:T(8,128)(2,1)S(1)}, f32[1024,128]{1,0:T(8,128)S(1)}) custom-call(bf16[1024,256]{1,0:T(8,128)(2,1)S(1)} %bitcast.66, bf16[1024,256]{1,0:T(8,128)(2,1)S(1)} %collective-permute-done.refs_1_, bf16[1024,256]{1,0:T(8,128)(2,1)S(1)} %collective-permute-done.1.refs_2_, ...), custom_call_target="tpu_custom_call" | custom-call | flops 2200000000 | bytes 7405568 | tf_op jit(solution)/shard_map/pallas_call | solution.py:54
  134.3 6.5 %shard_map.122.hidden = bf16[1024,1024]{1,0:T(8,128)(2,1)S(1)} custom-call(bf16[1024,2048]{1,0:T(8,128)(2,1)S(1)} %get-tuple-element.28.mixed, f32[1024,128]{1,0:T(8,128)S(1)} %get-tuple-element.29.factor, f32[1,1024]{1,0:T(1,128)S(1)} %get-tuple-element.30.s_up, bf16[4,128,1024]{2,1,0:T(8,128)(2,1)S(1)} %pad_maximum_fusion.2.b0, ...), custom_call_target="tpu_custom_call" | custom-call | flops 4300000256 | bytes 8916992 | tf_op jit(solution)/shard_map/pallas_call | solution.py:54
  140.8 3.3 %shard_map.124 = (bf16[2,1024,256]{2,1,0:T(8,128)(2,1)S(1)}, bf16[2,1024,256]{2,1,0:T(8,128)(2,1)S(1)}) custom-call(bf16[1024,1024]{1,0:T(8,128)(2,1)S(1)} %shard_map.122.hidden, bf16[4,128,1024]{2,1,0:T(8,128)(2,1)S(1)} %pad_maximum_fusion.3.b0, bf16[4,128,1024]{2,1,0:T(8,128)(2,1)S(1)} %collective-permute-done.29.b1, ...), custom_call_target="tpu_custom_call" | custom-call | flops 2150000128 | bytes 6291456 | tf_op jit(solution)/shard_map/pallas_call | solution.py:54
  144.1 4.8 %collective-permute-start.34 = (bf16[2,1024,256]{2,1,0:T(8,128)(2,1)S(1)}, bf16[2,1024,256]{2,1,0:T(8,128)(2,1)S(1)}, u32[]{:S(2)}, u32[]{:S(2)}) collective-permute-start(bf16[2,1024,256]{2,1,0:T(8,128)(2,1)S(1)} %get-tuple-element.36), channel_id=1, source_target_pairs={{0,1},{1,0},{2,3},{3,2},{4,5},{5,4},{6,7},{7,6},{8,9},{9,8},{10,11... | collective-permute-start | bytes 3145736 | tf_op jit(solution)/shard_map/ppermute | solution.py:23
  149.0 1.6 shard_map.125
  150.8 1.6 shard_map.123
  153.3 2.7 %collective-permute-start.38 = (bf16[512,256]{1,0:T(8,128)(2,1)S(1)}, bf16[512,256]{1,0:T(8,128)(2,1)S(1)}, u32[]{:S(2)}, u32[]{:S(2)}) collective-permute-start(bf16[512,256]{1,0:T(8,128)(2,1)S(1)} %get-tuple-element.42), channel_id=1, source_target_pairs={{0,6},{2,0},{4,2},{6,4},{1,7},{3,1},{5,3},{7,5},{8,14},{10,8},{12,... | collective-permute-start | bytes 786440 | tf_op jit(solution)/shard_map/ppermute | solution.py:23
  156.2 6.0 %collective-permute-done.36 = bf16[512,256]{1,0:T(8,128)(2,1)S(1)} collective-permute-done((bf16[512,256]{1,0:T(8,128)(2,1)S(1)}, bf16[512,256]{1,0:T(8,128)(2,1)S(1)}, u32[]{:S(2)}, u32[]{:S(2)}) %collective-permute-start.36) | collective-permute-done | bytes 262176 | tf_op jit(solution)/shard_map/ppermute | solution.py:23
  162.7 2.7 %collective-permute-start.39 = (bf16[1024,256]{1,0:T(8,128)(2,1)S(1)}, bf16[1024,256]{1,0:T(8,128)(2,1)S(1)}, u32[]{:S(2)}, u32[]{:S(2)}) collective-permute-start(bf16[1024,256]{1,0:T(8,128)(2,1)S(1)} %pad_maximum_fusion.5), channel_id=1, source_target_pairs={{0,6},{2,0},{4,2},{6,4},{1,7},{3,1},{5,3},{7,5},{8,14},{10,8},{12,... | collective-permute-start | bytes 1572872 | tf_op jit(solution)/shard_map/ppermute | solution.py:23
  165.4 10.9 %collective-permute-done.37 = bf16[1024,256]{1,0:T(8,128)(2,1)S(1)} collective-permute-done((bf16[1024,256]{1,0:T(8,128)(2,1)S(1)}, bf16[1024,256]{1,0:T(8,128)(2,1)S(1)}, u32[]{:S(2)}, u32[]{:S(2)}) %collective-permute-start.37) | collective-permute-done | bytes 524320 | tf_op jit(solution)/shard_map/ppermute | solution.py:23
  176.3 1.2 fusion.3
  (66 shorter events, 8.0 us)
Async XLA Ops:
  0.0 12.9 %collective-permute-start = (bf16[1024,256]{1,0:T(8,128)(2,1)}, bf16[1024,256]{1,0:T(8,128)(2,1)S(1)}, u32[]{:S(2)}, u32[]{:S(2)}) collective-permute-start(bf16[1024,256]{1,0:T(8,128)(2,1)} %bitcast.62), channel_id=1, source_target_pairs={{0,2},{2,4},{4,6},{6,0},{1,3},{3,5},{5,7},{7,1},{8,10},{10,12},{12... | collective-permute-start | bytes 1572872 | tf_op jit(solution)/shard_map/ppermute | solution.py:23
  2.0 12.5 %collective-permute-start.1 = (bf16[1024,256]{1,0:T(8,128)(2,1)}, bf16[1024,256]{1,0:T(8,128)(2,1)S(1)}, u32[]{:S(2)}, u32[]{:S(2)}) collective-permute-start(bf16[1024,256]{1,0:T(8,128)(2,1)} %bitcast.63), channel_id=1, source_target_pairs={{0,6},{2,0},{4,2},{6,4},{1,7},{3,1},{5,3},{7,5},{8,14},{10,8},{12,... | collective-permute-start | bytes 1572872 | tf_op jit(solution)/shard_map/ppermute | solution.py:23
  3.3 24.0 %collective-permute-start.2 = (bf16[1024,256]{1,0:T(8,128)(2,1)}, bf16[1024,256]{1,0:T(8,128)(2,1)S(1)}, u32[]{:S(2)}, u32[]{:S(2)}) collective-permute-start(bf16[1024,256]{1,0:T(8,128)(2,1)} %bitcast.64), channel_id=1, source_target_pairs={{0,4},{2,6},{4,0},{6,2},{1,5},{3,7},{5,1},{7,3},{8,12},{10,14},{12... | collective-permute-start | bytes 1572872 | tf_op jit(solution)/shard_map/ppermute | solution.py:23
  29.9 60.3 %collective-permute-start.3 = (bf16[4,1024,256]{2,1,0:T(8,128)(2,1)}, bf16[4,1024,256]{2,1,0:T(8,128)(2,1)S(1)}, u32[]{:S(2)}, u32[]{:S(2)}) collective-permute-start(bf16[4,1024,256]{2,1,0:T(8,128)(2,1)} %pad_maximum_fusion), channel_id=1, source_target_pairs={{0,1},{1,0},{2,3},{3,2},{4,5},{5,4},{6,7},{7,6},{8,9},{9,8},{10,11... | collective-permute-start | bytes 6291464 | tf_op jit(solution)/shard_map/ppermute | solution.py:23
  33.8 53.5 %copy-start.2 = (bf16[128,1024]{1,0:T(8,128)(2,1)S(1)}, bf16[128,1024]{1,0:T(8,128)(2,1)}, u32[]{:S(2)}) copy-start(bf16[128,1024]{1,0:T(8,128)(2,1)} %get-tuple-element.32) | copy-start | bytes 786436
  33.8 8.0 %collective-permute-start.4 = (bf16[24,1024]{1,0:T(8,128)(2,1)}, bf16[24,1024]{1,0:T(8,128)(2,1)S(1)}, u32[]{:S(2)}, u32[]{:S(2)}) collective-permute-start(bf16[24,1024]{1,0:T(8,128)(2,1)} %get-tuple-element.22), channel_id=1, source_target_pairs={{0,32},{32,64},{64,96},{96,128},{128,160},{160,192},{192,224},{224... | collective-permute-start | bytes 147464 | tf_op jit(solution)/shard_map/ppermute | solution.py:23
  35.5 6.3 %collective-permute-start.5 = (bf16[24,1024]{1,0:T(8,128)(2,1)}, bf16[24,1024]{1,0:T(8,128)(2,1)S(1)}, u32[]{:S(2)}, u32[]{:S(2)}) collective-permute-start(bf16[24,1024]{1,0:T(8,128)(2,1)} %get-tuple-element.22), channel_id=1, source_target_pairs={{0,224},{32,0},{64,32},{96,64},{128,96},{160,128},{192,160},{224,1... | collective-permute-start | bytes 147464 | tf_op jit(solution)/shard_map/ppermute | solution.py:23
  39.5 6.6 %collective-permute-start.6 = (bf16[24,1024]{1,0:T(8,128)(2,1)}, bf16[24,1024]{1,0:T(8,128)(2,1)S(1)}, u32[]{:S(2)}, u32[]{:S(2)}) collective-permute-start(bf16[24,1024]{1,0:T(8,128)(2,1)} %get-tuple-element.22), channel_id=1, source_target_pairs={{0,64},{32,96},{64,128},{96,160},{128,192},{160,224},{192,0},{224,... | collective-permute-start | bytes 147464 | tf_op jit(solution)/shard_map/ppermute | solution.py:23
  46.9 7.1 %collective-permute-start.7 = (bf16[4,24,1024]{2,1,0:T(8,128)(2,1)S(1)}, bf16[4,24,1024]{2,1,0:T(8,128)(2,1)S(1)}, u32[]{:S(2)}, u32[]{:S(2)}) collective-permute-start(bf16[4,24,1024]{2,1,0:T(8,128)(2,1)S(1)} %pad_maximum_fusion.7.m0), channel_id=1, source_target_pairs={{0,8},{8,16},{16,24},{24,0},{1,9},{9,17},{17,25},{25,1},{2,10},{10... | collective-permute-start | bytes 589832 | tf_op jit(solution)/shard_map/ppermute | solution.py:23
  48.3 7.2 %collective-permute-start.8 = (bf16[4,24,1024]{2,1,0:T(8,128)(2,1)S(1)}, bf16[4,24,1024]{2,1,0:T(8,128)(2,1)S(1)}, u32[]{:S(2)}, u32[]{:S(2)}) collective-permute-start(bf16[4,24,1024]{2,1,0:T(8,128)(2,1)S(1)} %pad_maximum_fusion.7.m0), channel_id=1, source_target_pairs={{0,24},{8,0},{16,8},{24,16},{1,25},{9,1},{17,9},{25,17},{2,26},{10... | collective-permute-start | bytes 589832 | tf_op jit(solution)/shard_map/ppermute | solution.py:23
  49.8 9.6 %collective-permute-start.9 = (bf16[4,24,1024]{2,1,0:T(8,128)(2,1)S(1)}, bf16[4,24,1024]{2,1,0:T(8,128)(2,1)S(1)}, u32[]{:S(2)}, u32[]{:S(2)}) collective-permute-start(bf16[4,24,1024]{2,1,0:T(8,128)(2,1)S(1)} %pad_maximum_fusion.7.m0), channel_id=1, source_target_pairs={{0,16},{8,24},{16,0},{24,8},{1,17},{9,25},{17,1},{25,9},{2,18},{10... | collective-permute-start | bytes 589832 | tf_op jit(solution)/shard_map/ppermute | solution.py:23
  51.4 12.8 %collective-permute-start.19 = (bf16[128,1024]{1,0:T(8,128)(2,1)}, bf16[128,1024]{1,0:T(8,128)(2,1)S(1)}, u32[]{:S(2)}, u32[]{:S(2)}) collective-permute-start(bf16[128,1024]{1,0:T(8,128)(2,1)} %get-tuple-element.31), channel_id=1, source_target_pairs={{0,8},{8,16},{16,24},{24,0},{1,9},{9,17},{17,25},{25,1},{2,10},{10... | collective-permute-start | bytes 786440 | tf_op jit(solution)/shard_map/ppermute | solution.py:23
  54.1 10.5 %collective-permute-start.20 = (bf16[128,1024]{1,0:T(8,128)(2,1)}, bf16[128,1024]{1,0:T(8,128)(2,1)S(1)}, u32[]{:S(2)}, u32[]{:S(2)}) collective-permute-start(bf16[128,1024]{1,0:T(8,128)(2,1)} %get-tuple-element.31), channel_id=1, source_target_pairs={{0,24},{8,0},{16,8},{24,16},{1,25},{9,1},{17,9},{25,17},{2,26},{10... | collective-permute-start | bytes 786440 | tf_op jit(solution)/shard_map/ppermute | solution.py:23
  55.5 15.2 %collective-permute-start.21 = (bf16[128,1024]{1,0:T(8,128)(2,1)}, bf16[128,1024]{1,0:T(8,128)(2,1)S(1)}, u32[]{:S(2)}, u32[]{:S(2)}) collective-permute-start(bf16[128,1024]{1,0:T(8,128)(2,1)} %get-tuple-element.31), channel_id=1, source_target_pairs={{0,16},{8,24},{16,0},{24,8},{1,17},{9,25},{17,1},{25,9},{2,18},{10... | collective-permute-start | bytes 786440 | tf_op jit(solution)/shard_map/ppermute | solution.py:23
  59.5 12.1 %collective-permute-start.26 = (bf16[128,1024]{1,0:T(8,128)(2,1)}, bf16[128,1024]{1,0:T(8,128)(2,1)S(1)}, u32[]{:S(2)}, u32[]{:S(2)}) collective-permute-start(bf16[128,1024]{1,0:T(8,128)(2,1)} %get-tuple-element.32), channel_id=1, source_target_pairs={{0,32},{32,64},{64,96},{96,128},{128,160},{160,192},{192,224},{224... | collective-permute-start | bytes 786440 | tf_op jit(solution)/shard_map/ppermute | solution.py:23
  64.2 7.4 %collective-permute-start.27 = (bf16[128,1024]{1,0:T(8,128)(2,1)}, bf16[128,1024]{1,0:T(8,128)(2,1)S(1)}, u32[]{:S(2)}, u32[]{:S(2)}) collective-permute-start(bf16[128,1024]{1,0:T(8,128)(2,1)} %get-tuple-element.32), channel_id=1, source_target_pairs={{0,224},{32,0},{64,32},{96,64},{128,96},{160,128},{192,160},{224,1... | collective-permute-start | bytes 786440 | tf_op jit(solution)/shard_map/ppermute | solution.py:23
  64.6 22.9 %collective-permute-start.10 = (bf16[2064,128]{1,0:T(8,128)(2,1)S(1)}, bf16[2064,128]{1,0:T(8,128)(2,1)S(1)}, u32[]{:S(2)}, u32[]{:S(2)}) collective-permute-start(bf16[2064,128]{1,0:T(8,128)(2,1)S(1)} %get-tuple-element.23.refs_5_), channel_id=1, source_target_pairs={{0,1},{1,0},{2,3},{3,2},{4,5},{5,4},{6,7},{7,6},{8,9},{9,8},{10,11... | collective-permute-start | bytes 1585160 | tf_op jit(solution)/shard_map/ppermute | solution.py:23
  70.7 16.6 %collective-permute-start.15 = (bf16[528,256]{1,0:T(8,128)(2,1)S(1)}, bf16[528,256]{1,0:T(8,128)(2,1)S(1)}, u32[]{:S(2)}, u32[]{:S(2)}) collective-permute-start(bf16[528,256]{1,0:T(8,128)(2,1)S(1)} %get-tuple-element.26.refs_10_), channel_id=1, source_target_pairs={{0,2},{2,4},{4,6},{6,0},{1,3},{3,5},{5,7},{7,1},{8,10},{10,12},{12... | collective-permute-start | bytes 811016 | tf_op jit(solution)/shard_map/ppermute | solution.py:23
  71.6 13.7 %collective-permute-start.28 = (bf16[128,1024]{1,0:T(8,128)(2,1)}, bf16[128,1024]{1,0:T(8,128)(2,1)S(1)}, u32[]{:S(2)}, u32[]{:S(2)}) collective-permute-start(bf16[128,1024]{1,0:T(8,128)(2,1)} %get-tuple-element.32), channel_id=1, source_target_pairs={{0,64},{32,96},{64,128},{96,160},{128,192},{160,224},{192,0},{224,... | collective-permute-start | bytes 786440 | tf_op jit(solution)/shard_map/ppermute | solution.py:23
  71.6 22.3 %collective-permute-start.16 = (bf16[528,256]{1,0:T(8,128)(2,1)S(1)}, bf16[528,256]{1,0:T(8,128)(2,1)S(1)}, u32[]{:S(2)}, u32[]{:S(2)}) collective-permute-start(bf16[528,256]{1,0:T(8,128)(2,1)S(1)} %get-tuple-element.26.refs_10_), channel_id=1, source_target_pairs={{0,6},{2,0},{4,2},{6,4},{1,7},{3,1},{5,3},{7,5},{8,14},{10,8},{12,... | collective-permute-start | bytes 811016 | tf_op jit(solution)/shard_map/ppermute | solution.py:23
  73.5 16.8 %copy-start = (bf16[1,1024,256]{2,1,0:T(8,128)(2,1)S(1)}, bf16[1,1024,256]{2,1,0:T(8,128)(2,1)}, u32[]{:S(2)}) copy-start(bf16[1,1024,256]{2,1,0:T(8,128)(2,1)} %param.12) | copy-start | bytes 1572868
  73.5 16.8 %copy-start.1 = (bf16[4,128,128]{2,1,0:T(8,128)(2,1)S(1)}, bf16[4,128,128]{2,1,0:T(8,128)(2,1)}, u32[]{:S(2)}) copy-start(bf16[4,128,128]{2,1,0:T(8,128)(2,1)} %refs_7_.1) | copy-start | bytes 393220
  85.3 9.0 %collective-permute-start.17 = (bf16[528,256]{1,0:T(8,128)(2,1)S(1)}, bf16[528,256]{1,0:T(8,128)(2,1)S(1)}, u32[]{:S(2)}, u32[]{:S(2)}) collective-permute-start(bf16[528,256]{1,0:T(8,128)(2,1)S(1)} %get-tuple-element.26.refs_10_), channel_id=1, source_target_pairs={{0,4},{2,6},{4,0},{6,2},{1,5},{3,7},{5,1},{7,3},{8,12},{10,14},{12... | collective-permute-start | bytes 811016 | tf_op jit(solution)/shard_map/ppermute | solution.py:23
  87.3 24.5 %collective-permute-start.22 = (bf16[4,128,1024]{2,1,0:T(8,128)(2,1)S(1)}, bf16[4,128,1024]{2,1,0:T(8,128)(2,1)S(1)}, u32[]{:S(2)}, u32[]{:S(2)}) collective-permute-start(bf16[4,128,1024]{2,1,0:T(8,128)(2,1)S(1)} %pad_maximum_fusion.2.b0), channel_id=1, source_target_pairs={{0,32},{32,64},{64,96},{96,128},{128,160},{160,192},{192,224},{224... | collective-permute-start | bytes 3145736 | tf_op jit(solution)/shard_map/ppermute | solution.py:23
  87.5 26.7 %collective-permute-start.23 = (bf16[4,128,1024]{2,1,0:T(8,128)(2,1)S(1)}, bf16[4,128,1024]{2,1,0:T(8,128)(2,1)S(1)}, u32[]{:S(2)}, u32[]{:S(2)}) collective-permute-start(bf16[4,128,1024]{2,1,0:T(8,128)(2,1)S(1)} %pad_maximum_fusion.2.b0), channel_id=1, source_target_pairs={{0,224},{32,0},{64,32},{96,64},{128,96},{160,128},{192,160},{224,1... | collective-permute-start | bytes 3145736 | tf_op jit(solution)/shard_map/ppermute | solution.py:23
  90.2 24.7 %collective-permute-start.29 = (bf16[4,128,1024]{2,1,0:T(8,128)(2,1)S(1)}, bf16[4,128,1024]{2,1,0:T(8,128)(2,1)S(1)}, u32[]{:S(2)}, u32[]{:S(2)}) collective-permute-start(bf16[4,128,1024]{2,1,0:T(8,128)(2,1)S(1)} %pad_maximum_fusion.3.b0), channel_id=1, source_target_pairs={{0,8},{8,16},{16,24},{24,0},{1,9},{9,17},{17,25},{25,1},{2,10},{10... | collective-permute-start | bytes 3145736 | tf_op jit(solution)/shard_map/ppermute | solution.py:23
  93.8 5.4 %collective-permute-start.11 = (bf16[512,128]{1,0:T(8,128)(2,1)S(1)}, bf16[512,128]{1,0:T(8,128)(2,1)S(1)}, u32[]{:S(2)}, u32[]{:S(2)}) collective-permute-start(bf16[512,128]{1,0:T(8,128)(2,1)S(1)} %get-tuple-element.25), channel_id=1, source_target_pairs={{0,2},{2,4},{4,6},{6,0},{1,3},{3,5},{5,7},{7,1},{8,10},{10,12},{12... | collective-permute-start | bytes 393224 | tf_op jit(solution)/shard_map/ppermute | solution.py:23
  94.3 5.1 %collective-permute-start.12 = (bf16[512,128]{1,0:T(8,128)(2,1)S(1)}, bf16[512,128]{1,0:T(8,128)(2,1)S(1)}, u32[]{:S(2)}, u32[]{:S(2)}) collective-permute-start(bf16[512,128]{1,0:T(8,128)(2,1)S(1)} %get-tuple-element.25), channel_id=1, source_target_pairs={{0,6},{2,0},{4,2},{6,4},{1,7},{3,1},{5,3},{7,5},{8,14},{10,8},{12,... | collective-permute-start | bytes 393224 | tf_op jit(solution)/shard_map/ppermute | solution.py:23
  99.2 5.3 %collective-permute-start.13 = (bf16[512,128]{1,0:T(8,128)(2,1)S(1)}, bf16[512,128]{1,0:T(8,128)(2,1)S(1)}, u32[]{:S(2)}, u32[]{:S(2)}) collective-permute-start(bf16[512,128]{1,0:T(8,128)(2,1)S(1)} %get-tuple-element.25), channel_id=1, source_target_pairs={{0,4},{2,6},{4,0},{6,2},{1,5},{3,7},{5,1},{7,3},{8,12},{10,14},{12... | collective-permute-start | bytes 393224 | tf_op jit(solution)/shard_map/ppermute | solution.py:23
  99.4 29.9 %collective-permute-start.18 = (bf16[4,528,256]{2,1,0:T(8,128)(2,1)S(1)}, bf16[4,528,256]{2,1,0:T(8,128)(2,1)S(1)}, u32[]{:S(2)}, u32[]{:S(2)}) collective-permute-start(bf16[4,528,256]{2,1,0:T(8,128)(2,1)S(1)} %pad_maximum_fusion.1), channel_id=1, source_target_pairs={{0,1},{1,0},{2,3},{3,2},{4,5},{5,4},{6,7},{7,6},{8,9},{9,8},{10,11... | collective-permute-start | bytes 3244040 | tf_op jit(solution)/shard_map/ppermute | solution.py:23
  104.6 23.5 %collective-permute-start.30 = (bf16[4,128,1024]{2,1,0:T(8,128)(2,1)S(1)}, bf16[4,128,1024]{2,1,0:T(8,128)(2,1)S(1)}, u32[]{:S(2)}, u32[]{:S(2)}) collective-permute-start(bf16[4,128,1024]{2,1,0:T(8,128)(2,1)S(1)} %pad_maximum_fusion.3.b0), channel_id=1, source_target_pairs={{0,24},{8,0},{16,8},{24,16},{1,25},{9,1},{17,9},{25,17},{2,26},{10... | collective-permute-start | bytes 3145736 | tf_op jit(solution)/shard_map/ppermute | solution.py:23
  111.8 19.1 %collective-permute-start.14 = (bf16[3,512,128]{2,1,0:T(8,128)(2,1)S(1)}, bf16[3,512,128]{2,1,0:T(8,128)(2,1)S(1)}, u32[]{:S(2)}, u32[]{:S(2)}) collective-permute-start(bf16[3,512,128]{2,1,0:T(8,128)(2,1)S(1)} %pad_maximum_fusion.6), channel_id=1, source_target_pairs={{0,1},{1,0},{2,3},{3,2},{4,5},{5,4},{6,7},{7,6},{8,9},{9,8},{10,11... | collective-permute-start | bytes 1179656 | tf_op jit(solution)/shard_map/ppermute | solution.py:23
  114.1 20.1 %collective-permute-start.24 = (bf16[2,128,1024]{2,1,0:T(8,128)(2,1)S(1)}, bf16[2,128,1024]{2,1,0:T(8,128)(2,1)S(1)}, u32[]{:S(2)}, u32[]{:S(2)}) collective-permute-start(bf16[2,128,1024]{2,1,0:T(8,128)(2,1)S(1)} %slice.78), channel_id=1, source_target_pairs={{0,32},{32,64},{64,96},{96,128},{128,160},{160,192},{192,224},{224... | collective-permute-start | bytes 1572872 | tf_op jit(solution)/shard_map/ppermute | solution.py:23
  114.9 19.3 %collective-permute-start.25 = (bf16[2,128,1024]{2,1,0:T(8,128)(2,1)S(1)}, bf16[2,128,1024]{2,1,0:T(8,128)(2,1)S(1)}, u32[]{:S(2)}, u32[]{:S(2)}) collective-permute-start(bf16[2,128,1024]{2,1,0:T(8,128)(2,1)S(1)} %slice.79), channel_id=1, source_target_pairs={{0,224},{32,0},{64,32},{96,64},{128,96},{160,128},{192,160},{224,1... | collective-permute-start | bytes 1572872 | tf_op jit(solution)/shard_map/ppermute | solution.py:23
  128.1 12.7 %collective-permute-start.31 = (bf16[2,128,1024]{2,1,0:T(8,128)(2,1)S(1)}, bf16[2,128,1024]{2,1,0:T(8,128)(2,1)S(1)}, u32[]{:S(2)}, u32[]{:S(2)}) collective-permute-start(bf16[2,128,1024]{2,1,0:T(8,128)(2,1)S(1)} %slice.80), channel_id=1, source_target_pairs={{0,8},{8,16},{16,24},{24,0},{1,9},{9,17},{17,25},{25,1},{2,10},{10... | collective-permute-start | bytes 1572872 | tf_op jit(solution)/shard_map/ppermute | solution.py:23
  129.3 11.5 %collective-permute-start.32 = (bf16[2,128,1024]{2,1,0:T(8,128)(2,1)S(1)}, bf16[2,128,1024]{2,1,0:T(8,128)(2,1)S(1)}, u32[]{:S(2)}, u32[]{:S(2)}) collective-permute-start(bf16[2,128,1024]{2,1,0:T(8,128)(2,1)S(1)} %slice.81), channel_id=1, source_target_pairs={{0,24},{8,0},{16,8},{24,16},{1,25},{9,1},{17,9},{25,17},{2,26},{10... | collective-permute-start | bytes 1572872 | tf_op jit(solution)/shard_map/ppermute | solution.py:23
  144.1 11.8 %collective-permute-start.34 = (bf16[2,1024,256]{2,1,0:T(8,128)(2,1)S(1)}, bf16[2,1024,256]{2,1,0:T(8,128)(2,1)S(1)}, u32[]{:S(2)}, u32[]{:S(2)}) collective-permute-start(bf16[2,1024,256]{2,1,0:T(8,128)(2,1)S(1)} %get-tuple-element.36), channel_id=1, source_target_pairs={{0,1},{1,0},{2,3},{3,2},{4,5},{5,4},{6,7},{7,6},{8,9},{9,8},{10,11... | collective-permute-start | bytes 3145736 | tf_op jit(solution)/shard_map/ppermute | solution.py:23
  150.6 2.3 %collective-permute-start.35 = (bf16[1,1024,256]{2,1,0:T(8,128)(2,1)S(1)}, bf16[1,1024,256]{2,1,0:T(8,128)(2,1)S(1)}, u32[]{:S(2)}, u32[]{:S(2)}) collective-permute-start(bf16[1,1024,256]{2,1,0:T(8,128)(2,1)S(1)} %get-tuple-element.38), channel_id=1, source_target_pairs={{0,1},{1,0},{2,3},{3,2},{4,5},{5,4},{6,7},{7,6},{8,9},{9,8},{10,11... | collective-permute-start | bytes 1572872 | tf_op jit(solution)/shard_map/ppermute | solution.py:23
  152.4 13.0 %collective-permute-start.33 = (bf16[1,1024,256]{2,1,0:T(8,128)(2,1)S(1)}, bf16[1,1024,256]{2,1,0:T(8,128)(2,1)S(1)}, u32[]{:S(2)}, u32[]{:S(2)}) collective-permute-start(bf16[1,1024,256]{2,1,0:T(8,128)(2,1)S(1)} %get-tuple-element.34), channel_id=1, source_target_pairs={{0,1},{1,0},{2,3},{3,2},{4,5},{5,4},{6,7},{7,6},{8,9},{9,8},{10,11... | collective-permute-start | bytes 1572872 | tf_op jit(solution)/shard_map/ppermute | solution.py:23
  153.2 9.1 %collective-permute-start.36 = (bf16[512,256]{1,0:T(8,128)(2,1)S(1)}, bf16[512,256]{1,0:T(8,128)(2,1)S(1)}, u32[]{:S(2)}, u32[]{:S(2)}) collective-permute-start(bf16[512,256]{1,0:T(8,128)(2,1)S(1)} %get-tuple-element.41), channel_id=1, source_target_pairs={{0,2},{2,4},{4,6},{6,0},{1,3},{3,5},{5,7},{7,1},{8,10},{10,12},{12... | collective-permute-start | bytes 786440 | tf_op jit(solution)/shard_map/ppermute | solution.py:23
  153.3 9.3 %collective-permute-start.38 = (bf16[512,256]{1,0:T(8,128)(2,1)S(1)}, bf16[512,256]{1,0:T(8,128)(2,1)S(1)}, u32[]{:S(2)}, u32[]{:S(2)}) collective-permute-start(bf16[512,256]{1,0:T(8,128)(2,1)S(1)} %get-tuple-element.42), channel_id=1, source_target_pairs={{0,6},{2,0},{4,2},{6,4},{1,7},{3,1},{5,3},{7,5},{8,14},{10,8},{12,... | collective-permute-start | bytes 786440 | tf_op jit(solution)/shard_map/ppermute | solution.py:23
  162.4 13.9 %collective-permute-start.37 = (bf16[1024,256]{1,0:T(8,128)(2,1)S(1)}, bf16[1024,256]{1,0:T(8,128)(2,1)S(1)}, u32[]{:S(2)}, u32[]{:S(2)}) collective-permute-start(bf16[1024,256]{1,0:T(8,128)(2,1)S(1)} %pad_maximum_fusion.4), channel_id=1, source_target_pairs={{0,2},{2,4},{4,6},{6,0},{1,3},{3,5},{5,7},{7,1},{8,10},{10,12},{12... | collective-permute-start | bytes 1572872 | tf_op jit(solution)/shard_map/ppermute | solution.py:23
  162.7 13.6 %collective-permute-start.39 = (bf16[1024,256]{1,0:T(8,128)(2,1)S(1)}, bf16[1024,256]{1,0:T(8,128)(2,1)S(1)}, u32[]{:S(2)}, u32[]{:S(2)}) collective-permute-start(bf16[1024,256]{1,0:T(8,128)(2,1)S(1)} %pad_maximum_fusion.5), channel_id=1, source_target_pairs={{0,6},{2,0},{4,2},{6,4},{1,7},{3,1},{5,3},{7,5},{8,14},{10,8},{12,... | collective-permute-start | bytes 1572872 | tf_op jit(solution)/shard_map/ppermute | solution.py:23

commit v2 on v1

--- a/solution.py
+++ b/solution.py
@@ -209,12 +209,16 @@
     chips, whose = around(lax.axis_index("x")), owners()
     c = lax.axis_index("c")
 
-    @pl.loop(0, 2)
+    @pl.loop(0, 4)
     def _(block):
-        rows = pl.ds(pl.multiple_of(block * 512, 512), 512)
-        squares = jnp.zeros((512, 128), F32)
+        rows = pl.ds(pl.multiple_of(block * 256, 256), 256)
+        inner = pl.ds(pl.multiple_of(lax.rem(block, 2) * 256, 256), 256)
+        squares = jnp.zeros((256, 128), F32)
         left = jnp.concatenate(
-            [grouped[rows, :]] + [jnp.where(block == c, a[...], across[k]) for k, a in enumerate(near)],
+            [grouped[rows, :]] + [
+                jnp.where(lax.div(block, 2) == c, a[inner, :], across[k, inner, :])
+                for k, a in enumerate(near)
+            ],
             axis=1,
         )
         for k in range(8):
@@ -231,24 +235,44 @@
             wide = wide * wide
             squares += wide[:, :128] + wide[:, 128:]
         mean = jnp.sum(squares, axis=1, keepdims=True) / 2048
-        factor[rows, :] = jnp.broadcast_to(lax.rsqrt(mean + EPS), (512, 128))
-
-
-def up_kernel(mixed, factor, s_up, b0, b1, b2, b3, b4, hidden):
-    ys, zs = around(lax.axis_index("y")), around(lax.axis_index("z"))
-    parts = [b.at[pl.ds(2 * k, 2)] for b in (b0, b1, b2) for k in range(2)] + [b3, b4]
-
-    @pl.loop(0, 8)
+        factor[rows, :] = jnp.broadcast_to(lax.rsqrt(mean + EPS), (256, 128))
+
+
+def up_parts_sum(mixed, parts, zs, rows, cols, total):
+    ys = around(lax.axis_index("y"))
+    for k, part in enumerate(parts):
+        left = [
+            mixed[rows, pl.ds(pl.multiple_of((4 * zs[k // 2] + ys[2 * (k % 2) + i]) * 128, 128), 128)]
+            for i in range(2)
+        ]
+        total += dot(jnp.concatenate(left, axis=1), part[:, :, cols].reshape(256, 256))
+    return total
+
+
+def tile_of(step):
+    rows = pl.ds(pl.multiple_of(lax.rem(step, 2) * 512, 512), 512)
+    return rows, pl.ds(pl.multiple_of(lax.div(step, 2) * 256, 256), 256)
+
+
+def up_near_kernel(mixed, *refs):
+    parts, out = refs[:-1], refs[-1]
+    zs = around(lax.axis_index("z"))
+    if len(parts) == 3:
+        parts = [b.at[pl.ds(2 * k, 2)] for b in parts for k in range(2)]
+
+    @pl.loop(0, 4 * 2)
     def _(step):
-        rows = pl.ds(pl.multiple_of(lax.rem(step, 2) * 512, 512), 512)
-        cols = pl.ds(pl.multiple_of(lax.div(step, 2) * 256, 256), 256)
-        total = jnp.zeros((512, 256), F32)
-        for k in range(8):
-            left = [
-                mixed[rows, pl.ds(pl.multiple_of((4 * zs[k // 2] + ys[2 * (k % 2) + i]) * 128, 128), 128)]
-                for i in range(2)
-            ]
-            total += dot(jnp.concatenate(left, axis=1), parts[k][:, :, cols].reshape(256, 256))
+        rows, cols = tile_of(step)
+        out[rows, cols] = up_parts_sum(mixed, parts, zs, rows, cols, jnp.zeros((512, 256), F32))
+
+
+def up_far_kernel(mixed, factor, s_up, near, b3, b4, hidden):
+    zs = around(lax.axis_index("z"))[3:]
+
+    @pl.loop(0, 4 * 2)
+    def _(step):
+        rows, cols = tile_of(step)
+        total = up_parts_sum(mixed, (b3, b4), zs, rows, cols, near[rows, cols])
         scale = jnp.concatenate([factor[rows, :]] * 2, axis=1) * s_up[:, cols]
         value = jnp.maximum(total * scale, 0.0)
         hidden[rows, cols] = (value * value).astype(BF)
@@ -261,10 +285,10 @@
     low_is_own = y_is_own == (jnp.bitwise_and(y, 1) == 1)
     side = jnp.bitwise_and(y, 1)
 
-    @pl.loop(0, 2 * len(steps))
+    @pl.loop(0, 4 * len(steps))
     def _(step):
-        rows = pl.ds(pl.multiple_of(lax.rem(step, 2) * 512, 512), 512)
-        k = lax.div(step, 2)
+        rows = pl.ds(pl.multiple_of(lax.rem(step, 4) * 256, 256), 256)
+        k = lax.div(step, 4)
         chip = lax.rem(x + ((2 * k + 1) if len(steps) > 1 else steps[0]), 4)
         away = lax.rem(chip - z + 4, 4)
         place = jnp.where(away == 0, 0, jnp.where(away == 1, 2, jnp.where(away == 2, 3, 1)))
@@ -377,9 +401,10 @@
         *outs,
     )
 
-    hidden = call(
-        up_kernel, bf(SEQ, 1024), [], 32, 4_300_000_000, mixed, factor, s_up_row, *up_parts
-    )
+    sums = call(
+        up_near_kernel, f32(SEQ, 1024), [], 24, 3_200_000_000, mixed, *up_parts[:-2]
+    )
+    hidden = call(up_far_kernel, bf(SEQ, 1024), [], 24, 1_100_000_000, mixed, factor, s_up_row, sums, *up_parts[-2:])
 
     def block_sums(steps):
         count = len(steps)

time: 179 us -> 183 us (1.022)
  starting transfers between devices: 60.6 us -> 68 us
  waiting for transfers between devices: 86.7 us -> 80.7 us
  Pallas kernels: 22.8 us -> 26.5 us
    ppermute x40, starting transfers between devices: 60.6 us -> 68 us  [send(): lax.ppermute(array, axes, [(i, (i + shift) % count) for i in range(count)])]
    ppermute x40, waiting for transfers between devices: 86.7 us -> 80.7 us  [send(): lax.ppermute(array, axes, [(i, (i + shift) % count) for i in range(count)])]
    pallas_call x8 -> x9, Pallas kernels: 22.8 us -> 26.5 us  [call(): pl.pallas_call(kernel, out_shape=out_shape, in_specs=[VMEM] * (len(args)...]
  transfers between devices with their start and end apart: 40 -> 40, of which waited for: 17 -> 18; matrix products, arithmetic and copies ran while one was open for 2% -> 2% of each run, Pallas kernels for 11% -> 12%
where the time goes in v2:
time: 183 us
  waiting for transfers between devices  80.7 us (44%)
  starting transfers between devices  68 us (37%)
  Pallas kernels  26.5 us (14%)
  other arithmetic  6.81 us (4%)
    ppermute x40, waiting for transfers between devices, send(): lax.ppermute(array, axes, [(i, (i + shift) % count) for i in range(count)])  80.7 us
    ppermute x40, starting transfers between devices, send(): lax.ppermute(array, axes, [(i, (i + shift) % count) for i in range(count)])  68 us
    pallas_call x9, Pallas kernels, call(): pl.pallas_call(kernel, out_shape=out_shape, in_specs=[VMEM] * (len(args)...  26.5 us
  transfers between devices with their start and end apart: 40, of which 18 were waited for; matrix products, arithmetic and copies ran while one was open for 2% of the time, Pallas kernels for 12%

profile of v2, /device:TPU:1, one launch (start us, length us, event | category | flops | bytes accessed | tf_op | source)
XLA Modules:
  0.0 182.5 jit_solution(13227032265190045968)
XLA Ops:
  0.0 2.0 %collective-permute-start = (bf16[1024,256]{1,0:T(8,128)(2,1)}, bf16[1024,256]{1,0:T(8,128)(2,1)S(1)}, u32[]{:S(2)}, u32[]{:S(2)}) collective-permute-start(bf16[1024,256]{1,0:T(8,128)(2,1)} %bitcast.62), channel_id=1, source_target_pairs={{0,2},{2,4},{4,6},{6,0},{1,3},{3,5},{5,7},{7,1},{8,10},{10,12},{12... | collective-permute-start | bytes 1572872 | tf_op jit(solution)/shard_map/ppermute | solution.py:23
  3.3 1.7 collective-permute-start.2
  5.0 7.9 %collective-permute-done.refs_1_ = bf16[1024,256]{1,0:T(8,128)(2,1)S(1)} collective-permute-done((bf16[1024,256]{1,0:T(8,128)(2,1)}, bf16[1024,256]{1,0:T(8,128)(2,1)S(1)}, u32[]{:S(2)}, u32[]{:S(2)}) %collective-permute-start) | collective-permute-done | bytes 524320 | tf_op jit(solution)/shard_map/ppermute | solution.py:23
  12.9 1.6 collective-permute-done.1.refs_2_
  14.6 12.7 %collective-permute-done.2.refs_3_ = bf16[1024,256]{1,0:T(8,128)(2,1)S(1)} collective-permute-done((bf16[1024,256]{1,0:T(8,128)(2,1)}, bf16[1024,256]{1,0:T(8,128)(2,1)S(1)}, u32[]{:S(2)}, u32[]{:S(2)}) %collective-permute-start.2) | collective-permute-done | bytes 524320 | tf_op jit(solution)/shard_map/ppermute | solution.py:23
  27.3 2.8 %pad_maximum_fusion = bf16[4,1024,256]{2,1,0:T(8,128)(2,1)} fusion(bf16[1,1024,256]{2,1,0:T(8,128)(2,1)S(1)} %bitcast.69, bf16[1,1024,256]{2,1,0:T(8,128)(2,1)S(1)} %bitcast.68, bf16[1,1024,256]{2,1,0:T(8,128)(2,1)S(1)} %bitcast.67, bf16[1,1024,256]{2,1,0:T(8,128)(2,1)} %param.12), kind=kLoop, calls=%fused_computation | loop fusion | flops 3145728 | bytes 4194304 | tf_op jit(solution)/shard_map/stack | solution.py:340
  30.1 1.5 collective-permute-start.3
  31.6 2.4 %shard_map.118 = (bf16[24,1024]{1,0:T(8,128)(2,1)}, bf16[128,1024]{1,0:T(8,128)(2,1)}, bf16[128,1024]{1,0:T(8,128)(2,1)}) custom-call(f32[16,128]{1,0:T(8,128)} %bitcast.90, f32[64,128]{1,0:T(8,128)} %bitcast.89, f32[1,4]{1,0:T(1,128)} %bitcast.92, f32[32,256]{1,0:T(8,128)} %w_out_at.1, f32[1,16]{1,0:T(1,128)} %bitcast.93, f32[16,128]{1,0:T(8,128)} %bitcast.91, ...), custom_call_target="tpu_custom_call" | custom-call | flops 1000000 | bytes 1131344 | tf_op jit(solution)/shard_map/pallas_call | solution.py:54
  34.0 3.1 %collective-permute-start.6 = (bf16[24,1024]{1,0:T(8,128)(2,1)}, bf16[24,1024]{1,0:T(8,128)(2,1)S(1)}, u32[]{:S(2)}, u32[]{:S(2)}) collective-permute-start(bf16[24,1024]{1,0:T(8,128)(2,1)} %get-tuple-element.22), channel_id=1, source_target_pairs={{0,64},{32,96},{64,128},{96,160},{128,192},{160,224},{192,0},{224,... | collective-permute-start | bytes 147464 | tf_op jit(solution)/shard_map/ppermute | solution.py:23
  37.1 2.7 %collective-permute-start.5 = (bf16[24,1024]{1,0:T(8,128)(2,1)}, bf16[24,1024]{1,0:T(8,128)(2,1)S(1)}, u32[]{:S(2)}, u32[]{:S(2)}) collective-permute-start(bf16[24,1024]{1,0:T(8,128)(2,1)} %get-tuple-element.22), channel_id=1, source_target_pairs={{0,224},{32,0},{64,32},{96,64},{128,96},{160,128},{192,160},{224,1... | collective-permute-start | bytes 147464 | tf_op jit(solution)/shard_map/ppermute | solution.py:23
  39.8 2.7 %collective-permute-done.6 = bf16[24,1024]{1,0:T(8,128)(2,1)S(1)} collective-permute-done((bf16[24,1024]{1,0:T(8,128)(2,1)}, bf16[24,1024]{1,0:T(8,128)(2,1)S(1)}, u32[]{:S(2)}, u32[]{:S(2)}) %collective-permute-start.6) | collective-permute-done | bytes 49184 | tf_op jit(solution)/shard_map/ppermute | solution.py:23
  42.4 1.7 collective-permute-done.4
  46.3 1.5 collective-permute-start.8
  47.9 1.6 collective-permute-start.9
  49.4 1.4 collective-permute-start.21
  52.8 3.9 %collective-permute-done.9.m3 = bf16[4,24,1024]{2,1,0:T(8,128)(2,1)S(1)} collective-permute-done((bf16[4,24,1024]{2,1,0:T(8,128)(2,1)S(1)}, bf16[4,24,1024]{2,1,0:T(8,128)(2,1)S(1)}, u32[]{:S(2)}, u32[]{:S(2)}) %collective-permute-start.9) | collective-permute-done | bytes 196640 | tf_op jit(solution)/shard_map/ppermute | solution.py:23
  57.1 5.5 %collective-permute-start.10 = (bf16[2064,128]{1,0:T(8,128)(2,1)S(1)}, bf16[2064,128]{1,0:T(8,128)(2,1)S(1)}, u32[]{:S(2)}, u32[]{:S(2)}) collective-permute-start(bf16[2064,128]{1,0:T(8,128)(2,1)S(1)} %get-tuple-element.23.refs_5_), channel_id=1, source_target_pairs={{0,1},{1,0},{2,3},{3,2},{4,5},{5,4},{6,7},{7,6},{8,9},{9,8},{10,11... | collective-permute-start | bytes 1585160 | tf_op jit(solution)/shard_map/ppermute | solution.py:23
  62.6 1.9 %collective-permute-start.19 = (bf16[128,1024]{1,0:T(8,128)(2,1)}, bf16[128,1024]{1,0:T(8,128)(2,1)S(1)}, u32[]{:S(2)}, u32[]{:S(2)}) collective-permute-start(bf16[128,1024]{1,0:T(8,128)(2,1)} %get-tuple-element.31), channel_id=1, source_target_pairs={{0,8},{8,16},{16,24},{24,0},{1,9},{9,17},{17,25},{25,1},{2,10},{10... | collective-permute-start | bytes 786440 | tf_op jit(solution)/shard_map/ppermute | solution.py:23
  65.3 2.0 %collective-permute-done.20 = bf16[128,1024]{1,0:T(8,128)(2,1)S(1)} collective-permute-done((bf16[128,1024]{1,0:T(8,128)(2,1)}, bf16[128,1024]{1,0:T(8,128)(2,1)S(1)}, u32[]{:S(2)}, u32[]{:S(2)}) %collective-permute-start.20) | collective-permute-done | bytes 262176 | tf_op jit(solution)/shard_map/ppermute | solution.py:23
  67.3 1.7 collective-permute-start.16
  69.0 4.2 %collective-permute-done.19 = bf16[128,1024]{1,0:T(8,128)(2,1)S(1)} collective-permute-done((bf16[128,1024]{1,0:T(8,128)(2,1)}, bf16[128,1024]{1,0:T(8,128)(2,1)S(1)}, u32[]{:S(2)}, u32[]{:S(2)}) %collective-permute-start.19) | collective-permute-done | bytes 262176 | tf_op jit(solution)/shard_map/ppermute | solution.py:23
  74.2 1.9 %collective-permute-start.27 = (bf16[128,1024]{1,0:T(8,128)(2,1)}, bf16[128,1024]{1,0:T(8,128)(2,1)S(1)}, u32[]{:S(2)}, u32[]{:S(2)}) collective-permute-start(bf16[128,1024]{1,0:T(8,128)(2,1)} %get-tuple-element.32), channel_id=1, source_target_pairs={{0,224},{32,0},{64,32},{96,64},{128,96},{160,128},{192,160},{224,1... | collective-permute-start | bytes 786440 | tf_op jit(solution)/shard_map/ppermute | solution.py:23
  77.3 3.9 %collective-permute-start.22 = (bf16[4,128,1024]{2,1,0:T(8,128)(2,1)S(1)}, bf16[4,128,1024]{2,1,0:T(8,128)(2,1)S(1)}, u32[]{:S(2)}, u32[]{:S(2)}) collective-permute-start(bf16[4,128,1024]{2,1,0:T(8,128)(2,1)S(1)} %pad_maximum_fusion.2.refs_0_), channel_id=1, source_target_pairs={{0,32},{32,64},{64,96},{96,128},{128,160},{160,192},{192,224},{224... | collective-permute-start | bytes 3145736 | tf_op jit(solution)/shard_map/ppermute | solution.py:23
  81.1 3.6 %shard_map.120 = (bf16[1024,128]{1,0:T(8,128)(2,1)S(1)}, bf16[512,128]{1,0:T(8,128)(2,1)S(1)}) custom-call(bf16[1024,256]{1,0:T(8,128)(2,1)S(1)} %bitcast.65, bf16[1024,256]{1,0:T(8,128)(2,1)S(1)} %collective-permute-done.refs_1_, bf16[1024,256]{1,0:T(8,128)(2,1)S(1)} %collective-permute-done.1.refs_2_, bf16[1024,256]{1,0:T(8,128)(2,1)S(1)} %copy-done.2, ...), custom_call_target="tpu_custom_call" | custom-call | flops 800000000 | bytes 5382144 | tf_op jit(solution)/shard_map/pallas_call | solution.py:54
  86.1 3.3 %collective-permute-done.28 = bf16[128,1024]{1,0:T(8,128)(2,1)S(1)} collective-permute-done((bf16[128,1024]{1,0:T(8,128)(2,1)}, bf16[128,1024]{1,0:T(8,128)(2,1)S(1)}, u32[]{:S(2)}, u32[]{:S(2)}) %collective-permute-start.28) | collective-permute-done | bytes 262176 | tf_op jit(solution)/shard_map/ppermute | solution.py:23
  89.3 1.5 collective-permute-start.18
  90.9 2.0 %collective-permute-done.26 = bf16[128,1024]{1,0:T(8,128)(2,1)S(1)} collective-permute-done((bf16[128,1024]{1,0:T(8,128)(2,1)}, bf16[128,1024]{1,0:T(8,128)(2,1)S(1)}, u32[]{:S(2)}, u32[]{:S(2)}) %collective-permute-start.26) | collective-permute-done | bytes 262176 | tf_op jit(solution)/shard_map/ppermute | solution.py:23
  92.9 2.7 %collective-permute-start.12 = (bf16[512,128]{1,0:T(8,128)(2,1)S(1)}, bf16[512,128]{1,0:T(8,128)(2,1)S(1)}, u32[]{:S(2)}, u32[]{:S(2)}) collective-permute-start(bf16[512,128]{1,0:T(8,128)(2,1)S(1)} %get-tuple-element.25), channel_id=1, source_target_pairs={{0,6},{2,0},{4,2},{6,4},{1,7},{3,1},{5,3},{7,5},{8,14},{10,8},{12,... | collective-permute-start | bytes 393224 | tf_op jit(solution)/shard_map/ppermute | solution.py:23
  96.6 2.4 %collective-permute-done.12.refs_7_ = bf16[512,128]{1,0:T(8,128)(2,1)S(1)} collective-permute-done((bf16[512,128]{1,0:T(8,128)(2,1)S(1)}, bf16[512,128]{1,0:T(8,128)(2,1)S(1)}, u32[]{:S(2)}, u32[]{:S(2)}) %collective-permute-start.12) | collective-permute-done | bytes 131104 | tf_op jit(solution)/shard_map/ppermute | solution.py:23
  98.9 2.0 %collective-permute-done.13.refs_8_ = bf16[512,128]{1,0:T(8,128)(2,1)S(1)} collective-permute-done((bf16[512,128]{1,0:T(8,128)(2,1)S(1)}, bf16[512,128]{1,0:T(8,128)(2,1)S(1)}, u32[]{:S(2)}, u32[]{:S(2)}) %collective-permute-start.13) | collective-permute-done | bytes 131104 | tf_op jit(solution)/shard_map/ppermute | solution.py:23
  100.9 3.0 %collective-permute-start.30 = (bf16[4,128,1024]{2,1,0:T(8,128)(2,1)S(1)}, bf16[4,128,1024]{2,1,0:T(8,128)(2,1)S(1)}, u32[]{:S(2)}, u32[]{:S(2)}) collective-permute-start(bf16[4,128,1024]{2,1,0:T(8,128)(2,1)S(1)} %pad_maximum_fusion.3.b0), channel_id=1, source_target_pairs={{0,24},{8,0},{16,8},{24,16},{1,25},{9,1},{17,9},{25,17},{2,26},{10... | collective-permute-start | bytes 3145736 | tf_op jit(solution)/shard_map/ppermute | solution.py:23
  104.0 11.4 %collective-permute-done.22.refs_1_ = bf16[4,128,1024]{2,1,0:T(8,128)(2,1)S(1)} collective-permute-done((bf16[4,128,1024]{2,1,0:T(8,128)(2,1)S(1)}, bf16[4,128,1024]{2,1,0:T(8,128)(2,1)S(1)}, u32[]{:S(2)}, u32[]{:S(2)}) %collective-permute-start.22) | collective-permute-done | bytes 1048608 | tf_op jit(solution)/shard_map/ppermute | solution.py:23
  115.4 1.8 collective-permute-start.14
  117.4 3.4 %collective-permute-done.29.b1 = bf16[4,128,1024]{2,1,0:T(8,128)(2,1)S(1)} collective-permute-done((bf16[4,128,1024]{2,1,0:T(8,128)(2,1)S(1)}, bf16[4,128,1024]{2,1,0:T(8,128)(2,1)S(1)}, u32[]{:S(2)}, u32[]{:S(2)}) %collective-permute-start.29) | collective-permute-done | bytes 1048608 | tf_op jit(solution)/shard_map/ppermute | solution.py:23
  120.8 2.6 %collective-permute-start.25 = (bf16[2,128,1024]{2,1,0:T(8,128)(2,1)S(1)}, bf16[2,128,1024]{2,1,0:T(8,128)(2,1)S(1)}, u32[]{:S(2)}, u32[]{:S(2)}) collective-permute-start(bf16[2,128,1024]{2,1,0:T(8,128)(2,1)S(1)} %slice.79), channel_id=1, source_target_pairs={{0,224},{32,0},{64,32},{96,64},{128,96},{160,128},{192,160},{224,1... | collective-permute-start | bytes 1572872 | tf_op jit(solution)/shard_map/ppermute | solution.py:23
  123.6 3.4 %collective-permute-start.32 = (bf16[2,128,1024]{2,1,0:T(8,128)(2,1)S(1)}, bf16[2,128,1024]{2,1,0:T(8,128)(2,1)S(1)}, u32[]{:S(2)}, u32[]{:S(2)}) collective-permute-start(bf16[2,128,1024]{2,1,0:T(8,128)(2,1)S(1)} %slice.81), channel_id=1, source_target_pairs={{0,24},{8,0},{16,8},{24,16},{1,25},{9,1},{17,9},{25,17},{2,26},{10... | collective-permute-start | bytes 1572872 | tf_op jit(solution)/shard_map/ppermute | solution.py:23
  126.9 4.0 %shard_map.121 = (bf16[1024,2048]{1,0:T(8,128)(2,1)S(1)}, bf16[1024,256]{1,0:T(8,128)(2,1)S(1)}, f32[1024,128]{1,0:T(8,128)S(1)}) custom-call(bf16[1024,256]{1,0:T(8,128)(2,1)S(1)} %bitcast.66, bf16[1024,256]{1,0:T(8,128)(2,1)S(1)} %collective-permute-done.refs_1_, bf16[1024,256]{1,0:T(8,128)(2,1)S(1)} %collective-permute-done.1.refs_2_, ...), custom_call_target="tpu_custom_call" | custom-call | flops 2200000000 | bytes 7405568 | tf_op jit(solution)/shard_map/pallas_call | solution.py:54
  130.9 5.1 %shard_map.122.near = f32[1024,1024]{1,0:T(8,128)S(1)} custom-call(bf16[1024,2048]{1,0:T(8,128)(2,1)S(1)} %get-tuple-element.28.mixed, bf16[4,128,1024]{2,1,0:T(8,128)(2,1)S(1)} %pad_maximum_fusion.2.refs_0_, bf16[4,128,1024]{2,1,0:T(8,128)(2,1)S(1)} %collective-permute-done.22.refs_1_, bf16[4,128,1024]{2,1,0:T(8,128)(2,1)S(1)} %collective-permute-done.23.refs_2_), custom_call_target="tpu_custom_call" | custom-call | flops 3200000000 | bytes 7340032 | tf_op jit(solution)/shard_map/pallas_call | solution.py:54
  136.0 2.6 %shard_map.123.hidden = bf16[1024,1024]{1,0:T(8,128)(2,1)S(1)} custom-call(bf16[1024,2048]{1,0:T(8,128)(2,1)S(1)} %get-tuple-element.28.mixed, f32[1024,128]{1,0:T(8,128)S(1)} %get-tuple-element.29.factor, f32[1,1024]{1,0:T(1,128)S(1)} %get-tuple-element.30.s_up, f32[1024,1024]{1,0:T(8,128)S(1)} %shard_map.122.near, ...), custom_call_target="tpu_custom_call" | custom-call | flops 1100000000 | bytes 9965568 | tf_op jit(solution)/shard_map/pallas_call | solution.py:54
  138.7 4.3 %shard_map.125 = (bf16[2,1024,256]{2,1,0:T(8,128)(2,1)S(1)}, bf16[2,1024,256]{2,1,0:T(8,128)(2,1)S(1)}) custom-call(bf16[1024,1024]{1,0:T(8,128)(2,1)S(1)} %shard_map.123.hidden, bf16[4,128,1024]{2,1,0:T(8,128)(2,1)S(1)} %pad_maximum_fusion.3.b0, bf16[4,128,1024]{2,1,0:T(8,128)(2,1)S(1)} %collective-permute-done.29.b1, ...), custom_call_target="tpu_custom_call" | custom-call | flops 2150000128 | bytes 6291456 | tf_op jit(solution)/shard_map/pallas_call | solution.py:54
  142.9 4.7 %collective-permute-start.34 = (bf16[2,1024,256]{2,1,0:T(8,128)(2,1)S(1)}, bf16[2,1024,256]{2,1,0:T(8,128)(2,1)S(1)}, u32[]{:S(2)}, u32[]{:S(2)}) collective-permute-start(bf16[2,1024,256]{2,1,0:T(8,128)(2,1)S(1)} %get-tuple-element.36), channel_id=1, source_target_pairs={{0,1},{1,0},{2,3},{3,2},{4,5},{5,4},{6,7},{7,6},{8,9},{9,8},{10,11... | collective-permute-start | bytes 3145736 | tf_op jit(solution)/shard_map/ppermute | solution.py:23
  147.6 2.1 %shard_map.126 = (bf16[1,1024,256]{2,1,0:T(8,128)(2,1)S(1)}, bf16[1,1024,256]{2,1,0:T(8,128)(2,1)S(1)}) custom-call(bf16[1024,1024]{1,0:T(8,128)(2,1)S(1)} %shard_map.123.hidden, bf16[4,128,1024]{2,1,0:T(8,128)(2,1)S(1)} %pad_maximum_fusion.3.b0, bf16[4,128,1024]{2,1,0:T(8,128)(2,1)S(1)} %collective-permute-done.29.b1, ...), custom_call_target="tpu_custom_call" | custom-call | flops 1075000064 | bytes 6291456 | tf_op jit(solution)/shard_map/pallas_call | solution.py:54
  149.9 2.1 %shard_map.124 = (bf16[1,1024,256]{2,1,0:T(8,128)(2,1)S(1)}, bf16[1,1024,256]{2,1,0:T(8,128)(2,1)S(1)}) custom-call(bf16[1024,1024]{1,0:T(8,128)(2,1)S(1)} %shard_map.123.hidden, bf16[4,128,1024]{2,1,0:T(8,128)(2,1)S(1)} %pad_maximum_fusion.3.b0, bf16[4,128,1024]{2,1,0:T(8,128)(2,1)S(1)} %collective-permute-done.29.b1, ...), custom_call_target="tpu_custom_call" | custom-call | flops 1075000064 | bytes 6291456 | tf_op jit(solution)/shard_map/pallas_call | solution.py:54
  152.7 5.7 %collective-permute-start.38 = (bf16[512,256]{1,0:T(8,128)(2,1)S(1)}, bf16[512,256]{1,0:T(8,128)(2,1)S(1)}, u32[]{:S(2)}, u32[]{:S(2)}) collective-permute-start(bf16[512,256]{1,0:T(8,128)(2,1)S(1)} %get-tuple-element.42), channel_id=1, source_target_pairs={{0,6},{2,0},{4,2},{6,4},{1,7},{3,1},{5,3},{7,5},{8,14},{10,8},{12,... | collective-permute-start | bytes 786440 | tf_op jit(solution)/shard_map/ppermute | solution.py:23
  158.7 5.3 %collective-permute-done.38 = bf16[512,256]{1,0:T(8,128)(2,1)S(1)} collective-permute-done((bf16[512,256]{1,0:T(8,128)(2,1)S(1)}, bf16[512,256]{1,0:T(8,128)(2,1)S(1)}, u32[]{:S(2)}, u32[]{:S(2)}) %collective-permute-start.38) | collective-permute-done | bytes 262176 | tf_op jit(solution)/shard_map/ppermute | solution.py:23
  164.1 3.5 %collective-permute-start.39 = (bf16[1024,256]{1,0:T(8,128)(2,1)S(1)}, bf16[1024,256]{1,0:T(8,128)(2,1)S(1)}, u32[]{:S(2)}, u32[]{:S(2)}) collective-permute-start(bf16[1024,256]{1,0:T(8,128)(2,1)S(1)} %pad_maximum_fusion.5), channel_id=1, source_target_pairs={{0,6},{2,0},{4,2},{6,4},{1,7},{3,1},{5,3},{7,5},{8,14},{10,8},{12,... | collective-permute-start | bytes 1572872 | tf_op jit(solution)/shard_map/ppermute | solution.py:23
  167.9 10.1 %collective-permute-done.39 = bf16[1024,256]{1,0:T(8,128)(2,1)S(1)} collective-permute-done((bf16[1024,256]{1,0:T(8,128)(2,1)S(1)}, bf16[1024,256]{1,0:T(8,128)(2,1)S(1)}, u32[]{:S(2)}, u32[]{:S(2)}) %collective-permute-start.39) | collective-permute-done | bytes 524320 | tf_op jit(solution)/shard_map/ppermute | solution.py:23
  178.0 3.4 %collective-permute-done.37 = bf16[1024,256]{1,0:T(8,128)(2,1)S(1)} collective-permute-done((bf16[1024,256]{1,0:T(8,128)(2,1)S(1)}, bf16[1024,256]{1,0:T(8,128)(2,1)S(1)}, u32[]{:S(2)}, u32[]{:S(2)}) %collective-permute-start.37) | collective-permute-done | bytes 524320 | tf_op jit(solution)/shard_map/ppermute | solution.py:23
  (71 shorter events, 14.1 us)
Async XLA Ops:
  0.0 12.9 %collective-permute-start = (bf16[1024,256]{1,0:T(8,128)(2,1)}, bf16[1024,256]{1,0:T(8,128)(2,1)S(1)}, u32[]{:S(2)}, u32[]{:S(2)}) collective-permute-start(bf16[1024,256]{1,0:T(8,128)(2,1)} %bitcast.62), channel_id=1, source_target_pairs={{0,2},{2,4},{4,6},{6,0},{1,3},{3,5},{5,7},{7,1},{8,10},{10,12},{12... | collective-permute-start | bytes 1572872 | tf_op jit(solution)/shard_map/ppermute | solution.py:23
  2.0 12.5 %collective-permute-start.1 = (bf16[1024,256]{1,0:T(8,128)(2,1)}, bf16[1024,256]{1,0:T(8,128)(2,1)S(1)}, u32[]{:S(2)}, u32[]{:S(2)}) collective-permute-start(bf16[1024,256]{1,0:T(8,128)(2,1)} %bitcast.63), channel_id=1, source_target_pairs={{0,6},{2,0},{4,2},{6,4},{1,7},{3,1},{5,3},{7,5},{8,14},{10,8},{12,... | collective-permute-start | bytes 1572872 | tf_op jit(solution)/shard_map/ppermute | solution.py:23
  3.3 24.0 %collective-permute-start.2 = (bf16[1024,256]{1,0:T(8,128)(2,1)}, bf16[1024,256]{1,0:T(8,128)(2,1)S(1)}, u32[]{:S(2)}, u32[]{:S(2)}) collective-permute-start(bf16[1024,256]{1,0:T(8,128)(2,1)} %bitcast.64), channel_id=1, source_target_pairs={{0,4},{2,6},{4,0},{6,2},{1,5},{3,7},{5,1},{7,3},{8,12},{10,14},{12... | collective-permute-start | bytes 1572872 | tf_op jit(solution)/shard_map/ppermute | solution.py:23
  27.3 2.8 %copy-start.1 = (bf16[1024,256]{1,0:T(8,128)(2,1)}, bf16[1024,256]{1,0:T(8,128)(2,1)S(1)}, u32[]{:S(2)}) copy-start(bf16[1024,256]{1,0:T(8,128)(2,1)S(1)} %collective-permute-done.2.refs_3_) | copy-start | bytes 1572868
  30.1 47.2 %collective-permute-start.3 = (bf16[4,1024,256]{2,1,0:T(8,128)(2,1)}, bf16[4,1024,256]{2,1,0:T(8,128)(2,1)S(1)}, u32[]{:S(2)}, u32[]{:S(2)}) collective-permute-start(bf16[4,1024,256]{2,1,0:T(8,128)(2,1)} %pad_maximum_fusion), channel_id=1, source_target_pairs={{0,1},{1,0},{2,3},{3,2},{4,5},{5,4},{6,7},{7,6},{8,9},{9,8},{10,11... | collective-permute-start | bytes 6291464 | tf_op jit(solution)/shard_map/ppermute | solution.py:23
  31.6 49.5 %copy-start = (bf16[1,1024,256]{2,1,0:T(8,128)(2,1)S(1)}, bf16[1,1024,256]{2,1,0:T(8,128)(2,1)}, u32[]{:S(2)}) copy-start(bf16[1,1024,256]{2,1,0:T(8,128)(2,1)} %param.12) | copy-start | bytes 1572868
  31.6 49.5 %copy-start.3 = (bf16[4,128,128]{2,1,0:T(8,128)(2,1)S(1)}, bf16[4,128,128]{2,1,0:T(8,128)(2,1)}, u32[]{:S(2)}) copy-start(bf16[4,128,128]{2,1,0:T(8,128)(2,1)} %refs_7_.1) | copy-start | bytes 393220
  34.0 47.1 %copy-start.2 = (bf16[1024,256]{1,0:T(8,128)(2,1)S(1)}, bf16[1024,256]{1,0:T(8,128)(2,1)}, u32[]{:S(2)}) copy-start(bf16[1024,256]{1,0:T(8,128)(2,1)} %copy-done.1) | copy-start | bytes 1572868
  34.0 8.4 %collective-permute-start.6 = (bf16[24,1024]{1,0:T(8,128)(2,1)}, bf16[24,1024]{1,0:T(8,128)(2,1)S(1)}, u32[]{:S(2)}, u32[]{:S(2)}) collective-permute-start(bf16[24,1024]{1,0:T(8,128)(2,1)} %get-tuple-element.22), channel_id=1, source_target_pairs={{0,64},{32,96},{64,128},{96,160},{128,192},{160,224},{192,0},{224,... | collective-permute-start | bytes 147464 | tf_op jit(solution)/shard_map/ppermute | solution.py:23
  37.1 5.3 %collective-permute-start.5 = (bf16[24,1024]{1,0:T(8,128)(2,1)}, bf16[24,1024]{1,0:T(8,128)(2,1)S(1)}, u32[]{:S(2)}, u32[]{:S(2)}) collective-permute-start(bf16[24,1024]{1,0:T(8,128)(2,1)} %get-tuple-element.22), channel_id=1, source_target_pairs={{0,224},{32,0},{64,32},{96,64},{128,96},{160,128},{192,160},{224,1... | collective-permute-start | bytes 147464 | tf_op jit(solution)/shard_map/ppermute | solution.py:23
  39.8 4.4 %collective-permute-start.4 = (bf16[24,1024]{1,0:T(8,128)(2,1)}, bf16[24,1024]{1,0:T(8,128)(2,1)S(1)}, u32[]{:S(2)}, u32[]{:S(2)}) collective-permute-start(bf16[24,1024]{1,0:T(8,128)(2,1)} %get-tuple-element.22), channel_id=1, source_target_pairs={{0,32},{32,64},{64,96},{96,128},{128,160},{160,192},{192,224},{224... | collective-permute-start | bytes 147464 | tf_op jit(solution)/shard_map/ppermute | solution.py:23
  45.0 6.4 %collective-permute-start.7 = (bf16[4,24,1024]{2,1,0:T(8,128)(2,1)S(1)}, bf16[4,24,1024]{2,1,0:T(8,128)(2,1)S(1)}, u32[]{:S(2)}, u32[]{:S(2)}) collective-permute-start(bf16[4,24,1024]{2,1,0:T(8,128)(2,1)S(1)} %pad_maximum_fusion.7.m0), channel_id=1, source_target_pairs={{0,8},{8,16},{16,24},{24,0},{1,9},{9,17},{17,25},{25,1},{2,10},{10... | collective-permute-start | bytes 589832 | tf_op jit(solution)/shard_map/ppermute | solution.py:23
  46.3 6.5 %collective-permute-start.8 = (bf16[4,24,1024]{2,1,0:T(8,128)(2,1)S(1)}, bf16[4,24,1024]{2,1,0:T(8,128)(2,1)S(1)}, u32[]{:S(2)}, u32[]{:S(2)}) collective-permute-start(bf16[4,24,1024]{2,1,0:T(8,128)(2,1)S(1)} %pad_maximum_fusion.7.m0), channel_id=1, source_target_pairs={{0,24},{8,0},{16,8},{24,16},{1,25},{9,1},{17,9},{25,17},{2,26},{10... | collective-permute-start | bytes 589832 | tf_op jit(solution)/shard_map/ppermute | solution.py:23
  47.9 8.9 %collective-permute-start.9 = (bf16[4,24,1024]{2,1,0:T(8,128)(2,1)S(1)}, bf16[4,24,1024]{2,1,0:T(8,128)(2,1)S(1)}, u32[]{:S(2)}, u32[]{:S(2)}) collective-permute-start(bf16[4,24,1024]{2,1,0:T(8,128)(2,1)S(1)} %pad_maximum_fusion.7.m0), channel_id=1, source_target_pairs={{0,16},{8,24},{16,0},{24,8},{1,17},{9,25},{17,1},{25,9},{2,18},{10... | collective-permute-start | bytes 589832 | tf_op jit(solution)/shard_map/ppermute | solution.py:23
  49.4 15.0 %collective-permute-start.21 = (bf16[128,1024]{1,0:T(8,128)(2,1)}, bf16[128,1024]{1,0:T(8,128)(2,1)S(1)}, u32[]{:S(2)}, u32[]{:S(2)}) collective-permute-start(bf16[128,1024]{1,0:T(8,128)(2,1)} %get-tuple-element.31), channel_id=1, source_target_pairs={{0,16},{8,24},{16,0},{24,8},{1,17},{9,25},{17,1},{25,9},{2,18},{10... | collective-permute-start | bytes 786440 | tf_op jit(solution)/shard_map/ppermute | solution.py:23
  51.4 15.9 %collective-permute-start.20 = (bf16[128,1024]{1,0:T(8,128)(2,1)}, bf16[128,1024]{1,0:T(8,128)(2,1)S(1)}, u32[]{:S(2)}, u32[]{:S(2)}) collective-permute-start(bf16[128,1024]{1,0:T(8,128)(2,1)} %get-tuple-element.31), channel_id=1, source_target_pairs={{0,24},{8,0},{16,8},{24,16},{1,25},{9,1},{17,9},{25,17},{2,26},{10... | collective-permute-start | bytes 786440 | tf_op jit(solution)/shard_map/ppermute | solution.py:23
  57.1 18.9 %collective-permute-start.10 = (bf16[2064,128]{1,0:T(8,128)(2,1)S(1)}, bf16[2064,128]{1,0:T(8,128)(2,1)S(1)}, u32[]{:S(2)}, u32[]{:S(2)}) collective-permute-start(bf16[2064,128]{1,0:T(8,128)(2,1)S(1)} %get-tuple-element.23.refs_5_), channel_id=1, source_target_pairs={{0,1},{1,0},{2,3},{3,2},{4,5},{5,4},{6,7},{7,6},{8,9},{9,8},{10,11... | collective-permute-start | bytes 1585160 | tf_op jit(solution)/shard_map/ppermute | solution.py:23
  62.6 10.7 %collective-permute-start.19 = (bf16[128,1024]{1,0:T(8,128)(2,1)}, bf16[128,1024]{1,0:T(8,128)(2,1)S(1)}, u32[]{:S(2)}, u32[]{:S(2)}) collective-permute-start(bf16[128,1024]{1,0:T(8,128)(2,1)} %get-tuple-element.31), channel_id=1, source_target_pairs={{0,8},{8,16},{16,24},{24,0},{1,9},{9,17},{17,25},{25,1},{2,10},{10... | collective-permute-start | bytes 786440 | tf_op jit(solution)/shard_map/ppermute | solution.py:23
  64.4 9.4 %collective-permute-start.15 = (bf16[528,256]{1,0:T(8,128)(2,1)S(1)}, bf16[528,256]{1,0:T(8,128)(2,1)S(1)}, u32[]{:S(2)}, u32[]{:S(2)}) collective-permute-start(bf16[528,256]{1,0:T(8,128)(2,1)S(1)} %get-tuple-element.26.refs_10_), channel_id=1, source_target_pairs={{0,2},{2,4},{4,6},{6,0},{1,3},{3,5},{5,7},{7,1},{8,10},{10,12},{12... | collective-permute-start | bytes 811016 | tf_op jit(solution)/shard_map/ppermute | solution.py:23
  67.3 6.8 %collective-permute-start.16 = (bf16[528,256]{1,0:T(8,128)(2,1)S(1)}, bf16[528,256]{1,0:T(8,128)(2,1)S(1)}, u32[]{:S(2)}, u32[]{:S(2)}) collective-permute-start(bf16[528,256]{1,0:T(8,128)(2,1)S(1)} %get-tuple-element.26.refs_10_), channel_id=1, source_target_pairs={{0,6},{2,0},{4,2},{6,4},{1,7},{3,1},{5,3},{7,5},{8,14},{10,8},{12,... | collective-permute-start | bytes 811016 | tf_op jit(solution)/shard_map/ppermute | solution.py:23
  73.3 11.5 %collective-permute-start.17 = (bf16[528,256]{1,0:T(8,128)(2,1)S(1)}, bf16[528,256]{1,0:T(8,128)(2,1)S(1)}, u32[]{:S(2)}, u32[]{:S(2)}) collective-permute-start(bf16[528,256]{1,0:T(8,128)(2,1)S(1)} %get-tuple-element.26.refs_10_), channel_id=1, source_target_pairs={{0,4},{2,6},{4,0},{6,2},{1,5},{3,7},{5,1},{7,3},{8,12},{10,14},{12... | collective-permute-start | bytes 811016 | tf_op jit(solution)/shard_map/ppermute | solution.py:23
  73.8 15.5 %collective-permute-start.28 = (bf16[128,1024]{1,0:T(8,128)(2,1)}, bf16[128,1024]{1,0:T(8,128)(2,1)S(1)}, u32[]{:S(2)}, u32[]{:S(2)}) collective-permute-start(bf16[128,1024]{1,0:T(8,128)(2,1)} %get-tuple-element.32), channel_id=1, source_target_pairs={{0,64},{32,96},{64,128},{96,160},{128,192},{160,224},{192,0},{224,... | collective-permute-start | bytes 786440 | tf_op jit(solution)/shard_map/ppermute | solution.py:23
  74.2 15.2 %collective-permute-start.27 = (bf16[128,1024]{1,0:T(8,128)(2,1)}, bf16[128,1024]{1,0:T(8,128)(2,1)S(1)}, u32[]{:S(2)}, u32[]{:S(2)}) collective-permute-start(bf16[128,1024]{1,0:T(8,128)(2,1)} %get-tuple-element.32), channel_id=1, source_target_pairs={{0,224},{32,0},{64,32},{96,64},{128,96},{160,128},{192,160},{224,1... | collective-permute-start | bytes 786440 | tf_op jit(solution)/shard_map/ppermute | solution.py:23
  76.0 16.9 %collective-permute-start.26 = (bf16[128,1024]{1,0:T(8,128)(2,1)}, bf16[128,1024]{1,0:T(8,128)(2,1)S(1)}, u32[]{:S(2)}, u32[]{:S(2)}) collective-permute-start(bf16[128,1024]{1,0:T(8,128)(2,1)} %get-tuple-element.32), channel_id=1, source_target_pairs={{0,32},{32,64},{64,96},{96,128},{128,160},{160,192},{192,224},{224... | collective-permute-start | bytes 786440 | tf_op jit(solution)/shard_map/ppermute | solution.py:23
  77.3 38.1 %collective-permute-start.22 = (bf16[4,128,1024]{2,1,0:T(8,128)(2,1)S(1)}, bf16[4,128,1024]{2,1,0:T(8,128)(2,1)S(1)}, u32[]{:S(2)}, u32[]{:S(2)}) collective-permute-start(bf16[4,128,1024]{2,1,0:T(8,128)(2,1)S(1)} %pad_maximum_fusion.2.refs_0_), channel_id=1, source_target_pairs={{0,32},{32,64},{64,96},{96,128},{128,160},{160,192},{192,224},{224... | collective-permute-start | bytes 3145736 | tf_op jit(solution)/shard_map/ppermute | solution.py:23
  84.7 11.7 %copy-start.4 = (bf16[128,1024]{1,0:T(8,128)(2,1)S(1)}, bf16[128,1024]{1,0:T(8,128)(2,1)}, u32[]{:S(2)}) copy-start(bf16[128,1024]{1,0:T(8,128)(2,1)} %get-tuple-element.32) | copy-start | bytes 786436
  84.8 10.9 %collective-permute-start.11 = (bf16[512,128]{1,0:T(8,128)(2,1)S(1)}, bf16[512,128]{1,0:T(8,128)(2,1)S(1)}, u32[]{:S(2)}, u32[]{:S(2)}) collective-permute-start(bf16[512,128]{1,0:T(8,128)(2,1)S(1)} %get-tuple-element.25), channel_id=1, source_target_pairs={{0,2},{2,4},{4,6},{6,0},{1,3},{3,5},{5,7},{7,1},{8,10},{10,12},{12... | collective-permute-start | bytes 393224 | tf_op jit(solution)/shard_map/ppermute | solution.py:23
  89.3 27.9 %collective-permute-start.23 = (bf16[4,128,1024]{2,1,0:T(8,128)(2,1)S(1)}, bf16[4,128,1024]{2,1,0:T(8,128)(2,1)S(1)}, u32[]{:S(2)}, u32[]{:S(2)}) collective-permute-start(bf16[4,128,1024]{2,1,0:T(8,128)(2,1)S(1)} %pad_maximum_fusion.2.refs_0_), channel_id=1, source_target_pairs={{0,224},{32,0},{64,32},{96,64},{128,96},{160,128},{192,160},{224,1... | collective-permute-start | bytes 3145736 | tf_op jit(solution)/shard_map/ppermute | solution.py:23
  89.3 34.2 %collective-permute-start.18 = (bf16[4,528,256]{2,1,0:T(8,128)(2,1)S(1)}, bf16[4,528,256]{2,1,0:T(8,128)(2,1)S(1)}, u32[]{:S(2)}, u32[]{:S(2)}) collective-permute-start(bf16[4,528,256]{2,1,0:T(8,128)(2,1)S(1)} %pad_maximum_fusion.1), channel_id=1, source_target_pairs={{0,1},{1,0},{2,3},{3,2},{4,5},{5,4},{6,7},{7,6},{8,9},{9,8},{10,11... | collective-permute-start | bytes 3244040 | tf_op jit(solution)/shard_map/ppermute | solution.py:23
  92.9 6.0 %collective-permute-start.12 = (bf16[512,128]{1,0:T(8,128)(2,1)S(1)}, bf16[512,128]{1,0:T(8,128)(2,1)S(1)}, u32[]{:S(2)}, u32[]{:S(2)}) collective-permute-start(bf16[512,128]{1,0:T(8,128)(2,1)S(1)} %get-tuple-element.25), channel_id=1, source_target_pairs={{0,6},{2,0},{4,2},{6,4},{1,7},{3,1},{5,3},{7,5},{8,14},{10,8},{12,... | collective-permute-start | bytes 393224 | tf_op jit(solution)/shard_map/ppermute | solution.py:23
  95.6 5.3 %collective-permute-start.13 = (bf16[512,128]{1,0:T(8,128)(2,1)S(1)}, bf16[512,128]{1,0:T(8,128)(2,1)S(1)}, u32[]{:S(2)}, u32[]{:S(2)}) collective-permute-start(bf16[512,128]{1,0:T(8,128)(2,1)S(1)} %get-tuple-element.25), channel_id=1, source_target_pairs={{0,4},{2,6},{4,0},{6,2},{1,5},{3,7},{5,1},{7,3},{8,12},{10,14},{12... | collective-permute-start | bytes 393224 | tf_op jit(solution)/shard_map/ppermute | solution.py:23
  98.9 21.8 %collective-permute-start.29 = (bf16[4,128,1024]{2,1,0:T(8,128)(2,1)S(1)}, bf16[4,128,1024]{2,1,0:T(8,128)(2,1)S(1)}, u32[]{:S(2)}, u32[]{:S(2)}) collective-permute-start(bf16[4,128,1024]{2,1,0:T(8,128)(2,1)S(1)} %pad_maximum_fusion.3.b0), channel_id=1, source_target_pairs={{0,8},{8,16},{16,24},{24,0},{1,9},{9,17},{17,25},{25,1},{2,10},{10... | collective-permute-start | bytes 3145736 | tf_op jit(solution)/shard_map/ppermute | solution.py:23
  100.9 22.5 %collective-permute-start.30 = (bf16[4,128,1024]{2,1,0:T(8,128)(2,1)S(1)}, bf16[4,128,1024]{2,1,0:T(8,128)(2,1)S(1)}, u32[]{:S(2)}, u32[]{:S(2)}) collective-permute-start(bf16[4,128,1024]{2,1,0:T(8,128)(2,1)S(1)} %pad_maximum_fusion.3.b0), channel_id=1, source_target_pairs={{0,24},{8,0},{16,8},{24,16},{1,25},{9,1},{17,9},{25,17},{2,26},{10... | collective-permute-start | bytes 3145736 | tf_op jit(solution)/shard_map/ppermute | solution.py:23
  115.4 11.6 %collective-permute-start.14 = (bf16[3,512,128]{2,1,0:T(8,128)(2,1)S(1)}, bf16[3,512,128]{2,1,0:T(8,128)(2,1)S(1)}, u32[]{:S(2)}, u32[]{:S(2)}) collective-permute-start(bf16[3,512,128]{2,1,0:T(8,128)(2,1)S(1)} %pad_maximum_fusion.6), channel_id=1, source_target_pairs={{0,1},{1,0},{2,3},{3,2},{4,5},{5,4},{6,7},{7,6},{8,9},{9,8},{10,11... | collective-permute-start | bytes 1179656 | tf_op jit(solution)/shard_map/ppermute | solution.py:23
  117.2 18.8 %collective-permute-start.24 = (bf16[2,128,1024]{2,1,0:T(8,128)(2,1)S(1)}, bf16[2,128,1024]{2,1,0:T(8,128)(2,1)S(1)}, u32[]{:S(2)}, u32[]{:S(2)}) collective-permute-start(bf16[2,128,1024]{2,1,0:T(8,128)(2,1)S(1)} %slice.78), channel_id=1, source_target_pairs={{0,32},{32,64},{64,96},{96,128},{128,160},{160,192},{192,224},{224... | collective-permute-start | bytes 1572872 | tf_op jit(solution)/shard_map/ppermute | solution.py:23
  120.8 15.3 %collective-permute-start.25 = (bf16[2,128,1024]{2,1,0:T(8,128)(2,1)S(1)}, bf16[2,128,1024]{2,1,0:T(8,128)(2,1)S(1)}, u32[]{:S(2)}, u32[]{:S(2)}) collective-permute-start(bf16[2,128,1024]{2,1,0:T(8,128)(2,1)S(1)} %slice.79), channel_id=1, source_target_pairs={{0,224},{32,0},{64,32},{96,64},{128,96},{160,128},{192,160},{224,1... | collective-permute-start | bytes 1572872 | tf_op jit(solution)/shard_map/ppermute | solution.py:23
  123.4 15.2 %collective-permute-start.31 = (bf16[2,128,1024]{2,1,0:T(8,128)(2,1)S(1)}, bf16[2,128,1024]{2,1,0:T(8,128)(2,1)S(1)}, u32[]{:S(2)}, u32[]{:S(2)}) collective-permute-start(bf16[2,128,1024]{2,1,0:T(8,128)(2,1)S(1)} %slice.80), channel_id=1, source_target_pairs={{0,8},{8,16},{16,24},{24,0},{1,9},{9,17},{17,25},{25,1},{2,10},{10... | collective-permute-start | bytes 1572872 | tf_op jit(solution)/shard_map/ppermute | solution.py:23
  123.6 15.1 %collective-permute-start.32 = (bf16[2,128,1024]{2,1,0:T(8,128)(2,1)S(1)}, bf16[2,128,1024]{2,1,0:T(8,128)(2,1)S(1)}, u32[]{:S(2)}, u32[]{:S(2)}) collective-permute-start(bf16[2,128,1024]{2,1,0:T(8,128)(2,1)S(1)} %slice.81), channel_id=1, source_target_pairs={{0,24},{8,0},{16,8},{24,16},{1,25},{9,1},{17,9},{25,17},{2,26},{10... | collective-permute-start | bytes 1572872 | tf_op jit(solution)/shard_map/ppermute | solution.py:23
  142.9 15.5 %collective-permute-start.34 = (bf16[2,1024,256]{2,1,0:T(8,128)(2,1)S(1)}, bf16[2,1024,256]{2,1,0:T(8,128)(2,1)S(1)}, u32[]{:S(2)}, u32[]{:S(2)}) collective-permute-start(bf16[2,1024,256]{2,1,0:T(8,128)(2,1)S(1)} %get-tuple-element.36), channel_id=1, source_target_pairs={{0,1},{1,0},{2,3},{3,2},{4,5},{5,4},{6,7},{7,6},{8,9},{9,8},{10,11... | collective-permute-start | bytes 3145736 | tf_op jit(solution)/shard_map/ppermute | solution.py:23
  149.7 2.8 %collective-permute-start.35 = (bf16[1,1024,256]{2,1,0:T(8,128)(2,1)S(1)}, bf16[1,1024,256]{2,1,0:T(8,128)(2,1)S(1)}, u32[]{:S(2)}, u32[]{:S(2)}) collective-permute-start(bf16[1,1024,256]{2,1,0:T(8,128)(2,1)S(1)} %get-tuple-element.38), channel_id=1, source_target_pairs={{0,1},{1,0},{2,3},{3,2},{4,5},{5,4},{6,7},{7,6},{8,9},{9,8},{10,11... | collective-permute-start | bytes 1572872 | tf_op jit(solution)/shard_map/ppermute | solution.py:23
  152.0 15.9 %collective-permute-start.33 = (bf16[1,1024,256]{2,1,0:T(8,128)(2,1)S(1)}, bf16[1,1024,256]{2,1,0:T(8,128)(2,1)S(1)}, u32[]{:S(2)}, u32[]{:S(2)}) collective-permute-start(bf16[1,1024,256]{2,1,0:T(8,128)(2,1)S(1)} %get-tuple-element.34), channel_id=1, source_target_pairs={{0,1},{1,0},{2,3},{3,2},{4,5},{5,4},{6,7},{7,6},{8,9},{9,8},{10,11... | collective-permute-start | bytes 1572872 | tf_op jit(solution)/shard_map/ppermute | solution.py:23
  152.7 11.3 %collective-permute-start.38 = (bf16[512,256]{1,0:T(8,128)(2,1)S(1)}, bf16[512,256]{1,0:T(8,128)(2,1)S(1)}, u32[]{:S(2)}, u32[]{:S(2)}) collective-permute-start(bf16[512,256]{1,0:T(8,128)(2,1)S(1)} %get-tuple-element.42), channel_id=1, source_target_pairs={{0,6},{2,0},{4,2},{6,4},{1,7},{3,1},{5,3},{7,5},{8,14},{10,8},{12,... | collective-permute-start | bytes 786440 | tf_op jit(solution)/shard_map/ppermute | solution.py:23
  158.4 9.2 %collective-permute-start.36 = (bf16[512,256]{1,0:T(8,128)(2,1)S(1)}, bf16[512,256]{1,0:T(8,128)(2,1)S(1)}, u32[]{:S(2)}, u32[]{:S(2)}) collective-permute-start(bf16[512,256]{1,0:T(8,128)(2,1)S(1)} %get-tuple-element.41), channel_id=1, source_target_pairs={{0,2},{2,4},{4,6},{6,0},{1,3},{3,5},{5,7},{7,1},{8,10},{10,12},{12... | collective-permute-start | bytes 786440 | tf_op jit(solution)/shard_map/ppermute | solution.py:23
  164.1 13.9 %collective-permute-start.39 = (bf16[1024,256]{1,0:T(8,128)(2,1)S(1)}, bf16[1024,256]{1,0:T(8,128)(2,1)S(1)}, u32[]{:S(2)}, u32[]{:S(2)}) collective-permute-start(bf16[1024,256]{1,0:T(8,128)(2,1)S(1)} %pad_maximum_fusion.5), channel_id=1, source_target_pairs={{0,6},{2,0},{4,2},{6,4},{1,7},{3,1},{5,3},{7,5},{8,14},{10,8},{12,... | collective-permute-start | bytes 1572872 | tf_op jit(solution)/shard_map/ppermute | solution.py:23
  167.8 13.6 %collective-permute-start.37 = (bf16[1024,256]{1,0:T(8,128)(2,1)S(1)}, bf16[1024,256]{1,0:T(8,128)(2,1)S(1)}, u32[]{:S(2)}, u32[]{:S(2)}) collective-permute-start(bf16[1024,256]{1,0:T(8,128)(2,1)S(1)} %pad_maximum_fusion.4), channel_id=1, source_target_pairs={{0,2},{2,4},{4,6},{6,0},{1,3},{3,5},{5,7},{7,1},{8,10},{10,12},{12... | collective-permute-start | bytes 1572872 | tf_op jit(solution)/shard_map/ppermute | solution.py:23

commit v3 on v2

--- a/solution.py
+++ b/solution.py
@@ -68,7 +68,7 @@
 
 def prep_kernel(
     norm_gain_at, w_in_at, s_in_at, w_out_at, s_out_at, ffn_gain_at, w_up_at, s_up_at, w_down_at, s_down_at,
-    mixer, up, down, small, norm_gain, w_in, s_in, w_out, s_out, ffn_gain, w_up, s_up, w_down, s_down, done,
+    packet, up, top, bottom, small, norm_gain, w_in, s_in, w_out, s_out, ffn_gain, w_up, s_up, w_down, s_down, done,
 ):
     sources = (norm_gain_at, w_in_at, s_in_at, w_out_at, s_out_at, s_up_at, ffn_gain_at, w_up_at, w_down_at, s_down_at)
     targets = (norm_gain, w_in, s_in, w_out, s_out, s_up, ffn_gain, w_up, w_down, s_down)
@@ -90,26 +90,29 @@
         high, low = two_parts(row)
         small[16:17, at : at + row.shape[1]] = high
         small[16:17, at + 128 : at + 128 + row.shape[1]] = low
-    mixer[...] = small[...].astype(BF)
+    packet[128:] = small[...].astype(BF)
     for copy in copies[6:]:
         copy.wait()
     gain = column_of(ffn_gain[pl.ds(f, 1), :])
     for j in range(8):
         lanes = slice(j * 128, j * 128 + 128)
         up[:, lanes] = (w_up[:, lanes] * gain).astype(BF)
-        down[:, lanes] = (w_down[lanes, :] * s_down[...]).T.astype(BF)
-
-
-def unpack_kernel(m0, m1, m2, m3, w_in, w_out, s_up):
+        packet[:128, lanes] = (w_down[lanes, :] * s_down[...]).T.astype(BF)
+    top[...] = up[:64]
+    bottom[...] = up[64:]
+
+
+def unpack_kernel(m0, m1, m2, m3, m4, w_in, w_out, s_up):
     ys, zs = around(lax.axis_index("y")), around(lax.axis_index("z"))
     lane = lax.broadcasted_iota(jnp.int32, (16, 128), 1)
     at = lax.broadcasted_iota(jnp.int32, (16, 128), 0)
     low_lanes = lane[:8] < 64
     firsts = [jnp.zeros((16, 128), F32) for _ in range(6)]
-    for m, yy in zip((m0, m1, m2, m3), ys):
-        for k, zz in enumerate(zs):
+    for p, zz in enumerate(zs):
+        for k, yy in enumerate(ys):
             f = 4 * zz + yy
-            block = m[k].astype(F32)
+            source = (m0, m1, m2)[p].at[k] if p < 3 else (m3, m4)[k // 2].at[k % 2]
+            block = source[...].astype(F32)
             for j in range(8):
                 part = block[:8, j * 128 : j * 128 + 128]
                 turned = pltpu.roll(part, 64, 1)
@@ -238,11 +241,11 @@
         factor[rows, :] = jnp.broadcast_to(lax.rsqrt(mean + EPS), (256, 128))
 
 
-def up_parts_sum(mixed, parts, zs, rows, cols, total):
-    ys = around(lax.axis_index("y"))
+def up_parts_sum(mixed, parts, ys, rows, cols, total):
+    zs = around(lax.axis_index("z"))
     for k, part in enumerate(parts):
         left = [
-            mixed[rows, pl.ds(pl.multiple_of((4 * zs[k // 2] + ys[2 * (k % 2) + i]) * 128, 128), 128)]
+            mixed[rows, pl.ds(pl.multiple_of((4 * zs[2 * (k % 2) + i] + ys[k // 2]) * 128, 128), 128)]
             for i in range(2)
         ]
         total += dot(jnp.concatenate(left, axis=1), part[:, :, cols].reshape(256, 256))
@@ -256,55 +259,69 @@
 
 def up_near_kernel(mixed, *refs):
     parts, out = refs[:-1], refs[-1]
-    zs = around(lax.axis_index("z"))
+    ys = around(lax.axis_index("y"))
     if len(parts) == 3:
         parts = [b.at[pl.ds(2 * k, 2)] for b in parts for k in range(2)]
 
     @pl.loop(0, 4 * 2)
     def _(step):
         rows, cols = tile_of(step)
-        out[rows, cols] = up_parts_sum(mixed, parts, zs, rows, cols, jnp.zeros((512, 256), F32))
+        out[rows, cols] = up_parts_sum(mixed, parts, ys, rows, cols, jnp.zeros((512, 256), F32))
 
 
 def up_far_kernel(mixed, factor, s_up, near, b3, b4, hidden):
-    zs = around(lax.axis_index("z"))[3:]
+    ys = around(lax.axis_index("y"))[3:]
 
     @pl.loop(0, 4 * 2)
     def _(step):
         rows, cols = tile_of(step)
-        total = up_parts_sum(mixed, (b3, b4), zs, rows, cols, near[rows, cols])
+        total = up_parts_sum(mixed, (b3, b4), ys, rows, cols, near[rows, cols])
         scale = jnp.concatenate([factor[rows, :]] * 2, axis=1) * s_up[:, cols]
         value = jnp.maximum(total * scale, 0.0)
         hidden[rows, cols] = (value * value).astype(BF)
 
 
-def down_kernel(steps, hidden, b0, b1, b2, b3, b4, own, other):
+def down_kernel(steps, hidden, b0, b1, b2, b3, b4, own, other, taken):
     x, y, z = (lax.axis_index(name) for name in ("x", "y", "z"))
     core = lax.shift_right_logical(y, 1)
     y_is_own = core == lax.axis_index("c")
     low_is_own = y_is_own == (jnp.bitwise_and(y, 1) == 1)
     side = jnp.bitwise_and(y, 1)
 
-    @pl.loop(0, 4 * len(steps))
-    def _(step):
-        rows = pl.ds(pl.multiple_of(lax.rem(step, 4) * 256, 256), 256)
-        k = lax.div(step, 4)
+    @pl.loop(0, len(steps))
+    def _(k):
         chip = lax.rem(x + ((2 * k + 1) if len(steps) > 1 else steps[0]), 4)
         away = lax.rem(chip - z + 4, 4)
-        place = jnp.where(away == 0, 0, jnp.where(away == 1, 2, jnp.where(away == 2, 3, 1)))
-        inner = jnp.bitwise_and(place, 1)
-        far = jnp.where(place < 2, b3[inner], b4[inner])
-        for first, second, first_is_own, lane in (
-            (b0[place], far, y_is_own, side),
-            (b1[place], b2[place], low_is_own, 1 - side),
-        ):
-            weight = jnp.concatenate(
-                [jnp.where(first_is_own, second, first), jnp.where(first_is_own, first, second)], axis=0
-            )
-            value = dot_t(hidden[rows, :], weight).astype(BF)
-            lanes = pl.ds(pl.multiple_of(lane * 128, 128), 128)
-            other[k, rows, lanes] = value[:, :128]
-            own[k, rows, lanes] = value[:, 128:]
+        for place, source in ((0, b0), (3, b1), (1, b2)):
+
+            @pl.when(away == place)
+            def _(source=source):
+                @pl.loop(0, 4)
+                def _(i):
+                    taken[i] = source[i]
+
+        @pl.when(away == 2)
+        def _():
+            @pl.loop(0, 2)
+            def _(i):
+                taken[i] = b3[i]
+                taken[i + 2] = b4[i]
+
+        @pl.loop(0, 2)
+        def _(block):
+            rows = pl.ds(pl.multiple_of(block * 512, 512), 512)
+            for first, second, first_is_own, lane in (
+                (taken[0], taken[3], y_is_own, side),
+                (taken[1], taken[2], low_is_own, 1 - side),
+            ):
+                weight = jnp.concatenate(
+                    [jnp.where(first_is_own, second, first), jnp.where(first_is_own, first, second)],
+                    axis=0,
+                )
+                value = dot_t(hidden[rows, :], weight).astype(BF)
+                lanes = pl.ds(pl.multiple_of(lane * 128, 128), 128)
+                other[k, rows, lanes] = value[:, :128]
+                own[k, rows, lanes] = value[:, 128:]
 
 
 def along(bundle, axes):
@@ -351,9 +368,9 @@
         w_down,
         s_down[None],
     )
-    packet, up, down = call(
+    packet, up, top, bottom = call(
         prep_kernel,
-        (bf(24, 1024), bf(128, 1024), bf(128, 1024)),
+        (bf(152, 1024), bf(128, 1024), bf(64, 1024), bf(64, 1024)),
         [pltpu.VMEM((24, 1024), F32)]
         + [pltpu.VMEM(a.shape, F32) for a in arrays]
         + [pltpu.SemaphoreType.DMA((10,))],
@@ -362,12 +379,16 @@
         *arrays,
         in_hbm=10,
     )
-    mixer = jnp.stack([packet] + three(packet, ring_z))
-    up_bundle = [up] + three(up, "y")
-    down_bundle = [down] + three(down, ring_z)
-    mixers = [mixer] + three(mixer, "y")
-    up_parts = along(jnp.stack(up_bundle), ring_z)
-    down_parts = along(jnp.stack(down_bundle), "y")
+    packets = [packet] + three(packet, "y")
+    far_top, far_bottom = send(top, ring_z, 2), send(bottom, ring_z, -2)
+    low, high = send(up, ring_z, 1), send(up, ring_z, -1)
+    far = jnp.concatenate([far_top, far_bottom], axis=0)
+    up_bundle = jnp.stack([up, low, high, far])
+    mixer = jnp.stack([p[128:] for p in packets])
+    mixers = [mixer, send(mixer, ring_z, 1), send(mixer, ring_z, -1)]
+    mixers += [send(mixer[:2], ring_z, 2), send(mixer[2:], ring_z, -2)]
+    up_parts = along(up_bundle, "y")
+    down_parts = along(jnp.stack([p[:128] for p in packets]), ring_z)
     w_in_own, out_own, s_up_row = call(
         unpack_kernel, (bf(2064, 128), bf(528, 256), f32(1, 1024)), [], 8, 1_000_000, *mixers
     )
@@ -411,7 +432,7 @@
         own, other = call(
             functools.partial(down_kernel, steps),
             (bf(count, SEQ, 256), bf(count, SEQ, 256)),
-            [],
+            [pltpu.VMEM((4, 128, 1024), BF)],
             32,
             1_075_000_000 * count,
             hidden,
@@ -421,12 +442,14 @@
         return [own[k].astype(F32) + crossed[k].astype(F32) for k in range(count)]
 
     (far,) = block_sums((2,))
-    from_low, from_high = send(far[:512].astype(BF), "x", 1), send(far[512:].astype(BF), "x", -1)
+    from_low = send(far[:512].astype(BF), "x", 1)
+    from_high = send(far[512:].astype(BF), "x", -1)
     after, before = block_sums((1, 3))
     (here,) = block_sums((0,))
     after = jnp.concatenate([after[:512] + from_low.astype(F32), after[512:]], axis=0)
     before = jnp.concatenate([before[:512], before[512:] + from_high.astype(F32)], axis=0)
-    low, high = send(after.astype(BF), "x", 1), send(before.astype(BF), "x", -1)
+    low = send(after.astype(BF), "x", 1)
+    high = send(before.astype(BF), "x", -1)
     total = mixed_own.astype(F32) + here + low.astype(F32) + high.astype(F32)
     return total.astype(BF)[None]
 

time: 183 us -> 159 us (0.87)
  waiting for transfers between devices: 80.7 us -> 65.5 us
  starting transfers between devices: 68 us -> 63 us
  other arithmetic: 6.81 us -> 3.54 us
    ppermute x40 -> x39, waiting for transfers between devices: 80.7 us -> 65.5 us  [send(): lax.ppermute(array, axes, [(i, (i + shift) % count) for i in range(count)])]
    ppermute x40 -> x39, starting transfers between devices: 68 us -> 63 us  [send(): lax.ppermute(array, axes, [(i, (i + shift) % count) for i in range(count)])]
  transfers between devices with their start and end apart: 40 -> 39, of which waited for: 18 -> 13; matrix products, arithmetic and copies ran while one was open for 2% -> 2% of each run, Pallas kernels for 12% -> 13%
where the time goes in v3:
time: 159 us; the launch traced here: 158 us
  waiting for transfers between devices  65.5 us (41%)
  starting transfers between devices  63 us (40%)
  Pallas kernels  24.7 us (16%)
  other arithmetic  3.54 us (2%)
    ppermute x39, waiting for transfers between devices, send(): lax.ppermute(array, axes, [(i, (i + shift) % count) for i in range(count)])  65.5 us
    ppermute x39, starting transfers between devices, send(): lax.ppermute(array, axes, [(i, (i + shift) % count) for i in range(count)])  63 us
    pallas_call x9, Pallas kernels, call(): pl.pallas_call(kernel, out_shape=out_shape, in_specs=[VMEM] * (len(args)...  24.7 us
  transfers between devices with their start and end apart: 39, of which 13 were waited for; matrix products, arithmetic and copies ran while one was open for 2% of the time, Pallas kernels for 13%

profile of v3, /device:TPU:1, one launch (start us, length us, event | category | flops | bytes accessed | tf_op | source)
XLA Modules:
  0.0 158.4 jit_solution(715481435684323563)
XLA Ops:
  0.0 2.0 %collective-permute-start = (bf16[1024,256]{1,0:T(8,128)(2,1)}, bf16[1024,256]{1,0:T(8,128)(2,1)S(1)}, u32[]{:S(2)}, u32[]{:S(2)}) collective-permute-start(bf16[1024,256]{1,0:T(8,128)(2,1)} %bitcast.71), channel_id=1, source_target_pairs={{0,2},{2,4},{4,6},{6,0},{1,3},{3,5},{5,7},{7,1},{8,10},{10,12},{12... | collective-permute-start | bytes 1572872 | tf_op jit(solution)/shard_map/ppermute | solution.py:23
  2.0 1.3 collective-permute-start.1
  3.3 1.7 %collective-permute-start.2 = (bf16[1024,256]{1,0:T(8,128)(2,1)}, bf16[1024,256]{1,0:T(8,128)(2,1)S(1)}, u32[]{:S(2)}, u32[]{:S(2)}) collective-permute-start(bf16[1024,256]{1,0:T(8,128)(2,1)} %bitcast.73), channel_id=1, source_target_pairs={{0,4},{2,6},{4,0},{6,2},{1,5},{3,7},{5,1},{7,3},{8,12},{10,14},{12... | collective-permute-start | bytes 1572872 | tf_op jit(solution)/shard_map/ppermute | solution.py:23
  5.0 2.4 %shard_map.118 = (bf16[152,1024]{1,0:T(8,128)(2,1)}, bf16[128,1024]{1,0:T(8,128)(2,1)}, bf16[64,1024]{1,0:T(8,128)(2,1)}, bf16[64,1024]{1,0:T(8,128)(2,1)}) custom-call(f32[16,128]{1,0:T(8,128)} %bitcast.90, f32[64,128]{1,0:T(8,128)} %bitcast.89, f32[1,4]{1,0:T(1,128)} %bitcast.92, f32[32,256]{1,0:T(8,128)} %w_out_at.1, f32[1,16]{1,0:T(1,128)} %bitcast.93, ...), custom_call_target="tpu_custom_call" | custom-call | flops 1000000 | bytes 1131344 | tf_op jit(solution)/shard_map/pallas_call | solution.py:54
  7.5 1.4 collective-permute-start.4
  8.8 2.6 %collective-permute-start.6 = (bf16[152,1024]{1,0:T(8,128)(2,1)}, bf16[152,1024]{1,0:T(8,128)(2,1)S(1)}, u32[]{:S(2)}, u32[]{:S(2)}) collective-permute-start(bf16[152,1024]{1,0:T(8,128)(2,1)} %get-tuple-element.23), channel_id=1, source_target_pairs={{0,16},{8,24},{16,0},{24,8},{1,17},{9,25},{17,1},{25,9},{2,18},{10... | collective-permute-start | bytes 933896 | tf_op jit(solution)/shard_map/ppermute | solution.py:23
  12.9 4.8 %collective-permute-start.5 = (bf16[152,1024]{1,0:T(8,128)(2,1)}, bf16[152,1024]{1,0:T(8,128)(2,1)S(1)}, u32[]{:S(2)}, u32[]{:S(2)}) collective-permute-start(bf16[152,1024]{1,0:T(8,128)(2,1)} %get-tuple-element.23), channel_id=1, source_target_pairs={{0,24},{8,0},{16,8},{24,16},{1,25},{9,1},{17,9},{25,17},{2,26},{10... | collective-permute-start | bytes 933896 | tf_op jit(solution)/shard_map/ppermute | solution.py:23
  17.8 3.0 %collective-permute-start.22 = (bf16[64,1024]{1,0:T(8,128)(2,1)}, bf16[64,1024]{1,0:T(8,128)(2,1)S(1)}, u32[]{:S(2)}, u32[]{:S(2)}) collective-permute-start(bf16[64,1024]{1,0:T(8,128)(2,1)} %get-tuple-element.33), channel_id=1, source_target_pairs={{0,64},{32,96},{64,128},{96,160},{128,192},{160,224},{192,0},{224,... | collective-permute-start | bytes 393224 | tf_op jit(solution)/shard_map/ppermute | solution.py:23
  20.8 6.5 %collective-permute-done.2.refs_3_ = bf16[1024,256]{1,0:T(8,128)(2,1)S(1)} collective-permute-done((bf16[1024,256]{1,0:T(8,128)(2,1)}, bf16[1024,256]{1,0:T(8,128)(2,1)S(1)}, u32[]{:S(2)}, u32[]{:S(2)}) %collective-permute-start.2) | collective-permute-done | bytes 524320 | tf_op jit(solution)/shard_map/ppermute | solution.py:23
  27.3 6.0 %collective-permute-start.23 = (bf16[64,1024]{1,0:T(8,128)(2,1)}, bf16[64,1024]{1,0:T(8,128)(2,1)S(1)}, u32[]{:S(2)}, u32[]{:S(2)}) collective-permute-start(bf16[64,1024]{1,0:T(8,128)(2,1)} %get-tuple-element.34), channel_id=1, source_target_pairs={{0,192},{32,224},{64,0},{96,32},{128,64},{160,96},{192,128},{224,1... | collective-permute-start | bytes 393224 | tf_op jit(solution)/shard_map/ppermute | solution.py:23
  33.3 1.4 pad_maximum_fusion
  34.7 1.9 %collective-permute-start.3 = (bf16[4,1024,256]{2,1,0:T(8,128)(2,1)S(1)}, bf16[4,1024,256]{2,1,0:T(8,128)(2,1)S(1)}, u32[]{:S(2)}, u32[]{:S(2)}) collective-permute-start(bf16[4,1024,256]{2,1,0:T(8,128)(2,1)S(1)} %pad_maximum_fusion), channel_id=1, source_target_pairs={{0,1},{1,0},{2,3},{3,2},{4,5},{5,4},{6,7},{7,6},{8,9},{9,8},{10,11... | collective-permute-start | bytes 6291464 | tf_op jit(solution)/shard_map/ppermute | solution.py:23
  36.6 1.2 collective-permute-start.10
  37.9 1.3 collective-permute-start.9
  40.0 1.9 %collective-permute-start.21 = (bf16[128,1024]{1,0:T(8,128)(2,1)S(1)}, bf16[128,1024]{1,0:T(8,128)(2,1)S(1)}, u32[]{:S(2)}, u32[]{:S(2)}) collective-permute-start(bf16[128,1024]{1,0:T(8,128)(2,1)S(1)} %copy-done.3), channel_id=1, source_target_pairs={{0,224},{32,0},{64,32},{96,64},{128,96},{160,128},{192,160},{224,1... | collective-permute-start | bytes 786440 | tf_op jit(solution)/shard_map/ppermute | solution.py:23
  42.0 1.1 collective-permute-done.10.m4
  43.1 1.5 collective-permute-start.7
  44.6 0.9 collective-permute-done.9.m3
  45.6 1.0 collective-permute-start.8
  46.6 9.2 %collective-permute-done.7.m1 = bf16[4,24,1024]{2,1,0:T(8,128)(2,1)S(1)} collective-permute-done((bf16[4,24,1024]{2,1,0:T(8,128)(2,1)S(1)}, bf16[4,24,1024]{2,1,0:T(8,128)(2,1)S(1)}, u32[]{:S(2)}, u32[]{:S(2)}) %collective-permute-start.7) | collective-permute-done | bytes 196640 | tf_op jit(solution)/shard_map/ppermute | solution.py:23
  56.2 1.2 collective-permute-start.11
  57.6 1.4 collective-permute-start.24
  59.0 0.9 collective-permute-start.16
  59.9 2.4 %collective-permute-start.17 = (bf16[528,256]{1,0:T(8,128)(2,1)S(1)}, bf16[528,256]{1,0:T(8,128)(2,1)S(1)}, u32[]{:S(2)}, u32[]{:S(2)}) collective-permute-start(bf16[528,256]{1,0:T(8,128)(2,1)S(1)} %get-tuple-element.27.refs_10_), channel_id=1, source_target_pairs={{0,6},{2,0},{4,2},{6,4},{1,7},{3,1},{5,3},{7,5},{8,14},{10,8},{12,... | collective-permute-start | bytes 811016 | tf_op jit(solution)/shard_map/ppermute | solution.py:23
  62.3 1.1 collective-permute-start.18
  63.5 1.5 collective-permute-start.25
  65.0 3.6 %shard_map.120 = (bf16[1024,128]{1,0:T(8,128)(2,1)S(1)}, bf16[512,128]{1,0:T(8,128)(2,1)S(1)}) custom-call(bf16[1024,256]{1,0:T(8,128)(2,1)S(1)} %bitcast.74, bf16[1024,256]{1,0:T(8,128)(2,1)S(1)} %collective-permute-done.refs_1_, bf16[1024,256]{1,0:T(8,128)(2,1)S(1)} %collective-permute-done.1.refs_2_, ...), custom_call_target="tpu_custom_call" | custom-call | flops 800000000 | bytes 5382144 | tf_op jit(solution)/shard_map/pallas_call | solution.py:54
  69.5 6.0 %collective-permute-done.18.refs_13_ = bf16[528,256]{1,0:T(8,128)(2,1)S(1)} collective-permute-done((bf16[528,256]{1,0:T(8,128)(2,1)S(1)}, bf16[528,256]{1,0:T(8,128)(2,1)S(1)}, u32[]{:S(2)}, u32[]{:S(2)}) %collective-permute-start.18) | collective-permute-done | bytes 270368 | tf_op jit(solution)/shard_map/ppermute | solution.py:23
  75.7 2.0 %collective-permute-start.19 = (bf16[4,528,256]{2,1,0:T(8,128)(2,1)S(1)}, bf16[4,528,256]{2,1,0:T(8,128)(2,1)S(1)}, u32[]{:S(2)}, u32[]{:S(2)}) collective-permute-start(bf16[4,528,256]{2,1,0:T(8,128)(2,1)S(1)} %pad_maximum_fusion.1), channel_id=1, source_target_pairs={{0,1},{1,0},{2,3},{3,2},{4,5},{5,4},{6,7},{7,6},{8,9},{9,8},{10,11... | collective-permute-start | bytes 3244040 | tf_op jit(solution)/shard_map/ppermute | solution.py:23
  79.7 3.0 %collective-permute-done.13.refs_7_ = bf16[512,128]{1,0:T(8,128)(2,1)S(1)} collective-permute-done((bf16[512,128]{1,0:T(8,128)(2,1)S(1)}, bf16[512,128]{1,0:T(8,128)(2,1)S(1)}, u32[]{:S(2)}, u32[]{:S(2)}) %collective-permute-start.13) | collective-permute-done | bytes 131104 | tf_op jit(solution)/shard_map/ppermute | solution.py:23
  82.7 2.4 %collective-permute-done.14.refs_8_ = bf16[512,128]{1,0:T(8,128)(2,1)S(1)} collective-permute-done((bf16[512,128]{1,0:T(8,128)(2,1)S(1)}, bf16[512,128]{1,0:T(8,128)(2,1)S(1)}, u32[]{:S(2)}, u32[]{:S(2)}) %collective-permute-start.14) | collective-permute-done | bytes 131104 | tf_op jit(solution)/shard_map/ppermute | solution.py:23
  85.8 1.7 %collective-permute-start.15 = (bf16[3,512,128]{2,1,0:T(8,128)(2,1)S(1)}, bf16[3,512,128]{2,1,0:T(8,128)(2,1)S(1)}, u32[]{:S(2)}, u32[]{:S(2)}) collective-permute-start(bf16[3,512,128]{2,1,0:T(8,128)(2,1)S(1)} %pad_maximum_fusion.6), channel_id=1, source_target_pairs={{0,1},{1,0},{2,3},{3,2},{4,5},{5,4},{6,7},{7,6},{8,9},{9,8},{10,11... | collective-permute-start | bytes 1179656 | tf_op jit(solution)/shard_map/ppermute | solution.py:23
  87.6 1.4 collective-permute-start.26
  89.0 18.1 %collective-permute-done.28.b1 = bf16[4,128,1024]{2,1,0:T(8,128)(2,1)S(1)} collective-permute-done((bf16[4,128,1024]{2,1,0:T(8,128)(2,1)S(1)}, bf16[4,128,1024]{2,1,0:T(8,128)(2,1)S(1)}, u32[]{:S(2)}, u32[]{:S(2)}) %collective-permute-start.28) | collective-permute-done | bytes 1048608 | tf_op jit(solution)/shard_map/ppermute | solution.py:23
  107.1 1.4 collective-permute-start.27
  108.9 2.7 %collective-permute-start.31 = (bf16[2,128,1024]{2,1,0:T(8,128)(2,1)S(1)}, bf16[2,128,1024]{2,1,0:T(8,128)(2,1)S(1)}, u32[]{:S(2)}, u32[]{:S(2)}) collective-permute-start(bf16[2,128,1024]{2,1,0:T(8,128)(2,1)S(1)} %slice.123), channel_id=1, source_target_pairs={{0,224},{32,0},{64,32},{96,64},{128,96},{160,128},{192,160},{224,1... | collective-permute-start | bytes 1572872 | tf_op jit(solution)/shard_map/ppermute | solution.py:23
  111.6 4.0 %shard_map.121 = (bf16[1024,2048]{1,0:T(8,128)(2,1)S(1)}, bf16[1024,256]{1,0:T(8,128)(2,1)S(1)}, f32[1024,128]{1,0:T(8,128)S(1)}) custom-call(bf16[1024,256]{1,0:T(8,128)(2,1)S(1)} %bitcast.75, bf16[1024,256]{1,0:T(8,128)(2,1)S(1)} %collective-permute-done.refs_1_, bf16[1024,256]{1,0:T(8,128)(2,1)S(1)} %collective-permute-done.1.refs_2_, ...), custom_call_target="tpu_custom_call" | custom-call | flops 2200000000 | bytes 7405568 | tf_op jit(solution)/shard_map/pallas_call | solution.py:54
  115.6 5.1 %shard_map.122.near = f32[1024,1024]{1,0:T(8,128)S(1)} custom-call(bf16[1024,2048]{1,0:T(8,128)(2,1)S(1)} %get-tuple-element.29.mixed, bf16[4,128,1024]{2,1,0:T(8,128)(2,1)S(1)} %pad_maximum_fusion.2.refs_0_, bf16[4,128,1024]{2,1,0:T(8,128)(2,1)S(1)} %collective-permute-done.24.refs_1_, bf16[4,128,1024]{2,1,0:T(8,128)(2,1)S(1)} %collective-permute-done.25.refs_2_), custom_call_target="tpu_custom_call" | custom-call | flops 3200000000 | bytes 7340032 | tf_op jit(solution)/shard_map/pallas_call | solution.py:54
  120.7 2.6 %shard_map.123.hidden = bf16[1024,1024]{1,0:T(8,128)(2,1)S(1)} custom-call(bf16[1024,2048]{1,0:T(8,128)(2,1)S(1)} %get-tuple-element.29.mixed, f32[1024,128]{1,0:T(8,128)S(1)} %get-tuple-element.30.factor, f32[1,1024]{1,0:T(1,128)S(1)} %get-tuple-element.31.s_up, f32[1024,1024]{1,0:T(8,128)S(1)} %shard_map.122.near, ...), custom_call_target="tpu_custom_call" | custom-call | flops 1100000000 | bytes 9965568 | tf_op jit(solution)/shard_map/pallas_call | solution.py:54
  123.3 3.4 %shard_map.125 = (bf16[2,1024,256]{2,1,0:T(8,128)(2,1)S(1)}, bf16[2,1024,256]{2,1,0:T(8,128)(2,1)S(1)}) custom-call(bf16[1024,1024]{1,0:T(8,128)(2,1)S(1)} %shard_map.123.hidden, bf16[4,128,1024]{2,1,0:T(8,128)(2,1)S(1)} %pad_maximum_fusion.3.b0, bf16[4,128,1024]{2,1,0:T(8,128)(2,1)S(1)} %collective-permute-done.28.b1, ...), custom_call_target="tpu_custom_call" | custom-call | flops 2150000128 | bytes 6291456 | tf_op jit(solution)/shard_map/pallas_call | solution.py:54
  126.7 3.3 %collective-permute-start.33 = (bf16[2,1024,256]{2,1,0:T(8,128)(2,1)S(1)}, bf16[2,1024,256]{2,1,0:T(8,128)(2,1)S(1)}, u32[]{:S(2)}, u32[]{:S(2)}) collective-permute-start(bf16[2,1024,256]{2,1,0:T(8,128)(2,1)S(1)} %get-tuple-element.38), channel_id=1, source_target_pairs={{0,1},{1,0},{2,3},{3,2},{4,5},{5,4},{6,7},{7,6},{8,9},{9,8},{10,11... | collective-permute-start | bytes 3145736 | tf_op jit(solution)/shard_map/ppermute | solution.py:23
  130.0 1.6 %shard_map.126 = (bf16[1,1024,256]{2,1,0:T(8,128)(2,1)S(1)}, bf16[1,1024,256]{2,1,0:T(8,128)(2,1)S(1)}) custom-call(bf16[1024,1024]{1,0:T(8,128)(2,1)S(1)} %shard_map.123.hidden, bf16[4,128,1024]{2,1,0:T(8,128)(2,1)S(1)} %pad_maximum_fusion.3.b0, bf16[4,128,1024]{2,1,0:T(8,128)(2,1)S(1)} %collective-permute-done.28.b1, ...), custom_call_target="tpu_custom_call" | custom-call | flops 1075000064 | bytes 6291456 | tf_op jit(solution)/shard_map/pallas_call | solution.py:54
  131.8 1.7 %shard_map.124 = (bf16[1,1024,256]{2,1,0:T(8,128)(2,1)S(1)}, bf16[1,1024,256]{2,1,0:T(8,128)(2,1)S(1)}) custom-call(bf16[1024,1024]{1,0:T(8,128)(2,1)S(1)} %shard_map.123.hidden, bf16[4,128,1024]{2,1,0:T(8,128)(2,1)S(1)} %pad_maximum_fusion.3.b0, bf16[4,128,1024]{2,1,0:T(8,128)(2,1)S(1)} %collective-permute-done.28.b1, ...), custom_call_target="tpu_custom_call" | custom-call | flops 1075000064 | bytes 6291456 | tf_op jit(solution)/shard_map/pallas_call | solution.py:54
  134.4 2.5 %collective-permute-start.37 = (bf16[512,256]{1,0:T(8,128)(2,1)S(1)}, bf16[512,256]{1,0:T(8,128)(2,1)S(1)}, u32[]{:S(2)}, u32[]{:S(2)}) collective-permute-start(bf16[512,256]{1,0:T(8,128)(2,1)S(1)} %get-tuple-element.44), channel_id=1, source_target_pairs={{0,6},{2,0},{4,2},{6,4},{1,7},{3,1},{5,3},{7,5},{8,14},{10,8},{12,... | collective-permute-start | bytes 786440 | tf_op jit(solution)/shard_map/ppermute | solution.py:23
  137.2 6.1 %collective-permute-done.35 = bf16[512,256]{1,0:T(8,128)(2,1)S(1)} collective-permute-done((bf16[512,256]{1,0:T(8,128)(2,1)S(1)}, bf16[512,256]{1,0:T(8,128)(2,1)S(1)}, u32[]{:S(2)}, u32[]{:S(2)}) %collective-permute-start.35) | collective-permute-done | bytes 262176 | tf_op jit(solution)/shard_map/ppermute | solution.py:23
  143.6 2.7 %collective-permute-start.38 = (bf16[1024,256]{1,0:T(8,128)(2,1)S(1)}, bf16[1024,256]{1,0:T(8,128)(2,1)S(1)}, u32[]{:S(2)}, u32[]{:S(2)}) collective-permute-start(bf16[1024,256]{1,0:T(8,128)(2,1)S(1)} %pad_maximum_fusion.5), channel_id=1, source_target_pairs={{0,6},{2,0},{4,2},{6,4},{1,7},{3,1},{5,3},{7,5},{8,14},{10,8},{12,... | collective-permute-start | bytes 1572872 | tf_op jit(solution)/shard_map/ppermute | solution.py:23
  146.4 10.9 %collective-permute-done.36 = bf16[1024,256]{1,0:T(8,128)(2,1)S(1)} collective-permute-done((bf16[1024,256]{1,0:T(8,128)(2,1)S(1)}, bf16[1024,256]{1,0:T(8,128)(2,1)S(1)}, u32[]{:S(2)}, u32[]{:S(2)}) %collective-permute-start.36) | collective-permute-done | bytes 524320 | tf_op jit(solution)/shard_map/ppermute | solution.py:23
  157.2 1.1 fusion.3
  (78 shorter events, 8.9 us)
Async XLA Ops:
  0.0 12.9 %collective-permute-start = (bf16[1024,256]{1,0:T(8,128)(2,1)}, bf16[1024,256]{1,0:T(8,128)(2,1)S(1)}, u32[]{:S(2)}, u32[]{:S(2)}) collective-permute-start(bf16[1024,256]{1,0:T(8,128)(2,1)} %bitcast.71), channel_id=1, source_target_pairs={{0,2},{2,4},{4,6},{6,0},{1,3},{3,5},{5,7},{7,1},{8,10},{10,12},{12... | collective-permute-start | bytes 1572872 | tf_op jit(solution)/shard_map/ppermute | solution.py:23
  2.0 15.8 %collective-permute-start.1 = (bf16[1024,256]{1,0:T(8,128)(2,1)}, bf16[1024,256]{1,0:T(8,128)(2,1)S(1)}, u32[]{:S(2)}, u32[]{:S(2)}) collective-permute-start(bf16[1024,256]{1,0:T(8,128)(2,1)} %bitcast.72), channel_id=1, source_target_pairs={{0,6},{2,0},{4,2},{6,4},{1,7},{3,1},{5,3},{7,5},{8,14},{10,8},{12,... | collective-permute-start | bytes 1572872 | tf_op jit(solution)/shard_map/ppermute | solution.py:23
  3.3 24.0 %collective-permute-start.2 = (bf16[1024,256]{1,0:T(8,128)(2,1)}, bf16[1024,256]{1,0:T(8,128)(2,1)S(1)}, u32[]{:S(2)}, u32[]{:S(2)}) collective-permute-start(bf16[1024,256]{1,0:T(8,128)(2,1)} %bitcast.73), channel_id=1, source_target_pairs={{0,4},{2,6},{4,0},{6,2},{1,5},{3,7},{5,1},{7,3},{8,12},{10,14},{12... | collective-permute-start | bytes 1572872 | tf_op jit(solution)/shard_map/ppermute | solution.py:23
  7.5 30.4 %collective-permute-start.4 = (bf16[152,1024]{1,0:T(8,128)(2,1)}, bf16[152,1024]{1,0:T(8,128)(2,1)S(1)}, u32[]{:S(2)}, u32[]{:S(2)}) collective-permute-start(bf16[152,1024]{1,0:T(8,128)(2,1)} %get-tuple-element.23), channel_id=1, source_target_pairs={{0,8},{8,16},{16,24},{24,0},{1,9},{9,17},{17,25},{25,1},{2,10},{10... | collective-permute-start | bytes 933896 | tf_op jit(solution)/shard_map/ppermute | solution.py:23
  8.8 25.8 %collective-permute-start.6 = (bf16[152,1024]{1,0:T(8,128)(2,1)}, bf16[152,1024]{1,0:T(8,128)(2,1)S(1)}, u32[]{:S(2)}, u32[]{:S(2)}) collective-permute-start(bf16[152,1024]{1,0:T(8,128)(2,1)} %get-tuple-element.23), channel_id=1, source_target_pairs={{0,16},{8,24},{16,0},{24,8},{1,17},{9,25},{17,1},{25,9},{2,18},{10... | collective-permute-start | bytes 933896 | tf_op jit(solution)/shard_map/ppermute | solution.py:23
  12.9 23.6 %collective-permute-start.5 = (bf16[152,1024]{1,0:T(8,128)(2,1)}, bf16[152,1024]{1,0:T(8,128)(2,1)S(1)}, u32[]{:S(2)}, u32[]{:S(2)}) collective-permute-start(bf16[152,1024]{1,0:T(8,128)(2,1)} %get-tuple-element.23), channel_id=1, source_target_pairs={{0,24},{8,0},{16,8},{24,16},{1,25},{9,1},{17,9},{25,17},{2,26},{10... | collective-permute-start | bytes 933896 | tf_op jit(solution)/shard_map/ppermute | solution.py:23
  17.8 21.4 %collective-permute-start.22 = (bf16[64,1024]{1,0:T(8,128)(2,1)}, bf16[64,1024]{1,0:T(8,128)(2,1)S(1)}, u32[]{:S(2)}, u32[]{:S(2)}) collective-permute-start(bf16[64,1024]{1,0:T(8,128)(2,1)} %get-tuple-element.33), channel_id=1, source_target_pairs={{0,64},{32,96},{64,128},{96,160},{128,192},{160,224},{192,0},{224,... | collective-permute-start | bytes 393224 | tf_op jit(solution)/shard_map/ppermute | solution.py:23
  27.3 12.8 %collective-permute-start.23 = (bf16[64,1024]{1,0:T(8,128)(2,1)}, bf16[64,1024]{1,0:T(8,128)(2,1)S(1)}, u32[]{:S(2)}, u32[]{:S(2)}) collective-permute-start(bf16[64,1024]{1,0:T(8,128)(2,1)} %get-tuple-element.34), channel_id=1, source_target_pairs={{0,192},{32,224},{64,0},{96,32},{128,64},{160,96},{192,128},{224,1... | collective-permute-start | bytes 393224 | tf_op jit(solution)/shard_map/ppermute | solution.py:23
  33.3 5.9 %copy-start.3 = (bf16[128,1024]{1,0:T(8,128)(2,1)S(1)}, bf16[128,1024]{1,0:T(8,128)(2,1)}, u32[]{:S(2)}) copy-start(bf16[128,1024]{1,0:T(8,128)(2,1)} %get-tuple-element.32) | copy-start | bytes 786436
  33.3 13.3 %copy-start.2 = (bf16[152,1024]{1,0:T(8,128)(2,1)S(1)}, bf16[152,1024]{1,0:T(8,128)(2,1)}, u32[]{:S(2)}) copy-start(bf16[152,1024]{1,0:T(8,128)(2,1)} %get-tuple-element.23) | copy-start | bytes 933892
  34.7 28.8 %collective-permute-start.3 = (bf16[4,1024,256]{2,1,0:T(8,128)(2,1)S(1)}, bf16[4,1024,256]{2,1,0:T(8,128)(2,1)S(1)}, u32[]{:S(2)}, u32[]{:S(2)}) collective-permute-start(bf16[4,1024,256]{2,1,0:T(8,128)(2,1)S(1)} %pad_maximum_fusion), channel_id=1, source_target_pairs={{0,1},{1,0},{2,3},{3,2},{4,5},{5,4},{6,7},{7,6},{8,9},{9,8},{10,11... | collective-permute-start | bytes 6291464 | tf_op jit(solution)/shard_map/ppermute | solution.py:23
  36.6 6.5 %collective-permute-start.10 = (bf16[2,24,1024]{2,1,0:T(8,128)(2,1)S(1)}, bf16[2,24,1024]{2,1,0:T(8,128)(2,1)S(1)}, u32[]{:S(2)}, u32[]{:S(2)}) collective-permute-start(bf16[2,24,1024]{2,1,0:T(8,128)(2,1)S(1)} %pad_maximum_fusion.9), channel_id=1, source_target_pairs={{0,192},{32,224},{64,0},{96,32},{128,64},{160,96},{192,128},{224,1... | collective-permute-start | bytes 294920 | tf_op jit(solution)/shard_map/ppermute | solution.py:23
  37.9 7.7 %collective-permute-start.9 = (bf16[2,24,1024]{2,1,0:T(8,128)(2,1)S(1)}, bf16[2,24,1024]{2,1,0:T(8,128)(2,1)S(1)}, u32[]{:S(2)}, u32[]{:S(2)}) collective-permute-start(bf16[2,24,1024]{2,1,0:T(8,128)(2,1)S(1)} %pad_maximum_fusion.8), channel_id=1, source_target_pairs={{0,64},{32,96},{64,128},{96,160},{128,192},{160,224},{192,0},{224,... | collective-permute-start | bytes 294920 | tf_op jit(solution)/shard_map/ppermute | solution.py:23
  39.2 18.2 %collective-permute-start.20 = (bf16[128,1024]{1,0:T(8,128)(2,1)S(1)}, bf16[128,1024]{1,0:T(8,128)(2,1)S(1)}, u32[]{:S(2)}, u32[]{:S(2)}) collective-permute-start(bf16[128,1024]{1,0:T(8,128)(2,1)S(1)} %copy-done.3), channel_id=1, source_target_pairs={{0,32},{32,64},{64,96},{96,128},{128,160},{160,192},{192,224},{224... | collective-permute-start | bytes 786440 | tf_op jit(solution)/shard_map/ppermute | solution.py:23
  40.0 17.4 %collective-permute-start.21 = (bf16[128,1024]{1,0:T(8,128)(2,1)S(1)}, bf16[128,1024]{1,0:T(8,128)(2,1)S(1)}, u32[]{:S(2)}, u32[]{:S(2)}) collective-permute-start(bf16[128,1024]{1,0:T(8,128)(2,1)S(1)} %copy-done.3), channel_id=1, source_target_pairs={{0,224},{32,0},{64,32},{96,64},{128,96},{160,128},{192,160},{224,1... | collective-permute-start | bytes 786440 | tf_op jit(solution)/shard_map/ppermute | solution.py:23
  43.1 12.8 %collective-permute-start.7 = (bf16[4,24,1024]{2,1,0:T(8,128)(2,1)S(1)}, bf16[4,24,1024]{2,1,0:T(8,128)(2,1)S(1)}, u32[]{:S(2)}, u32[]{:S(2)}) collective-permute-start(bf16[4,24,1024]{2,1,0:T(8,128)(2,1)S(1)} %pad_maximum_fusion.7.m0), channel_id=1, source_target_pairs={{0,32},{32,64},{64,96},{96,128},{128,160},{160,192},{192,224},{224... | collective-permute-start | bytes 589832 | tf_op jit(solution)/shard_map/ppermute | solution.py:23
  45.6 10.3 %collective-permute-start.8 = (bf16[4,24,1024]{2,1,0:T(8,128)(2,1)S(1)}, bf16[4,24,1024]{2,1,0:T(8,128)(2,1)S(1)}, u32[]{:S(2)}, u32[]{:S(2)}) collective-permute-start(bf16[4,24,1024]{2,1,0:T(8,128)(2,1)S(1)} %pad_maximum_fusion.7.m0), channel_id=1, source_target_pairs={{0,224},{32,0},{64,32},{96,64},{128,96},{160,128},{192,160},{224,1... | collective-permute-start | bytes 589832 | tf_op jit(solution)/shard_map/ppermute | solution.py:23
  46.6 18.4 %copy-start = (bf16[1,1024,256]{2,1,0:T(8,128)(2,1)S(1)}, bf16[1,1024,256]{2,1,0:T(8,128)(2,1)}, u32[]{:S(2)}) copy-start(bf16[1,1024,256]{2,1,0:T(8,128)(2,1)} %param.12) | copy-start | bytes 1572868
  46.6 18.4 %copy-start.1 = (bf16[4,128,128]{2,1,0:T(8,128)(2,1)S(1)}, bf16[4,128,128]{2,1,0:T(8,128)(2,1)}, u32[]{:S(2)}) copy-start(bf16[4,128,128]{2,1,0:T(8,128)(2,1)} %refs_7_.1) | copy-start | bytes 393220
  56.2 6.1 %collective-permute-start.11 = (bf16[2064,128]{1,0:T(8,128)(2,1)S(1)}, bf16[2064,128]{1,0:T(8,128)(2,1)S(1)}, u32[]{:S(2)}, u32[]{:S(2)}) collective-permute-start(bf16[2064,128]{1,0:T(8,128)(2,1)S(1)} %get-tuple-element.24.refs_5_), channel_id=1, source_target_pairs={{0,1},{1,0},{2,3},{3,2},{4,5},{5,4},{6,7},{7,6},{8,9},{9,8},{10,11... | collective-permute-start | bytes 1585160 | tf_op jit(solution)/shard_map/ppermute | solution.py:23
  57.6 28.2 %collective-permute-start.24 = (bf16[4,128,1024]{2,1,0:T(8,128)(2,1)S(1)}, bf16[4,128,1024]{2,1,0:T(8,128)(2,1)S(1)}, u32[]{:S(2)}, u32[]{:S(2)}) collective-permute-start(bf16[4,128,1024]{2,1,0:T(8,128)(2,1)S(1)} %pad_maximum_fusion.2.refs_0_), channel_id=1, source_target_pairs={{0,8},{8,16},{16,24},{24,0},{1,9},{9,17},{17,25},{25,1},{2,10},{10... | collective-permute-start | bytes 3145736 | tf_op jit(solution)/shard_map/ppermute | solution.py:23
  59.0 9.8 %collective-permute-start.16 = (bf16[528,256]{1,0:T(8,128)(2,1)S(1)}, bf16[528,256]{1,0:T(8,128)(2,1)S(1)}, u32[]{:S(2)}, u32[]{:S(2)}) collective-permute-start(bf16[528,256]{1,0:T(8,128)(2,1)S(1)} %get-tuple-element.27.refs_10_), channel_id=1, source_target_pairs={{0,2},{2,4},{4,6},{6,0},{1,3},{3,5},{5,7},{7,1},{8,10},{10,12},{12... | collective-permute-start | bytes 811016 | tf_op jit(solution)/shard_map/ppermute | solution.py:23
  59.9 9.6 %collective-permute-start.17 = (bf16[528,256]{1,0:T(8,128)(2,1)S(1)}, bf16[528,256]{1,0:T(8,128)(2,1)S(1)}, u32[]{:S(2)}, u32[]{:S(2)}) collective-permute-start(bf16[528,256]{1,0:T(8,128)(2,1)S(1)} %get-tuple-element.27.refs_10_), channel_id=1, source_target_pairs={{0,6},{2,0},{4,2},{6,4},{1,7},{3,1},{5,3},{7,5},{8,14},{10,8},{12,... | collective-permute-start | bytes 811016 | tf_op jit(solution)/shard_map/ppermute | solution.py:23
  62.3 13.2 %collective-permute-start.18 = (bf16[528,256]{1,0:T(8,128)(2,1)S(1)}, bf16[528,256]{1,0:T(8,128)(2,1)S(1)}, u32[]{:S(2)}, u32[]{:S(2)}) collective-permute-start(bf16[528,256]{1,0:T(8,128)(2,1)S(1)} %get-tuple-element.27.refs_10_), channel_id=1, source_target_pairs={{0,4},{2,6},{4,0},{6,2},{1,5},{3,7},{5,1},{7,3},{8,12},{10,14},{12... | collective-permute-start | bytes 811016 | tf_op jit(solution)/shard_map/ppermute | solution.py:23
  63.5 24.1 %collective-permute-start.25 = (bf16[4,128,1024]{2,1,0:T(8,128)(2,1)S(1)}, bf16[4,128,1024]{2,1,0:T(8,128)(2,1)S(1)}, u32[]{:S(2)}, u32[]{:S(2)}) collective-permute-start(bf16[4,128,1024]{2,1,0:T(8,128)(2,1)S(1)} %pad_maximum_fusion.2.refs_0_), channel_id=1, source_target_pairs={{0,24},{8,0},{16,8},{24,16},{1,25},{9,1},{17,9},{25,17},{2,26},{10... | collective-permute-start | bytes 3145736 | tf_op jit(solution)/shard_map/ppermute | solution.py:23
  68.8 10.2 %collective-permute-start.12 = (bf16[512,128]{1,0:T(8,128)(2,1)S(1)}, bf16[512,128]{1,0:T(8,128)(2,1)S(1)}, u32[]{:S(2)}, u32[]{:S(2)}) collective-permute-start(bf16[512,128]{1,0:T(8,128)(2,1)S(1)} %get-tuple-element.26), channel_id=1, source_target_pairs={{0,2},{2,4},{4,6},{6,0},{1,3},{3,5},{5,7},{7,1},{8,10},{10,12},{12... | collective-permute-start | bytes 393224 | tf_op jit(solution)/shard_map/ppermute | solution.py:23
  75.7 33.2 %collective-permute-start.19 = (bf16[4,528,256]{2,1,0:T(8,128)(2,1)S(1)}, bf16[4,528,256]{2,1,0:T(8,128)(2,1)S(1)}, u32[]{:S(2)}, u32[]{:S(2)}) collective-permute-start(bf16[4,528,256]{2,1,0:T(8,128)(2,1)S(1)} %pad_maximum_fusion.1), channel_id=1, source_target_pairs={{0,1},{1,0},{2,3},{3,2},{4,5},{5,4},{6,7},{7,6},{8,9},{9,8},{10,11... | collective-permute-start | bytes 3244040 | tf_op jit(solution)/shard_map/ppermute | solution.py:23
  77.7 5.0 %collective-permute-start.13 = (bf16[512,128]{1,0:T(8,128)(2,1)S(1)}, bf16[512,128]{1,0:T(8,128)(2,1)S(1)}, u32[]{:S(2)}, u32[]{:S(2)}) collective-permute-start(bf16[512,128]{1,0:T(8,128)(2,1)S(1)} %get-tuple-element.26), channel_id=1, source_target_pairs={{0,6},{2,0},{4,2},{6,4},{1,7},{3,1},{5,3},{7,5},{8,14},{10,8},{12,... | collective-permute-start | bytes 393224 | tf_op jit(solution)/shard_map/ppermute | solution.py:23
  79.0 6.1 %collective-permute-start.14 = (bf16[512,128]{1,0:T(8,128)(2,1)S(1)}, bf16[512,128]{1,0:T(8,128)(2,1)S(1)}, u32[]{:S(2)}, u32[]{:S(2)}) collective-permute-start(bf16[512,128]{1,0:T(8,128)(2,1)S(1)} %get-tuple-element.26), channel_id=1, source_target_pairs={{0,4},{2,6},{4,0},{6,2},{1,5},{3,7},{5,1},{7,3},{8,12},{10,14},{12... | collective-permute-start | bytes 393224 | tf_op jit(solution)/shard_map/ppermute | solution.py:23
  82.7 24.4 %collective-permute-start.28 = (bf16[4,128,1024]{2,1,0:T(8,128)(2,1)S(1)}, bf16[4,128,1024]{2,1,0:T(8,128)(2,1)S(1)}, u32[]{:S(2)}, u32[]{:S(2)}) collective-permute-start(bf16[4,128,1024]{2,1,0:T(8,128)(2,1)S(1)} %pad_maximum_fusion.3.b0), channel_id=1, source_target_pairs={{0,32},{32,64},{64,96},{96,128},{128,160},{160,192},{192,224},{224... | collective-permute-start | bytes 3145736 | tf_op jit(solution)/shard_map/ppermute | solution.py:23
  85.0 23.5 %collective-permute-start.29 = (bf16[4,128,1024]{2,1,0:T(8,128)(2,1)S(1)}, bf16[4,128,1024]{2,1,0:T(8,128)(2,1)S(1)}, u32[]{:S(2)}, u32[]{:S(2)}) collective-permute-start(bf16[4,128,1024]{2,1,0:T(8,128)(2,1)S(1)} %pad_maximum_fusion.3.b0), channel_id=1, source_target_pairs={{0,224},{32,0},{64,32},{96,64},{128,96},{160,128},{192,160},{224,1... | collective-permute-start | bytes 3145736 | tf_op jit(solution)/shard_map/ppermute | solution.py:23
  85.8 25.8 %collective-permute-start.15 = (bf16[3,512,128]{2,1,0:T(8,128)(2,1)S(1)}, bf16[3,512,128]{2,1,0:T(8,128)(2,1)S(1)}, u32[]{:S(2)}, u32[]{:S(2)}) collective-permute-start(bf16[3,512,128]{2,1,0:T(8,128)(2,1)S(1)} %pad_maximum_fusion.6), channel_id=1, source_target_pairs={{0,1},{1,0},{2,3},{3,2},{4,5},{5,4},{6,7},{7,6},{8,9},{9,8},{10,11... | collective-permute-start | bytes 1179656 | tf_op jit(solution)/shard_map/ppermute | solution.py:23
  87.6 33.1 %collective-permute-start.26 = (bf16[2,128,1024]{2,1,0:T(8,128)(2,1)S(1)}, bf16[2,128,1024]{2,1,0:T(8,128)(2,1)S(1)}, u32[]{:S(2)}, u32[]{:S(2)}) collective-permute-start(bf16[2,128,1024]{2,1,0:T(8,128)(2,1)S(1)} %slice.117), channel_id=1, source_target_pairs={{0,8},{8,16},{16,24},{24,0},{1,9},{9,17},{17,25},{25,1},{2,10},{10... | collective-permute-start | bytes 1572872 | tf_op jit(solution)/shard_map/ppermute | solution.py:23
  107.1 13.6 %collective-permute-start.27 = (bf16[2,128,1024]{2,1,0:T(8,128)(2,1)S(1)}, bf16[2,128,1024]{2,1,0:T(8,128)(2,1)S(1)}, u32[]{:S(2)}, u32[]{:S(2)}) collective-permute-start(bf16[2,128,1024]{2,1,0:T(8,128)(2,1)S(1)} %slice.118), channel_id=1, source_target_pairs={{0,24},{8,0},{16,8},{24,16},{1,25},{9,1},{17,9},{25,17},{2,26},{10... | collective-permute-start | bytes 1572872 | tf_op jit(solution)/shard_map/ppermute | solution.py:23
  108.5 14.8 %collective-permute-start.30 = (bf16[2,128,1024]{2,1,0:T(8,128)(2,1)S(1)}, bf16[2,128,1024]{2,1,0:T(8,128)(2,1)S(1)}, u32[]{:S(2)}, u32[]{:S(2)}) collective-permute-start(bf16[2,128,1024]{2,1,0:T(8,128)(2,1)S(1)} %slice.122), channel_id=1, source_target_pairs={{0,32},{32,64},{64,96},{96,128},{128,160},{160,192},{192,224},{224... | collective-permute-start | bytes 1572872 | tf_op jit(solution)/shard_map/ppermute | solution.py:23
  108.9 14.4 %collective-permute-start.31 = (bf16[2,128,1024]{2,1,0:T(8,128)(2,1)S(1)}, bf16[2,128,1024]{2,1,0:T(8,128)(2,1)S(1)}, u32[]{:S(2)}, u32[]{:S(2)}) collective-permute-start(bf16[2,128,1024]{2,1,0:T(8,128)(2,1)S(1)} %slice.123), channel_id=1, source_target_pairs={{0,224},{32,0},{64,32},{96,64},{128,96},{160,128},{192,160},{224,1... | collective-permute-start | bytes 1572872 | tf_op jit(solution)/shard_map/ppermute | solution.py:23
  126.7 10.2 %collective-permute-start.33 = (bf16[2,1024,256]{2,1,0:T(8,128)(2,1)S(1)}, bf16[2,1024,256]{2,1,0:T(8,128)(2,1)S(1)}, u32[]{:S(2)}, u32[]{:S(2)}) collective-permute-start(bf16[2,1024,256]{2,1,0:T(8,128)(2,1)S(1)} %get-tuple-element.38), channel_id=1, source_target_pairs={{0,1},{1,0},{2,3},{3,2},{4,5},{5,4},{6,7},{7,6},{8,9},{9,8},{10,11... | collective-permute-start | bytes 3145736 | tf_op jit(solution)/shard_map/ppermute | solution.py:23
  131.7 2.3 %collective-permute-start.34 = (bf16[1,1024,256]{2,1,0:T(8,128)(2,1)S(1)}, bf16[1,1024,256]{2,1,0:T(8,128)(2,1)S(1)}, u32[]{:S(2)}, u32[]{:S(2)}) collective-permute-start(bf16[1,1024,256]{2,1,0:T(8,128)(2,1)S(1)} %get-tuple-element.40), channel_id=1, source_target_pairs={{0,1},{1,0},{2,3},{3,2},{4,5},{5,4},{6,7},{7,6},{8,9},{9,8},{10,11... | collective-permute-start | bytes 1572872 | tf_op jit(solution)/shard_map/ppermute | solution.py:23
  133.5 12.9 %collective-permute-start.32 = (bf16[1,1024,256]{2,1,0:T(8,128)(2,1)S(1)}, bf16[1,1024,256]{2,1,0:T(8,128)(2,1)S(1)}, u32[]{:S(2)}, u32[]{:S(2)}) collective-permute-start(bf16[1,1024,256]{2,1,0:T(8,128)(2,1)S(1)} %get-tuple-element.36), channel_id=1, source_target_pairs={{0,1},{1,0},{2,3},{3,2},{4,5},{5,4},{6,7},{7,6},{8,9},{9,8},{10,11... | collective-permute-start | bytes 1572872 | tf_op jit(solution)/shard_map/ppermute | solution.py:23
  134.2 9.1 %collective-permute-start.35 = (bf16[512,256]{1,0:T(8,128)(2,1)S(1)}, bf16[512,256]{1,0:T(8,128)(2,1)S(1)}, u32[]{:S(2)}, u32[]{:S(2)}) collective-permute-start(bf16[512,256]{1,0:T(8,128)(2,1)S(1)} %get-tuple-element.43), channel_id=1, source_target_pairs={{0,2},{2,4},{4,6},{6,0},{1,3},{3,5},{5,7},{7,1},{8,10},{10,12},{12... | collective-permute-start | bytes 786440 | tf_op jit(solution)/shard_map/ppermute | solution.py:23
  134.4 9.1 %collective-permute-start.37 = (bf16[512,256]{1,0:T(8,128)(2,1)S(1)}, bf16[512,256]{1,0:T(8,128)(2,1)S(1)}, u32[]{:S(2)}, u32[]{:S(2)}) collective-permute-start(bf16[512,256]{1,0:T(8,128)(2,1)S(1)} %get-tuple-element.44), channel_id=1, source_target_pairs={{0,6},{2,0},{4,2},{6,4},{1,7},{3,1},{5,3},{7,5},{8,14},{10,8},{12,... | collective-permute-start | bytes 786440 | tf_op jit(solution)/shard_map/ppermute | solution.py:23
  143.4 13.9 %collective-permute-start.36 = (bf16[1024,256]{1,0:T(8,128)(2,1)S(1)}, bf16[1024,256]{1,0:T(8,128)(2,1)S(1)}, u32[]{:S(2)}, u32[]{:S(2)}) collective-permute-start(bf16[1024,256]{1,0:T(8,128)(2,1)S(1)} %pad_maximum_fusion.4), channel_id=1, source_target_pairs={{0,2},{2,4},{4,6},{6,0},{1,3},{3,5},{5,7},{7,1},{8,10},{10,12},{12... | collective-permute-start | bytes 1572872 | tf_op jit(solution)/shard_map/ppermute | solution.py:23
  143.6 13.6 %collective-permute-start.38 = (bf16[1024,256]{1,0:T(8,128)(2,1)S(1)}, bf16[1024,256]{1,0:T(8,128)(2,1)S(1)}, u32[]{:S(2)}, u32[]{:S(2)}) collective-permute-start(bf16[1024,256]{1,0:T(8,128)(2,1)S(1)} %pad_maximum_fusion.5), channel_id=1, source_target_pairs={{0,6},{2,0},{4,2},{6,4},{1,7},{3,1},{5,3},{7,5},{8,14},{10,8},{12,... | collective-permute-start | bytes 1572872 | tf_op jit(solution)/shard_map/ppermute | solution.py:23

commit v4 on v3

--- a/solution.py
+++ b/solution.py
@@ -212,14 +212,13 @@
     chips, whose = around(lax.axis_index("x")), owners()
     c = lax.axis_index("c")
 
-    @pl.loop(0, 4)
+    @pl.loop(0, 2)
     def _(block):
-        rows = pl.ds(pl.multiple_of(block * 256, 256), 256)
-        inner = pl.ds(pl.multiple_of(lax.rem(block, 2) * 256, 256), 256)
-        squares = jnp.zeros((256, 128), F32)
+        rows = pl.ds(pl.multiple_of(block * 512, 512), 512)
+        squares = jnp.zeros((512, 128), F32)
         left = jnp.concatenate(
             [grouped[rows, :]] + [
-                jnp.where(lax.div(block, 2) == c, a[inner, :], across[k, inner, :])
+                jnp.where(block == c, a[...], across[k])
                 for k, a in enumerate(near)
             ],
             axis=1,
@@ -238,7 +237,7 @@
             wide = wide * wide
             squares += wide[:, :128] + wide[:, 128:]
         mean = jnp.sum(squares, axis=1, keepdims=True) / 2048
-        factor[rows, :] = jnp.broadcast_to(lax.rsqrt(mean + EPS), (256, 128))
+        factor[rows, :] = jnp.broadcast_to(lax.rsqrt(mean + EPS), (512, 128))
 
 
 def up_parts_sum(mixed, parts, ys, rows, cols, total):

time: 159 us -> 159 us (level)
  no operation moved by 1% of the time
where the time goes in v4:
time: 159 us; the launch traced here: 158 us
  waiting for transfers between devices  65.5 us (41%)
  starting transfers between devices  63 us (40%)
  Pallas kernels  24.2 us (15%)
  other arithmetic  3.54 us (2%)
    ppermute x39, waiting for transfers between devices, send(): lax.ppermute(array, axes, [(i, (i + shift) % count) for i in range(count)])  65.5 us
    ppermute x39, starting transfers between devices, send(): lax.ppermute(array, axes, [(i, (i + shift) % count) for i in range(count)])  63 us
    pallas_call x9, Pallas kernels, call(): pl.pallas_call(kernel, out_shape=out_shape, in_specs=[VMEM] * (len(args)...  24.2 us
  transfers between devices with their start and end apart: 39, of which 13 were waited for; matrix products, arithmetic and copies ran while one was open for 2% of the time, Pallas kernels for 13%

profile of v4, /device:TPU:1, one launch (start us, length us, event | category | flops | bytes accessed | tf_op | source)
XLA Modules:
  0.0 157.8 jit_solution(5203444008212813611)
XLA Ops:
  0.0 2.0 %collective-permute-start = (bf16[1024,256]{1,0:T(8,128)(2,1)}, bf16[1024,256]{1,0:T(8,128)(2,1)S(1)}, u32[]{:S(2)}, u32[]{:S(2)}) collective-permute-start(bf16[1024,256]{1,0:T(8,128)(2,1)} %bitcast.71), channel_id=1, source_target_pairs={{0,2},{2,4},{4,6},{6,0},{1,3},{3,5},{5,7},{7,1},{8,10},{10,12},{12... | collective-permute-start | bytes 1572872 | tf_op jit(solution)/shard_map/ppermute | solution.py:23
  2.0 1.3 collective-permute-start.1
  3.3 1.7 %collective-permute-start.2 = (bf16[1024,256]{1,0:T(8,128)(2,1)}, bf16[1024,256]{1,0:T(8,128)(2,1)S(1)}, u32[]{:S(2)}, u32[]{:S(2)}) collective-permute-start(bf16[1024,256]{1,0:T(8,128)(2,1)} %bitcast.73), channel_id=1, source_target_pairs={{0,4},{2,6},{4,0},{6,2},{1,5},{3,7},{5,1},{7,3},{8,12},{10,14},{12... | collective-permute-start | bytes 1572872 | tf_op jit(solution)/shard_map/ppermute | solution.py:23
  5.0 2.4 %shard_map.118 = (bf16[152,1024]{1,0:T(8,128)(2,1)}, bf16[128,1024]{1,0:T(8,128)(2,1)}, bf16[64,1024]{1,0:T(8,128)(2,1)}, bf16[64,1024]{1,0:T(8,128)(2,1)}) custom-call(f32[16,128]{1,0:T(8,128)} %bitcast.90, f32[64,128]{1,0:T(8,128)} %bitcast.89, f32[1,4]{1,0:T(1,128)} %bitcast.92, f32[32,256]{1,0:T(8,128)} %w_out_at.1, f32[1,16]{1,0:T(1,128)} %bitcast.93, ...), custom_call_target="tpu_custom_call" | custom-call | flops 1000000 | bytes 1131344 | tf_op jit(solution)/shard_map/pallas_call | solution.py:54
  7.5 1.4 collective-permute-start.4
  8.8 2.6 %collective-permute-start.6 = (bf16[152,1024]{1,0:T(8,128)(2,1)}, bf16[152,1024]{1,0:T(8,128)(2,1)S(1)}, u32[]{:S(2)}, u32[]{:S(2)}) collective-permute-start(bf16[152,1024]{1,0:T(8,128)(2,1)} %get-tuple-element.23), channel_id=1, source_target_pairs={{0,16},{8,24},{16,0},{24,8},{1,17},{9,25},{17,1},{25,9},{2,18},{10... | collective-permute-start | bytes 933896 | tf_op jit(solution)/shard_map/ppermute | solution.py:23
  12.9 4.8 %collective-permute-start.5 = (bf16[152,1024]{1,0:T(8,128)(2,1)}, bf16[152,1024]{1,0:T(8,128)(2,1)S(1)}, u32[]{:S(2)}, u32[]{:S(2)}) collective-permute-start(bf16[152,1024]{1,0:T(8,128)(2,1)} %get-tuple-element.23), channel_id=1, source_target_pairs={{0,24},{8,0},{16,8},{24,16},{1,25},{9,1},{17,9},{25,17},{2,26},{10... | collective-permute-start | bytes 933896 | tf_op jit(solution)/shard_map/ppermute | solution.py:23
  17.8 3.0 %collective-permute-start.22 = (bf16[64,1024]{1,0:T(8,128)(2,1)}, bf16[64,1024]{1,0:T(8,128)(2,1)S(1)}, u32[]{:S(2)}, u32[]{:S(2)}) collective-permute-start(bf16[64,1024]{1,0:T(8,128)(2,1)} %get-tuple-element.33), channel_id=1, source_target_pairs={{0,64},{32,96},{64,128},{96,160},{128,192},{160,224},{192,0},{224,... | collective-permute-start | bytes 393224 | tf_op jit(solution)/shard_map/ppermute | solution.py:23
  20.8 6.5 %collective-permute-done.2.refs_3_ = bf16[1024,256]{1,0:T(8,128)(2,1)S(1)} collective-permute-done((bf16[1024,256]{1,0:T(8,128)(2,1)}, bf16[1024,256]{1,0:T(8,128)(2,1)S(1)}, u32[]{:S(2)}, u32[]{:S(2)}) %collective-permute-start.2) | collective-permute-done | bytes 524320 | tf_op jit(solution)/shard_map/ppermute | solution.py:23
  27.3 6.0 %collective-permute-start.23 = (bf16[64,1024]{1,0:T(8,128)(2,1)}, bf16[64,1024]{1,0:T(8,128)(2,1)S(1)}, u32[]{:S(2)}, u32[]{:S(2)}) collective-permute-start(bf16[64,1024]{1,0:T(8,128)(2,1)} %get-tuple-element.34), channel_id=1, source_target_pairs={{0,192},{32,224},{64,0},{96,32},{128,64},{160,96},{192,128},{224,1... | collective-permute-start | bytes 393224 | tf_op jit(solution)/shard_map/ppermute | solution.py:23
  33.3 1.4 pad_maximum_fusion
  34.7 1.9 %collective-permute-start.3 = (bf16[4,1024,256]{2,1,0:T(8,128)(2,1)S(1)}, bf16[4,1024,256]{2,1,0:T(8,128)(2,1)S(1)}, u32[]{:S(2)}, u32[]{:S(2)}) collective-permute-start(bf16[4,1024,256]{2,1,0:T(8,128)(2,1)S(1)} %pad_maximum_fusion), channel_id=1, source_target_pairs={{0,1},{1,0},{2,3},{3,2},{4,5},{5,4},{6,7},{7,6},{8,9},{9,8},{10,11... | collective-permute-start | bytes 6291464 | tf_op jit(solution)/shard_map/ppermute | solution.py:23
  36.6 1.2 collective-permute-start.10
  37.9 1.3 collective-permute-start.9
  40.0 1.9 %collective-permute-start.21 = (bf16[128,1024]{1,0:T(8,128)(2,1)S(1)}, bf16[128,1024]{1,0:T(8,128)(2,1)S(1)}, u32[]{:S(2)}, u32[]{:S(2)}) collective-permute-start(bf16[128,1024]{1,0:T(8,128)(2,1)S(1)} %copy-done.3), channel_id=1, source_target_pairs={{0,224},{32,0},{64,32},{96,64},{128,96},{160,128},{192,160},{224,1... | collective-permute-start | bytes 786440 | tf_op jit(solution)/shard_map/ppermute | solution.py:23
  42.0 1.1 collective-permute-done.10.m4
  43.1 1.5 collective-permute-start.7
  44.6 0.9 collective-permute-done.9.m3
  45.6 1.0 collective-permute-start.8
  46.6 9.2 %collective-permute-done.7.m1 = bf16[4,24,1024]{2,1,0:T(8,128)(2,1)S(1)} collective-permute-done((bf16[4,24,1024]{2,1,0:T(8,128)(2,1)S(1)}, bf16[4,24,1024]{2,1,0:T(8,128)(2,1)S(1)}, u32[]{:S(2)}, u32[]{:S(2)}) %collective-permute-start.7) | collective-permute-done | bytes 196640 | tf_op jit(solution)/shard_map/ppermute | solution.py:23
  56.2 1.2 collective-permute-start.11
  57.6 1.4 collective-permute-start.24
  59.0 0.9 collective-permute-start.16
  59.9 2.4 %collective-permute-start.17 = (bf16[528,256]{1,0:T(8,128)(2,1)S(1)}, bf16[528,256]{1,0:T(8,128)(2,1)S(1)}, u32[]{:S(2)}, u32[]{:S(2)}) collective-permute-start(bf16[528,256]{1,0:T(8,128)(2,1)S(1)} %get-tuple-element.27.refs_10_), channel_id=1, source_target_pairs={{0,6},{2,0},{4,2},{6,4},{1,7},{3,1},{5,3},{7,5},{8,14},{10,8},{12,... | collective-permute-start | bytes 811016 | tf_op jit(solution)/shard_map/ppermute | solution.py:23
  62.3 1.1 collective-permute-start.18
  63.5 1.5 collective-permute-start.25
  65.0 3.6 %shard_map.120 = (bf16[1024,128]{1,0:T(8,128)(2,1)S(1)}, bf16[512,128]{1,0:T(8,128)(2,1)S(1)}) custom-call(bf16[1024,256]{1,0:T(8,128)(2,1)S(1)} %bitcast.74, bf16[1024,256]{1,0:T(8,128)(2,1)S(1)} %collective-permute-done.refs_1_, bf16[1024,256]{1,0:T(8,128)(2,1)S(1)} %collective-permute-done.1.refs_2_, ...), custom_call_target="tpu_custom_call" | custom-call | flops 800000000 | bytes 5382144 | tf_op jit(solution)/shard_map/pallas_call | solution.py:54
  69.5 6.0 %collective-permute-done.18.refs_13_ = bf16[528,256]{1,0:T(8,128)(2,1)S(1)} collective-permute-done((bf16[528,256]{1,0:T(8,128)(2,1)S(1)}, bf16[528,256]{1,0:T(8,128)(2,1)S(1)}, u32[]{:S(2)}, u32[]{:S(2)}) %collective-permute-start.18) | collective-permute-done | bytes 270368 | tf_op jit(solution)/shard_map/ppermute | solution.py:23
  75.7 2.0 %collective-permute-start.19 = (bf16[4,528,256]{2,1,0:T(8,128)(2,1)S(1)}, bf16[4,528,256]{2,1,0:T(8,128)(2,1)S(1)}, u32[]{:S(2)}, u32[]{:S(2)}) collective-permute-start(bf16[4,528,256]{2,1,0:T(8,128)(2,1)S(1)} %pad_maximum_fusion.1), channel_id=1, source_target_pairs={{0,1},{1,0},{2,3},{3,2},{4,5},{5,4},{6,7},{7,6},{8,9},{9,8},{10,11... | collective-permute-start | bytes 3244040 | tf_op jit(solution)/shard_map/ppermute | solution.py:23
  79.7 3.0 %collective-permute-done.13.refs_7_ = bf16[512,128]{1,0:T(8,128)(2,1)S(1)} collective-permute-done((bf16[512,128]{1,0:T(8,128)(2,1)S(1)}, bf16[512,128]{1,0:T(8,128)(2,1)S(1)}, u32[]{:S(2)}, u32[]{:S(2)}) %collective-permute-start.13) | collective-permute-done | bytes 131104 | tf_op jit(solution)/shard_map/ppermute | solution.py:23
  82.7 2.4 %collective-permute-done.14.refs_8_ = bf16[512,128]{1,0:T(8,128)(2,1)S(1)} collective-permute-done((bf16[512,128]{1,0:T(8,128)(2,1)S(1)}, bf16[512,128]{1,0:T(8,128)(2,1)S(1)}, u32[]{:S(2)}, u32[]{:S(2)}) %collective-permute-start.14) | collective-permute-done | bytes 131104 | tf_op jit(solution)/shard_map/ppermute | solution.py:23
  85.8 1.7 %collective-permute-start.15 = (bf16[3,512,128]{2,1,0:T(8,128)(2,1)S(1)}, bf16[3,512,128]{2,1,0:T(8,128)(2,1)S(1)}, u32[]{:S(2)}, u32[]{:S(2)}) collective-permute-start(bf16[3,512,128]{2,1,0:T(8,128)(2,1)S(1)} %pad_maximum_fusion.6), channel_id=1, source_target_pairs={{0,1},{1,0},{2,3},{3,2},{4,5},{5,4},{6,7},{7,6},{8,9},{9,8},{10,11... | collective-permute-start | bytes 1179656 | tf_op jit(solution)/shard_map/ppermute | solution.py:23
  87.6 1.4 collective-permute-start.26
  89.0 18.1 %collective-permute-done.28.b1 = bf16[4,128,1024]{2,1,0:T(8,128)(2,1)S(1)} collective-permute-done((bf16[4,128,1024]{2,1,0:T(8,128)(2,1)S(1)}, bf16[4,128,1024]{2,1,0:T(8,128)(2,1)S(1)}, u32[]{:S(2)}, u32[]{:S(2)}) %collective-permute-start.28) | collective-permute-done | bytes 1048608 | tf_op jit(solution)/shard_map/ppermute | solution.py:23
  107.1 1.4 collective-permute-start.27
  108.9 2.7 %collective-permute-start.31 = (bf16[2,128,1024]{2,1,0:T(8,128)(2,1)S(1)}, bf16[2,128,1024]{2,1,0:T(8,128)(2,1)S(1)}, u32[]{:S(2)}, u32[]{:S(2)}) collective-permute-start(bf16[2,128,1024]{2,1,0:T(8,128)(2,1)S(1)} %slice.123), channel_id=1, source_target_pairs={{0,224},{32,0},{64,32},{96,64},{128,96},{160,128},{192,160},{224,1... | collective-permute-start | bytes 1572872 | tf_op jit(solution)/shard_map/ppermute | solution.py:23
  111.6 3.5 %shard_map.121 = (bf16[1024,2048]{1,0:T(8,128)(2,1)S(1)}, bf16[1024,256]{1,0:T(8,128)(2,1)S(1)}, f32[1024,128]{1,0:T(8,128)S(1)}) custom-call(bf16[1024,256]{1,0:T(8,128)(2,1)S(1)} %bitcast.75, bf16[1024,256]{1,0:T(8,128)(2,1)S(1)} %collective-permute-done.refs_1_, bf16[1024,256]{1,0:T(8,128)(2,1)S(1)} %collective-permute-done.1.refs_2_, ...), custom_call_target="tpu_custom_call" | custom-call | flops 2200000000 | bytes 7405568 | tf_op jit(solution)/shard_map/pallas_call | solution.py:54
  115.1 5.1 %shard_map.122.near = f32[1024,1024]{1,0:T(8,128)S(1)} custom-call(bf16[1024,2048]{1,0:T(8,128)(2,1)S(1)} %get-tuple-element.29.mixed, bf16[4,128,1024]{2,1,0:T(8,128)(2,1)S(1)} %pad_maximum_fusion.2.refs_0_, bf16[4,128,1024]{2,1,0:T(8,128)(2,1)S(1)} %collective-permute-done.24.refs_1_, bf16[4,128,1024]{2,1,0:T(8,128)(2,1)S(1)} %collective-permute-done.25.refs_2_), custom_call_target="tpu_custom_call" | custom-call | flops 3200000000 | bytes 7340032 | tf_op jit(solution)/shard_map/pallas_call | solution.py:54
  120.2 2.6 %shard_map.123.hidden = bf16[1024,1024]{1,0:T(8,128)(2,1)S(1)} custom-call(bf16[1024,2048]{1,0:T(8,128)(2,1)S(1)} %get-tuple-element.29.mixed, f32[1024,128]{1,0:T(8,128)S(1)} %get-tuple-element.30.factor, f32[1,1024]{1,0:T(1,128)S(1)} %get-tuple-element.31.s_up, f32[1024,1024]{1,0:T(8,128)S(1)} %shard_map.122.near, ...), custom_call_target="tpu_custom_call" | custom-call | flops 1100000000 | bytes 9965568 | tf_op jit(solution)/shard_map/pallas_call | solution.py:54
  122.8 3.4 %shard_map.125 = (bf16[2,1024,256]{2,1,0:T(8,128)(2,1)S(1)}, bf16[2,1024,256]{2,1,0:T(8,128)(2,1)S(1)}) custom-call(bf16[1024,1024]{1,0:T(8,128)(2,1)S(1)} %shard_map.123.hidden, bf16[4,128,1024]{2,1,0:T(8,128)(2,1)S(1)} %pad_maximum_fusion.3.b0, bf16[4,128,1024]{2,1,0:T(8,128)(2,1)S(1)} %collective-permute-done.28.b1, ...), custom_call_target="tpu_custom_call" | custom-call | flops 2150000128 | bytes 6291456 | tf_op jit(solution)/shard_map/pallas_call | solution.py:54
  126.2 3.3 %collective-permute-start.33 = (bf16[2,1024,256]{2,1,0:T(8,128)(2,1)S(1)}, bf16[2,1024,256]{2,1,0:T(8,128)(2,1)S(1)}, u32[]{:S(2)}, u32[]{:S(2)}) collective-permute-start(bf16[2,1024,256]{2,1,0:T(8,128)(2,1)S(1)} %get-tuple-element.38), channel_id=1, source_target_pairs={{0,1},{1,0},{2,3},{3,2},{4,5},{5,4},{6,7},{7,6},{8,9},{9,8},{10,11... | collective-permute-start | bytes 3145736 | tf_op jit(solution)/shard_map/ppermute | solution.py:23
  129.5 1.6 %shard_map.126 = (bf16[1,1024,256]{2,1,0:T(8,128)(2,1)S(1)}, bf16[1,1024,256]{2,1,0:T(8,128)(2,1)S(1)}) custom-call(bf16[1024,1024]{1,0:T(8,128)(2,1)S(1)} %shard_map.123.hidden, bf16[4,128,1024]{2,1,0:T(8,128)(2,1)S(1)} %pad_maximum_fusion.3.b0, bf16[4,128,1024]{2,1,0:T(8,128)(2,1)S(1)} %collective-permute-done.28.b1, ...), custom_call_target="tpu_custom_call" | custom-call | flops 1075000064 | bytes 6291456 | tf_op jit(solution)/shard_map/pallas_call | solution.py:54
  131.3 1.7 %shard_map.124 = (bf16[1,1024,256]{2,1,0:T(8,128)(2,1)S(1)}, bf16[1,1024,256]{2,1,0:T(8,128)(2,1)S(1)}) custom-call(bf16[1024,1024]{1,0:T(8,128)(2,1)S(1)} %shard_map.123.hidden, bf16[4,128,1024]{2,1,0:T(8,128)(2,1)S(1)} %pad_maximum_fusion.3.b0, bf16[4,128,1024]{2,1,0:T(8,128)(2,1)S(1)} %collective-permute-done.28.b1, ...), custom_call_target="tpu_custom_call" | custom-call | flops 1075000064 | bytes 6291456 | tf_op jit(solution)/shard_map/pallas_call | solution.py:54
  133.9 2.5 %collective-permute-start.37 = (bf16[512,256]{1,0:T(8,128)(2,1)S(1)}, bf16[512,256]{1,0:T(8,128)(2,1)S(1)}, u32[]{:S(2)}, u32[]{:S(2)}) collective-permute-start(bf16[512,256]{1,0:T(8,128)(2,1)S(1)} %get-tuple-element.44), channel_id=1, source_target_pairs={{0,6},{2,0},{4,2},{6,4},{1,7},{3,1},{5,3},{7,5},{8,14},{10,8},{12,... | collective-permute-start | bytes 786440 | tf_op jit(solution)/shard_map/ppermute | solution.py:23
  136.7 6.1 %collective-permute-done.35 = bf16[512,256]{1,0:T(8,128)(2,1)S(1)} collective-permute-done((bf16[512,256]{1,0:T(8,128)(2,1)S(1)}, bf16[512,256]{1,0:T(8,128)(2,1)S(1)}, u32[]{:S(2)}, u32[]{:S(2)}) %collective-permute-start.35) | collective-permute-done | bytes 262176 | tf_op jit(solution)/shard_map/ppermute | solution.py:23
  143.1 2.7 %collective-permute-start.38 = (bf16[1024,256]{1,0:T(8,128)(2,1)S(1)}, bf16[1024,256]{1,0:T(8,128)(2,1)S(1)}, u32[]{:S(2)}, u32[]{:S(2)}) collective-permute-start(bf16[1024,256]{1,0:T(8,128)(2,1)S(1)} %pad_maximum_fusion.5), channel_id=1, source_target_pairs={{0,6},{2,0},{4,2},{6,4},{1,7},{3,1},{5,3},{7,5},{8,14},{10,8},{12,... | collective-permute-start | bytes 1572872 | tf_op jit(solution)/shard_map/ppermute | solution.py:23
  145.8 10.9 %collective-permute-done.36 = bf16[1024,256]{1,0:T(8,128)(2,1)S(1)} collective-permute-done((bf16[1024,256]{1,0:T(8,128)(2,1)S(1)}, bf16[1024,256]{1,0:T(8,128)(2,1)S(1)}, u32[]{:S(2)}, u32[]{:S(2)}) %collective-permute-start.36) | collective-permute-done | bytes 524320 | tf_op jit(solution)/shard_map/ppermute | solution.py:23
  156.7 1.1 fusion.3
  (78 shorter events, 8.9 us)
Async XLA Ops:
  0.0 12.9 %collective-permute-start = (bf16[1024,256]{1,0:T(8,128)(2,1)}, bf16[1024,256]{1,0:T(8,128)(2,1)S(1)}, u32[]{:S(2)}, u32[]{:S(2)}) collective-permute-start(bf16[1024,256]{1,0:T(8,128)(2,1)} %bitcast.71), channel_id=1, source_target_pairs={{0,2},{2,4},{4,6},{6,0},{1,3},{3,5},{5,7},{7,1},{8,10},{10,12},{12... | collective-permute-start | bytes 1572872 | tf_op jit(solution)/shard_map/ppermute | solution.py:23
  2.0 15.8 %collective-permute-start.1 = (bf16[1024,256]{1,0:T(8,128)(2,1)}, bf16[1024,256]{1,0:T(8,128)(2,1)S(1)}, u32[]{:S(2)}, u32[]{:S(2)}) collective-permute-start(bf16[1024,256]{1,0:T(8,128)(2,1)} %bitcast.72), channel_id=1, source_target_pairs={{0,6},{2,0},{4,2},{6,4},{1,7},{3,1},{5,3},{7,5},{8,14},{10,8},{12,... | collective-permute-start | bytes 1572872 | tf_op jit(solution)/shard_map/ppermute | solution.py:23
  3.3 24.0 %collective-permute-start.2 = (bf16[1024,256]{1,0:T(8,128)(2,1)}, bf16[1024,256]{1,0:T(8,128)(2,1)S(1)}, u32[]{:S(2)}, u32[]{:S(2)}) collective-permute-start(bf16[1024,256]{1,0:T(8,128)(2,1)} %bitcast.73), channel_id=1, source_target_pairs={{0,4},{2,6},{4,0},{6,2},{1,5},{3,7},{5,1},{7,3},{8,12},{10,14},{12... | collective-permute-start | bytes 1572872 | tf_op jit(solution)/shard_map/ppermute | solution.py:23
  7.5 30.4 %collective-permute-start.4 = (bf16[152,1024]{1,0:T(8,128)(2,1)}, bf16[152,1024]{1,0:T(8,128)(2,1)S(1)}, u32[]{:S(2)}, u32[]{:S(2)}) collective-permute-start(bf16[152,1024]{1,0:T(8,128)(2,1)} %get-tuple-element.23), channel_id=1, source_target_pairs={{0,8},{8,16},{16,24},{24,0},{1,9},{9,17},{17,25},{25,1},{2,10},{10... | collective-permute-start | bytes 933896 | tf_op jit(solution)/shard_map/ppermute | solution.py:23
  8.8 25.8 %collective-permute-start.6 = (bf16[152,1024]{1,0:T(8,128)(2,1)}, bf16[152,1024]{1,0:T(8,128)(2,1)S(1)}, u32[]{:S(2)}, u32[]{:S(2)}) collective-permute-start(bf16[152,1024]{1,0:T(8,128)(2,1)} %get-tuple-element.23), channel_id=1, source_target_pairs={{0,16},{8,24},{16,0},{24,8},{1,17},{9,25},{17,1},{25,9},{2,18},{10... | collective-permute-start | bytes 933896 | tf_op jit(solution)/shard_map/ppermute | solution.py:23
  12.9 23.6 %collective-permute-start.5 = (bf16[152,1024]{1,0:T(8,128)(2,1)}, bf16[152,1024]{1,0:T(8,128)(2,1)S(1)}, u32[]{:S(2)}, u32[]{:S(2)}) collective-permute-start(bf16[152,1024]{1,0:T(8,128)(2,1)} %get-tuple-element.23), channel_id=1, source_target_pairs={{0,24},{8,0},{16,8},{24,16},{1,25},{9,1},{17,9},{25,17},{2,26},{10... | collective-permute-start | bytes 933896 | tf_op jit(solution)/shard_map/ppermute | solution.py:23
  17.8 21.4 %collective-permute-start.22 = (bf16[64,1024]{1,0:T(8,128)(2,1)}, bf16[64,1024]{1,0:T(8,128)(2,1)S(1)}, u32[]{:S(2)}, u32[]{:S(2)}) collective-permute-start(bf16[64,1024]{1,0:T(8,128)(2,1)} %get-tuple-element.33), channel_id=1, source_target_pairs={{0,64},{32,96},{64,128},{96,160},{128,192},{160,224},{192,0},{224,... | collective-permute-start | bytes 393224 | tf_op jit(solution)/shard_map/ppermute | solution.py:23
  27.3 12.8 %collective-permute-start.23 = (bf16[64,1024]{1,0:T(8,128)(2,1)}, bf16[64,1024]{1,0:T(8,128)(2,1)S(1)}, u32[]{:S(2)}, u32[]{:S(2)}) collective-permute-start(bf16[64,1024]{1,0:T(8,128)(2,1)} %get-tuple-element.34), channel_id=1, source_target_pairs={{0,192},{32,224},{64,0},{96,32},{128,64},{160,96},{192,128},{224,1... | collective-permute-start | bytes 393224 | tf_op jit(solution)/shard_map/ppermute | solution.py:23
  33.3 5.9 %copy-start.3 = (bf16[128,1024]{1,0:T(8,128)(2,1)S(1)}, bf16[128,1024]{1,0:T(8,128)(2,1)}, u32[]{:S(2)}) copy-start(bf16[128,1024]{1,0:T(8,128)(2,1)} %get-tuple-element.32) | copy-start | bytes 786436
  33.3 13.3 %copy-start.2 = (bf16[152,1024]{1,0:T(8,128)(2,1)S(1)}, bf16[152,1024]{1,0:T(8,128)(2,1)}, u32[]{:S(2)}) copy-start(bf16[152,1024]{1,0:T(8,128)(2,1)} %get-tuple-element.23) | copy-start | bytes 933892
  34.7 28.8 %collective-permute-start.3 = (bf16[4,1024,256]{2,1,0:T(8,128)(2,1)S(1)}, bf16[4,1024,256]{2,1,0:T(8,128)(2,1)S(1)}, u32[]{:S(2)}, u32[]{:S(2)}) collective-permute-start(bf16[4,1024,256]{2,1,0:T(8,128)(2,1)S(1)} %pad_maximum_fusion), channel_id=1, source_target_pairs={{0,1},{1,0},{2,3},{3,2},{4,5},{5,4},{6,7},{7,6},{8,9},{9,8},{10,11... | collective-permute-start | bytes 6291464 | tf_op jit(solution)/shard_map/ppermute | solution.py:23
  36.6 6.5 %collective-permute-start.10 = (bf16[2,24,1024]{2,1,0:T(8,128)(2,1)S(1)}, bf16[2,24,1024]{2,1,0:T(8,128)(2,1)S(1)}, u32[]{:S(2)}, u32[]{:S(2)}) collective-permute-start(bf16[2,24,1024]{2,1,0:T(8,128)(2,1)S(1)} %pad_maximum_fusion.9), channel_id=1, source_target_pairs={{0,192},{32,224},{64,0},{96,32},{128,64},{160,96},{192,128},{224,1... | collective-permute-start | bytes 294920 | tf_op jit(solution)/shard_map/ppermute | solution.py:23
  37.9 7.7 %collective-permute-start.9 = (bf16[2,24,1024]{2,1,0:T(8,128)(2,1)S(1)}, bf16[2,24,1024]{2,1,0:T(8,128)(2,1)S(1)}, u32[]{:S(2)}, u32[]{:S(2)}) collective-permute-start(bf16[2,24,1024]{2,1,0:T(8,128)(2,1)S(1)} %pad_maximum_fusion.8), channel_id=1, source_target_pairs={{0,64},{32,96},{64,128},{96,160},{128,192},{160,224},{192,0},{224,... | collective-permute-start | bytes 294920 | tf_op jit(solution)/shard_map/ppermute | solution.py:23
  39.2 18.2 %collective-permute-start.20 = (bf16[128,1024]{1,0:T(8,128)(2,1)S(1)}, bf16[128,1024]{1,0:T(8,128)(2,1)S(1)}, u32[]{:S(2)}, u32[]{:S(2)}) collective-permute-start(bf16[128,1024]{1,0:T(8,128)(2,1)S(1)} %copy-done.3), channel_id=1, source_target_pairs={{0,32},{32,64},{64,96},{96,128},{128,160},{160,192},{192,224},{224... | collective-permute-start | bytes 786440 | tf_op jit(solution)/shard_map/ppermute | solution.py:23
  40.0 17.4 %collective-permute-start.21 = (bf16[128,1024]{1,0:T(8,128)(2,1)S(1)}, bf16[128,1024]{1,0:T(8,128)(2,1)S(1)}, u32[]{:S(2)}, u32[]{:S(2)}) collective-permute-start(bf16[128,1024]{1,0:T(8,128)(2,1)S(1)} %copy-done.3), channel_id=1, source_target_pairs={{0,224},{32,0},{64,32},{96,64},{128,96},{160,128},{192,160},{224,1... | collective-permute-start | bytes 786440 | tf_op jit(solution)/shard_map/ppermute | solution.py:23
  43.1 12.8 %collective-permute-start.7 = (bf16[4,24,1024]{2,1,0:T(8,128)(2,1)S(1)}, bf16[4,24,1024]{2,1,0:T(8,128)(2,1)S(1)}, u32[]{:S(2)}, u32[]{:S(2)}) collective-permute-start(bf16[4,24,1024]{2,1,0:T(8,128)(2,1)S(1)} %pad_maximum_fusion.7.m0), channel_id=1, source_target_pairs={{0,32},{32,64},{64,96},{96,128},{128,160},{160,192},{192,224},{224... | collective-permute-start | bytes 589832 | tf_op jit(solution)/shard_map/ppermute | solution.py:23
  45.6 10.3 %collective-permute-start.8 = (bf16[4,24,1024]{2,1,0:T(8,128)(2,1)S(1)}, bf16[4,24,1024]{2,1,0:T(8,128)(2,1)S(1)}, u32[]{:S(2)}, u32[]{:S(2)}) collective-permute-start(bf16[4,24,1024]{2,1,0:T(8,128)(2,1)S(1)} %pad_maximum_fusion.7.m0), channel_id=1, source_target_pairs={{0,224},{32,0},{64,32},{96,64},{128,96},{160,128},{192,160},{224,1... | collective-permute-start | bytes 589832 | tf_op jit(solution)/shard_map/ppermute | solution.py:23
  46.6 18.4 %copy-start = (bf16[1,1024,256]{2,1,0:T(8,128)(2,1)S(1)}, bf16[1,1024,256]{2,1,0:T(8,128)(2,1)}, u32[]{:S(2)}) copy-start(bf16[1,1024,256]{2,1,0:T(8,128)(2,1)} %param.12) | copy-start | bytes 1572868
  46.6 18.4 %copy-start.1 = (bf16[4,128,128]{2,1,0:T(8,128)(2,1)S(1)}, bf16[4,128,128]{2,1,0:T(8,128)(2,1)}, u32[]{:S(2)}) copy-start(bf16[4,128,128]{2,1,0:T(8,128)(2,1)} %refs_7_.1) | copy-start | bytes 393220
  56.2 6.1 %collective-permute-start.11 = (bf16[2064,128]{1,0:T(8,128)(2,1)S(1)}, bf16[2064,128]{1,0:T(8,128)(2,1)S(1)}, u32[]{:S(2)}, u32[]{:S(2)}) collective-permute-start(bf16[2064,128]{1,0:T(8,128)(2,1)S(1)} %get-tuple-element.24.refs_5_), channel_id=1, source_target_pairs={{0,1},{1,0},{2,3},{3,2},{4,5},{5,4},{6,7},{7,6},{8,9},{9,8},{10,11... | collective-permute-start | bytes 1585160 | tf_op jit(solution)/shard_map/ppermute | solution.py:23
  57.6 28.2 %collective-permute-start.24 = (bf16[4,128,1024]{2,1,0:T(8,128)(2,1)S(1)}, bf16[4,128,1024]{2,1,0:T(8,128)(2,1)S(1)}, u32[]{:S(2)}, u32[]{:S(2)}) collective-permute-start(bf16[4,128,1024]{2,1,0:T(8,128)(2,1)S(1)} %pad_maximum_fusion.2.refs_0_), channel_id=1, source_target_pairs={{0,8},{8,16},{16,24},{24,0},{1,9},{9,17},{17,25},{25,1},{2,10},{10... | collective-permute-start | bytes 3145736 | tf_op jit(solution)/shard_map/ppermute | solution.py:23
  59.0 9.8 %collective-permute-start.16 = (bf16[528,256]{1,0:T(8,128)(2,1)S(1)}, bf16[528,256]{1,0:T(8,128)(2,1)S(1)}, u32[]{:S(2)}, u32[]{:S(2)}) collective-permute-start(bf16[528,256]{1,0:T(8,128)(2,1)S(1)} %get-tuple-element.27.refs_10_), channel_id=1, source_target_pairs={{0,2},{2,4},{4,6},{6,0},{1,3},{3,5},{5,7},{7,1},{8,10},{10,12},{12... | collective-permute-start | bytes 811016 | tf_op jit(solution)/shard_map/ppermute | solution.py:23
  59.9 9.6 %collective-permute-start.17 = (bf16[528,256]{1,0:T(8,128)(2,1)S(1)}, bf16[528,256]{1,0:T(8,128)(2,1)S(1)}, u32[]{:S(2)}, u32[]{:S(2)}) collective-permute-start(bf16[528,256]{1,0:T(8,128)(2,1)S(1)} %get-tuple-element.27.refs_10_), channel_id=1, source_target_pairs={{0,6},{2,0},{4,2},{6,4},{1,7},{3,1},{5,3},{7,5},{8,14},{10,8},{12,... | collective-permute-start | bytes 811016 | tf_op jit(solution)/shard_map/ppermute | solution.py:23
  62.3 13.2 %collective-permute-start.18 = (bf16[528,256]{1,0:T(8,128)(2,1)S(1)}, bf16[528,256]{1,0:T(8,128)(2,1)S(1)}, u32[]{:S(2)}, u32[]{:S(2)}) collective-permute-start(bf16[528,256]{1,0:T(8,128)(2,1)S(1)} %get-tuple-element.27.refs_10_), channel_id=1, source_target_pairs={{0,4},{2,6},{4,0},{6,2},{1,5},{3,7},{5,1},{7,3},{8,12},{10,14},{12... | collective-permute-start | bytes 811016 | tf_op jit(solution)/shard_map/ppermute | solution.py:23
  63.5 24.1 %collective-permute-start.25 = (bf16[4,128,1024]{2,1,0:T(8,128)(2,1)S(1)}, bf16[4,128,1024]{2,1,0:T(8,128)(2,1)S(1)}, u32[]{:S(2)}, u32[]{:S(2)}) collective-permute-start(bf16[4,128,1024]{2,1,0:T(8,128)(2,1)S(1)} %pad_maximum_fusion.2.refs_0_), channel_id=1, source_target_pairs={{0,24},{8,0},{16,8},{24,16},{1,25},{9,1},{17,9},{25,17},{2,26},{10... | collective-permute-start | bytes 3145736 | tf_op jit(solution)/shard_map/ppermute | solution.py:23
  68.8 10.2 %collective-permute-start.12 = (bf16[512,128]{1,0:T(8,128)(2,1)S(1)}, bf16[512,128]{1,0:T(8,128)(2,1)S(1)}, u32[]{:S(2)}, u32[]{:S(2)}) collective-permute-start(bf16[512,128]{1,0:T(8,128)(2,1)S(1)} %get-tuple-element.26), channel_id=1, source_target_pairs={{0,2},{2,4},{4,6},{6,0},{1,3},{3,5},{5,7},{7,1},{8,10},{10,12},{12... | collective-permute-start | bytes 393224 | tf_op jit(solution)/shard_map/ppermute | solution.py:23
  75.7 33.2 %collective-permute-start.19 = (bf16[4,528,256]{2,1,0:T(8,128)(2,1)S(1)}, bf16[4,528,256]{2,1,0:T(8,128)(2,1)S(1)}, u32[]{:S(2)}, u32[]{:S(2)}) collective-permute-start(bf16[4,528,256]{2,1,0:T(8,128)(2,1)S(1)} %pad_maximum_fusion.1), channel_id=1, source_target_pairs={{0,1},{1,0},{2,3},{3,2},{4,5},{5,4},{6,7},{7,6},{8,9},{9,8},{10,11... | collective-permute-start | bytes 3244040 | tf_op jit(solution)/shard_map/ppermute | solution.py:23
  77.7 5.0 %collective-permute-start.13 = (bf16[512,128]{1,0:T(8,128)(2,1)S(1)}, bf16[512,128]{1,0:T(8,128)(2,1)S(1)}, u32[]{:S(2)}, u32[]{:S(2)}) collective-permute-start(bf16[512,128]{1,0:T(8,128)(2,1)S(1)} %get-tuple-element.26), channel_id=1, source_target_pairs={{0,6},{2,0},{4,2},{6,4},{1,7},{3,1},{5,3},{7,5},{8,14},{10,8},{12,... | collective-permute-start | bytes 393224 | tf_op jit(solution)/shard_map/ppermute | solution.py:23
  79.0 6.1 %collective-permute-start.14 = (bf16[512,128]{1,0:T(8,128)(2,1)S(1)}, bf16[512,128]{1,0:T(8,128)(2,1)S(1)}, u32[]{:S(2)}, u32[]{:S(2)}) collective-permute-start(bf16[512,128]{1,0:T(8,128)(2,1)S(1)} %get-tuple-element.26), channel_id=1, source_target_pairs={{0,4},{2,6},{4,0},{6,2},{1,5},{3,7},{5,1},{7,3},{8,12},{10,14},{12... | collective-permute-start | bytes 393224 | tf_op jit(solution)/shard_map/ppermute | solution.py:23
  82.7 24.4 %collective-permute-start.28 = (bf16[4,128,1024]{2,1,0:T(8,128)(2,1)S(1)}, bf16[4,128,1024]{2,1,0:T(8,128)(2,1)S(1)}, u32[]{:S(2)}, u32[]{:S(2)}) collective-permute-start(bf16[4,128,1024]{2,1,0:T(8,128)(2,1)S(1)} %pad_maximum_fusion.3.b0), channel_id=1, source_target_pairs={{0,32},{32,64},{64,96},{96,128},{128,160},{160,192},{192,224},{224... | collective-permute-start | bytes 3145736 | tf_op jit(solution)/shard_map/ppermute | solution.py:23
  85.0 23.5 %collective-permute-start.29 = (bf16[4,128,1024]{2,1,0:T(8,128)(2,1)S(1)}, bf16[4,128,1024]{2,1,0:T(8,128)(2,1)S(1)}, u32[]{:S(2)}, u32[]{:S(2)}) collective-permute-start(bf16[4,128,1024]{2,1,0:T(8,128)(2,1)S(1)} %pad_maximum_fusion.3.b0), channel_id=1, source_target_pairs={{0,224},{32,0},{64,32},{96,64},{128,96},{160,128},{192,160},{224,1... | collective-permute-start | bytes 3145736 | tf_op jit(solution)/shard_map/ppermute | solution.py:23
  85.8 25.8 %collective-permute-start.15 = (bf16[3,512,128]{2,1,0:T(8,128)(2,1)S(1)}, bf16[3,512,128]{2,1,0:T(8,128)(2,1)S(1)}, u32[]{:S(2)}, u32[]{:S(2)}) collective-permute-start(bf16[3,512,128]{2,1,0:T(8,128)(2,1)S(1)} %pad_maximum_fusion.6), channel_id=1, source_target_pairs={{0,1},{1,0},{2,3},{3,2},{4,5},{5,4},{6,7},{7,6},{8,9},{9,8},{10,11... | collective-permute-start | bytes 1179656 | tf_op jit(solution)/shard_map/ppermute | solution.py:23
  87.6 32.6 %collective-permute-start.26 = (bf16[2,128,1024]{2,1,0:T(8,128)(2,1)S(1)}, bf16[2,128,1024]{2,1,0:T(8,128)(2,1)S(1)}, u32[]{:S(2)}, u32[]{:S(2)}) collective-permute-start(bf16[2,128,1024]{2,1,0:T(8,128)(2,1)S(1)} %slice.117), channel_id=1, source_target_pairs={{0,8},{8,16},{16,24},{24,0},{1,9},{9,17},{17,25},{25,1},{2,10},{10... | collective-permute-start | bytes 1572872 | tf_op jit(solution)/shard_map/ppermute | solution.py:23
  107.1 13.1 %collective-permute-start.27 = (bf16[2,128,1024]{2,1,0:T(8,128)(2,1)S(1)}, bf16[2,128,1024]{2,1,0:T(8,128)(2,1)S(1)}, u32[]{:S(2)}, u32[]{:S(2)}) collective-permute-start(bf16[2,128,1024]{2,1,0:T(8,128)(2,1)S(1)} %slice.118), channel_id=1, source_target_pairs={{0,24},{8,0},{16,8},{24,16},{1,25},{9,1},{17,9},{25,17},{2,26},{10... | collective-permute-start | bytes 1572872 | tf_op jit(solution)/shard_map/ppermute | solution.py:23
  108.5 14.3 %collective-permute-start.30 = (bf16[2,128,1024]{2,1,0:T(8,128)(2,1)S(1)}, bf16[2,128,1024]{2,1,0:T(8,128)(2,1)S(1)}, u32[]{:S(2)}, u32[]{:S(2)}) collective-permute-start(bf16[2,128,1024]{2,1,0:T(8,128)(2,1)S(1)} %slice.122), channel_id=1, source_target_pairs={{0,32},{32,64},{64,96},{96,128},{128,160},{160,192},{192,224},{224... | collective-permute-start | bytes 1572872 | tf_op jit(solution)/shard_map/ppermute | solution.py:23
  108.9 13.9 %collective-permute-start.31 = (bf16[2,128,1024]{2,1,0:T(8,128)(2,1)S(1)}, bf16[2,128,1024]{2,1,0:T(8,128)(2,1)S(1)}, u32[]{:S(2)}, u32[]{:S(2)}) collective-permute-start(bf16[2,128,1024]{2,1,0:T(8,128)(2,1)S(1)} %slice.123), channel_id=1, source_target_pairs={{0,224},{32,0},{64,32},{96,64},{128,96},{160,128},{192,160},{224,1... | collective-permute-start | bytes 1572872 | tf_op jit(solution)/shard_map/ppermute | solution.py:23
  126.2 10.2 %collective-permute-start.33 = (bf16[2,1024,256]{2,1,0:T(8,128)(2,1)S(1)}, bf16[2,1024,256]{2,1,0:T(8,128)(2,1)S(1)}, u32[]{:S(2)}, u32[]{:S(2)}) collective-permute-start(bf16[2,1024,256]{2,1,0:T(8,128)(2,1)S(1)} %get-tuple-element.38), channel_id=1, source_target_pairs={{0,1},{1,0},{2,3},{3,2},{4,5},{5,4},{6,7},{7,6},{8,9},{9,8},{10,11... | collective-permute-start | bytes 3145736 | tf_op jit(solution)/shard_map/ppermute | solution.py:23
  131.1 2.3 %collective-permute-start.34 = (bf16[1,1024,256]{2,1,0:T(8,128)(2,1)S(1)}, bf16[1,1024,256]{2,1,0:T(8,128)(2,1)S(1)}, u32[]{:S(2)}, u32[]{:S(2)}) collective-permute-start(bf16[1,1024,256]{2,1,0:T(8,128)(2,1)S(1)} %get-tuple-element.40), channel_id=1, source_target_pairs={{0,1},{1,0},{2,3},{3,2},{4,5},{5,4},{6,7},{7,6},{8,9},{9,8},{10,11... | collective-permute-start | bytes 1572872 | tf_op jit(solution)/shard_map/ppermute | solution.py:23
  132.9 12.9 %collective-permute-start.32 = (bf16[1,1024,256]{2,1,0:T(8,128)(2,1)S(1)}, bf16[1,1024,256]{2,1,0:T(8,128)(2,1)S(1)}, u32[]{:S(2)}, u32[]{:S(2)}) collective-permute-start(bf16[1,1024,256]{2,1,0:T(8,128)(2,1)S(1)} %get-tuple-element.36), channel_id=1, source_target_pairs={{0,1},{1,0},{2,3},{3,2},{4,5},{5,4},{6,7},{7,6},{8,9},{9,8},{10,11... | collective-permute-start | bytes 1572872 | tf_op jit(solution)/shard_map/ppermute | solution.py:23
  133.7 9.1 %collective-permute-start.35 = (bf16[512,256]{1,0:T(8,128)(2,1)S(1)}, bf16[512,256]{1,0:T(8,128)(2,1)S(1)}, u32[]{:S(2)}, u32[]{:S(2)}) collective-permute-start(bf16[512,256]{1,0:T(8,128)(2,1)S(1)} %get-tuple-element.43), channel_id=1, source_target_pairs={{0,2},{2,4},{4,6},{6,0},{1,3},{3,5},{5,7},{7,1},{8,10},{10,12},{12... | collective-permute-start | bytes 786440 | tf_op jit(solution)/shard_map/ppermute | solution.py:23
  133.9 9.1 %collective-permute-start.37 = (bf16[512,256]{1,0:T(8,128)(2,1)S(1)}, bf16[512,256]{1,0:T(8,128)(2,1)S(1)}, u32[]{:S(2)}, u32[]{:S(2)}) collective-permute-start(bf16[512,256]{1,0:T(8,128)(2,1)S(1)} %get-tuple-element.44), channel_id=1, source_target_pairs={{0,6},{2,0},{4,2},{6,4},{1,7},{3,1},{5,3},{7,5},{8,14},{10,8},{12,... | collective-permute-start | bytes 786440 | tf_op jit(solution)/shard_map/ppermute | solution.py:23
  142.9 13.9 %collective-permute-start.36 = (bf16[1024,256]{1,0:T(8,128)(2,1)S(1)}, bf16[1024,256]{1,0:T(8,128)(2,1)S(1)}, u32[]{:S(2)}, u32[]{:S(2)}) collective-permute-start(bf16[1024,256]{1,0:T(8,128)(2,1)S(1)} %pad_maximum_fusion.4), channel_id=1, source_target_pairs={{0,2},{2,4},{4,6},{6,0},{1,3},{3,5},{5,7},{7,1},{8,10},{10,12},{12... | collective-permute-start | bytes 1572872 | tf_op jit(solution)/shard_map/ppermute | solution.py:23
  143.1 13.6 %collective-permute-start.38 = (bf16[1024,256]{1,0:T(8,128)(2,1)S(1)}, bf16[1024,256]{1,0:T(8,128)(2,1)S(1)}, u32[]{:S(2)}, u32[]{:S(2)}) collective-permute-start(bf16[1024,256]{1,0:T(8,128)(2,1)S(1)} %pad_maximum_fusion.5), channel_id=1, source_target_pairs={{0,6},{2,0},{4,2},{6,4},{1,7},{3,1},{5,3},{7,5},{8,14},{10,8},{12,... | collective-permute-start | bytes 1572872 | tf_op jit(solution)/shard_map/ppermute | solution.py:23

commit v5 on v4

--- a/solution.py
+++ b/solution.py
@@ -68,7 +68,7 @@
 
 def prep_kernel(
     norm_gain_at, w_in_at, s_in_at, w_out_at, s_out_at, ffn_gain_at, w_up_at, s_up_at, w_down_at, s_down_at,
-    packet, up, top, bottom, small, norm_gain, w_in, s_in, w_out, s_out, ffn_gain, w_up, s_up, w_down, s_down, done,
+    packet, up, mixer, down, small, norm_gain, w_in, s_in, w_out, s_out, ffn_gain, w_up, s_up, w_down, s_down, done,
 ):
     sources = (norm_gain_at, w_in_at, s_in_at, w_out_at, s_out_at, s_up_at, ffn_gain_at, w_up_at, w_down_at, s_down_at)
     targets = (norm_gain, w_in, s_in, w_out, s_out, s_up, ffn_gain, w_up, w_down, s_down)
@@ -90,19 +90,19 @@
         high, low = two_parts(row)
         small[16:17, at : at + row.shape[1]] = high
         small[16:17, at + 128 : at + 128 + row.shape[1]] = low
-    packet[128:] = small[...].astype(BF)
+    mixer[...] = small[...].astype(BF)
+    packet[128:] = mixer[...]
     for copy in copies[6:]:
         copy.wait()
     gain = column_of(ffn_gain[pl.ds(f, 1), :])
     for j in range(8):
         lanes = slice(j * 128, j * 128 + 128)
         up[:, lanes] = (w_up[:, lanes] * gain).astype(BF)
-        packet[:128, lanes] = (w_down[lanes, :] * s_down[...]).T.astype(BF)
-    top[...] = up[:64]
-    bottom[...] = up[64:]
-
-
-def unpack_kernel(m0, m1, m2, m3, m4, w_in, w_out, s_up):
+        down[:, lanes] = (w_down[lanes, :] * s_down[...]).T.astype(BF)
+    packet[:128] = down[...]
+
+
+def unpack_kernel(m0, m1, m2, m3, w_in, w_out, s_up):
     ys, zs = around(lax.axis_index("y")), around(lax.axis_index("z"))
     lane = lax.broadcasted_iota(jnp.int32, (16, 128), 1)
     at = lax.broadcasted_iota(jnp.int32, (16, 128), 0)
@@ -111,8 +111,7 @@
     for p, zz in enumerate(zs):
         for k, yy in enumerate(ys):
             f = 4 * zz + yy
-            source = (m0, m1, m2)[p].at[k] if p < 3 else (m3, m4)[k // 2].at[k % 2]
-            block = source[...].astype(F32)
+            block = (m0, m1, m2, m3)[p][k].astype(F32)
             for j in range(8):
                 part = block[:8, j * 128 : j * 128 + 128]
                 turned = pltpu.roll(part, 64, 1)
@@ -280,7 +279,8 @@
         hidden[rows, cols] = (value * value).astype(BF)
 
 
-def down_kernel(steps, hidden, b0, b1, b2, b3, b4, own, other, taken):
+def down_kernel(steps, hidden, *refs):
+    parts, (own, other, taken) = refs[:8], refs[8:]
     x, y, z = (lax.axis_index(name) for name in ("x", "y", "z"))
     core = lax.shift_right_logical(y, 1)
     y_is_own = core == lax.axis_index("c")
@@ -291,20 +291,14 @@
     def _(k):
         chip = lax.rem(x + ((2 * k + 1) if len(steps) > 1 else steps[0]), 4)
         away = lax.rem(chip - z + 4, 4)
-        for place, source in ((0, b0), (3, b1), (1, b2)):
+        for k_place, place in enumerate((0, 3, 1, 2)):
 
             @pl.when(away == place)
-            def _(source=source):
-                @pl.loop(0, 4)
+            def _(k_place=k_place):
+                @pl.loop(0, 2)
                 def _(i):
-                    taken[i] = source[i]
-
-        @pl.when(away == 2)
-        def _():
-            @pl.loop(0, 2)
-            def _(i):
-                taken[i] = b3[i]
-                taken[i + 2] = b4[i]
+                    taken[i] = parts[2 * k_place][i]
+                    taken[i + 2] = parts[2 * k_place + 1][i]
 
         @pl.loop(0, 2)
         def _(block):
@@ -367,9 +361,9 @@
         w_down,
         s_down[None],
     )
-    packet, up, top, bottom = call(
+    packet, up, mixer, down = call(
         prep_kernel,
-        (bf(152, 1024), bf(128, 1024), bf(64, 1024), bf(64, 1024)),
+        (bf(152, 1024), bf(128, 1024), bf(24, 1024), bf(128, 1024)),
         [pltpu.VMEM((24, 1024), F32)]
         + [pltpu.VMEM(a.shape, F32) for a in arrays]
         + [pltpu.SemaphoreType.DMA((10,))],
@@ -378,16 +372,19 @@
         *arrays,
         in_hbm=10,
     )
-    packets = [packet] + three(packet, "y")
-    far_top, far_bottom = send(top, ring_z, 2), send(bottom, ring_z, -2)
-    low, high = send(up, ring_z, 1), send(up, ring_z, -1)
-    far = jnp.concatenate([far_top, far_bottom], axis=0)
-    up_bundle = jnp.stack([up, low, high, far])
-    mixer = jnp.stack([p[128:] for p in packets])
-    mixers = [mixer, send(mixer, ring_z, 1), send(mixer, ring_z, -1)]
-    mixers += [send(mixer[:2], ring_z, 2), send(mixer[2:], ring_z, -2)]
+    packets = three(packet, "y")
+    far = send(up, ring_z, 2)
+    up_bundle = jnp.stack([up, send(up, ring_z, 1), send(up, ring_z, -1), far])
+    mixer = jnp.stack([mixer] + [p[128:] for p in packets])
+    far = send(mixer, ring_z, -2)
+    mixers = [mixer, send(mixer, ring_z, 1), send(mixer, ring_z, -1), far]
     up_parts = along(up_bundle, "y")
-    down_parts = along(jnp.stack([p[:128] for p in packets]), ring_z)
+    top = jnp.stack([down, packets[0][:128]])
+    bottom = jnp.stack([packets[1][:128], packets[2][:128]])
+    low_top, high_bottom = send(top, ring_z, 1), send(bottom, ring_z, -1)
+    low_bottom, high_top = send(bottom, ring_z, 1), send(top, ring_z, -1)
+    far_top, far_bottom = send(low_top, ring_z, 1), send(high_bottom, ring_z, -1)
+    down_parts = [top, bottom, low_top, low_bottom, high_top, high_bottom, far_top, far_bottom]
     w_in_own, out_own, s_up_row = call(
         unpack_kernel, (bf(2064, 128), bf(528, 256), f32(1, 1024)), [], 8, 1_000_000, *mixers
     )

time: 159 us -> 163 us (1.025)
  waiting for transfers between devices: 65.5 us -> 71.3 us
    ppermute x39, waiting for transfers between devices: 65.5 us -> 71.3 us  [send(): lax.ppermute(array, axes, [(i, (i + shift) % count) for i in range(count)])]
  transfers between devices with their start and end apart: 39 -> 39, of which waited for: 13 -> 16; matrix products, arithmetic and copies ran while one was open for 2% -> 2% of each run, Pallas kernels for 13% -> 13%
where the time goes in v5:
time: 163 us
  waiting for transfers between devices  71.3 us (44%)
  starting transfers between devices  63.3 us (39%)
  Pallas kernels  24.2 us (15%)
  other arithmetic  3.45 us (2%)
    ppermute x39, waiting for transfers between devices, send(): lax.ppermute(array, axes, [(i, (i + shift) % count) for i in range(count)])  71.3 us
    ppermute x39, starting transfers between devices, send(): lax.ppermute(array, axes, [(i, (i + shift) % count) for i in range(count)])  63.3 us
    pallas_call x9, Pallas kernels, call(): pl.pallas_call(kernel, out_shape=out_shape, in_specs=[VMEM] * (len(args)...  24.2 us
  transfers between devices with their start and end apart: 39, of which 16 were waited for; matrix products, arithmetic and copies ran while one was open for 2% of the time, Pallas kernels for 13%

profile of v5, /device:TPU:1, one launch (start us, length us, event | category | flops | bytes accessed | tf_op | source)
XLA Modules:
  0.0 162.9 jit_solution(3179500762492302362)
XLA Ops:
  0.0 2.0 %collective-permute-start = (bf16[1024,256]{1,0:T(8,128)(2,1)}, bf16[1024,256]{1,0:T(8,128)(2,1)S(1)}, u32[]{:S(2)}, u32[]{:S(2)}) collective-permute-start(bf16[1024,256]{1,0:T(8,128)(2,1)} %bitcast.68), channel_id=1, source_target_pairs={{0,2},{2,4},{4,6},{6,0},{1,3},{3,5},{5,7},{7,1},{8,10},{10,12},{12... | collective-permute-start | bytes 1572872 | tf_op jit(solution)/shard_map/ppermute | solution.py:23
  2.0 1.3 collective-permute-start.1
  3.3 1.7 %collective-permute-start.2 = (bf16[1024,256]{1,0:T(8,128)(2,1)}, bf16[1024,256]{1,0:T(8,128)(2,1)S(1)}, u32[]{:S(2)}, u32[]{:S(2)}) collective-permute-start(bf16[1024,256]{1,0:T(8,128)(2,1)} %bitcast.70), channel_id=1, source_target_pairs={{0,4},{2,6},{4,0},{6,2},{1,5},{3,7},{5,1},{7,3},{8,12},{10,14},{12... | collective-permute-start | bytes 1572872 | tf_op jit(solution)/shard_map/ppermute | solution.py:23
  5.0 2.4 %shard_map.118 = (bf16[152,1024]{1,0:T(8,128)(2,1)}, bf16[128,1024]{1,0:T(8,128)(2,1)}, bf16[24,1024]{1,0:T(8,128)(2,1)}, bf16[128,1024]{1,0:T(8,128)(2,1)}) custom-call(f32[16,128]{1,0:T(8,128)} %bitcast.90, f32[64,128]{1,0:T(8,128)} %bitcast.89, f32[1,4]{1,0:T(1,128)} %bitcast.92, f32[32,256]{1,0:T(8,128)} %w_out_at.1, f32[1,16]{1,0:T(1,128)} %bitcast.93, ...), custom_call_target="tpu_custom_call" | custom-call | flops 1000000 | bytes 1131344 | tf_op jit(solution)/shard_map/pallas_call | solution.py:54
  7.5 3.0 %collective-permute-start.6 = (bf16[152,1024]{1,0:T(8,128)(2,1)}, bf16[152,1024]{1,0:T(8,128)(2,1)S(1)}, u32[]{:S(2)}, u32[]{:S(2)}) collective-permute-start(bf16[152,1024]{1,0:T(8,128)(2,1)} %get-tuple-element.24), channel_id=1, source_target_pairs={{0,16},{8,24},{16,0},{24,8},{1,17},{9,25},{17,1},{25,9},{2,18},{10... | collective-permute-start | bytes 933896 | tf_op jit(solution)/shard_map/ppermute | solution.py:23
  11.2 1.7 %collective-permute-done.refs_1_ = bf16[1024,256]{1,0:T(8,128)(2,1)S(1)} collective-permute-done((bf16[1024,256]{1,0:T(8,128)(2,1)}, bf16[1024,256]{1,0:T(8,128)(2,1)S(1)}, u32[]{:S(2)}, u32[]{:S(2)}) %collective-permute-start) | collective-permute-done | bytes 524320 | tf_op jit(solution)/shard_map/ppermute | solution.py:23
  12.9 3.4 %collective-permute-start.4 = (bf16[152,1024]{1,0:T(8,128)(2,1)}, bf16[152,1024]{1,0:T(8,128)(2,1)S(1)}, u32[]{:S(2)}, u32[]{:S(2)}) collective-permute-start(bf16[152,1024]{1,0:T(8,128)(2,1)} %get-tuple-element.24), channel_id=1, source_target_pairs={{0,8},{8,16},{16,24},{24,0},{1,9},{9,17},{17,25},{25,1},{2,10},{10... | collective-permute-start | bytes 933896 | tf_op jit(solution)/shard_map/ppermute | solution.py:23
  16.3 10.9 %collective-permute-done.2.refs_3_ = bf16[1024,256]{1,0:T(8,128)(2,1)S(1)} collective-permute-done((bf16[1024,256]{1,0:T(8,128)(2,1)}, bf16[1024,256]{1,0:T(8,128)(2,1)S(1)}, u32[]{:S(2)}, u32[]{:S(2)}) %collective-permute-start.2) | collective-permute-done | bytes 524320 | tf_op jit(solution)/shard_map/ppermute | solution.py:23
  27.3 1.3 pad_maximum_fusion
  28.6 1.6 collective-permute-start.3
  30.3 1.7 %collective-permute-start.7 = (bf16[4,24,1024]{2,1,0:T(8,128)(2,1)S(1)}, bf16[4,24,1024]{2,1,0:T(8,128)(2,1)S(1)}, u32[]{:S(2)}, u32[]{:S(2)}) collective-permute-start(bf16[4,24,1024]{2,1,0:T(8,128)(2,1)S(1)} %pad_maximum_fusion.8.m0), channel_id=1, source_target_pairs={{0,32},{32,64},{64,96},{96,128},{128,160},{160,192},{192,224},{224... | collective-permute-start | bytes 589832 | tf_op jit(solution)/shard_map/ppermute | solution.py:23
  32.1 4.0 %collective-permute-start.8 = (bf16[4,24,1024]{2,1,0:T(8,128)(2,1)S(1)}, bf16[4,24,1024]{2,1,0:T(8,128)(2,1)S(1)}, u32[]{:S(2)}, u32[]{:S(2)}) collective-permute-start(bf16[4,24,1024]{2,1,0:T(8,128)(2,1)S(1)} %pad_maximum_fusion.8.m0), channel_id=1, source_target_pairs={{0,224},{32,0},{64,32},{96,64},{128,96},{160,128},{192,160},{224,1... | collective-permute-start | bytes 589832 | tf_op jit(solution)/shard_map/ppermute | solution.py:23
  36.1 1.4 collective-permute-start.20
  37.5 3.8 %collective-permute-done.7.m1 = bf16[4,24,1024]{2,1,0:T(8,128)(2,1)S(1)} collective-permute-done((bf16[4,24,1024]{2,1,0:T(8,128)(2,1)S(1)}, bf16[4,24,1024]{2,1,0:T(8,128)(2,1)S(1)}, u32[]{:S(2)}, u32[]{:S(2)}) %collective-permute-start.7) | collective-permute-done | bytes 196640 | tf_op jit(solution)/shard_map/ppermute | solution.py:23
  41.2 2.4 %collective-permute-start.9 = (bf16[4,24,1024]{2,1,0:T(8,128)(2,1)S(1)}, bf16[4,24,1024]{2,1,0:T(8,128)(2,1)S(1)}, u32[]{:S(2)}, u32[]{:S(2)}) collective-permute-start(bf16[4,24,1024]{2,1,0:T(8,128)(2,1)S(1)} %pad_maximum_fusion.8.m0), channel_id=1, source_target_pairs={{0,192},{32,224},{64,0},{96,32},{128,64},{160,96},{192,128},{224,1... | collective-permute-start | bytes 589832 | tf_op jit(solution)/shard_map/ppermute | solution.py:23
  43.6 10.9 %collective-permute-done.9.m3 = bf16[4,24,1024]{2,1,0:T(8,128)(2,1)S(1)} collective-permute-done((bf16[4,24,1024]{2,1,0:T(8,128)(2,1)S(1)}, bf16[4,24,1024]{2,1,0:T(8,128)(2,1)S(1)}, u32[]{:S(2)}, u32[]{:S(2)}) %collective-permute-start.9) | collective-permute-done | bytes 196640 | tf_op jit(solution)/shard_map/ppermute | solution.py:23
  54.9 0.9 collective-permute-start.15
  55.9 2.2 %collective-permute-done.19 = bf16[128,1024]{1,0:T(8,128)(2,1)S(1)} collective-permute-done((bf16[128,1024]{1,0:T(8,128)(2,1)S(1)}, bf16[128,1024]{1,0:T(8,128)(2,1)S(1)}, u32[]{:S(2)}, u32[]{:S(2)}) %collective-permute-start.19) | collective-permute-done | bytes 262176 | tf_op jit(solution)/shard_map/ppermute | solution.py:23
  58.3 1.4 collective-permute-start.22
  59.6 1.7 %collective-permute-start.16 = (bf16[528,256]{1,0:T(8,128)(2,1)S(1)}, bf16[528,256]{1,0:T(8,128)(2,1)S(1)}, u32[]{:S(2)}, u32[]{:S(2)}) collective-permute-start(bf16[528,256]{1,0:T(8,128)(2,1)S(1)} %get-tuple-element.28.refs_10_), channel_id=1, source_target_pairs={{0,6},{2,0},{4,2},{6,4},{1,7},{3,1},{5,3},{7,5},{8,14},{10,8},{12,... | collective-permute-start | bytes 811016 | tf_op jit(solution)/shard_map/ppermute | solution.py:23
  61.3 1.0 collective-permute-start.17
  62.8 2.3 %collective-permute-start.10 = (bf16[2064,128]{1,0:T(8,128)(2,1)S(1)}, bf16[2064,128]{1,0:T(8,128)(2,1)S(1)}, u32[]{:S(2)}, u32[]{:S(2)}) collective-permute-start(bf16[2064,128]{1,0:T(8,128)(2,1)S(1)} %get-tuple-element.25.refs_5_), channel_id=1, source_target_pairs={{0,1},{1,0},{2,3},{3,2},{4,5},{5,4},{6,7},{7,6},{8,9},{9,8},{10,11... | collective-permute-start | bytes 1585160 | tf_op jit(solution)/shard_map/ppermute | solution.py:23
  65.1 1.7 %collective-permute-done.16.refs_12_ = bf16[528,256]{1,0:T(8,128)(2,1)S(1)} collective-permute-done((bf16[528,256]{1,0:T(8,128)(2,1)S(1)}, bf16[528,256]{1,0:T(8,128)(2,1)S(1)}, u32[]{:S(2)}, u32[]{:S(2)}) %collective-permute-start.16) | collective-permute-done | bytes 270368 | tf_op jit(solution)/shard_map/ppermute | solution.py:23
  66.8 2.0 %collective-permute-start.23 = (bf16[4,128,1024]{2,1,0:T(8,128)(2,1)S(1)}, bf16[4,128,1024]{2,1,0:T(8,128)(2,1)S(1)}, u32[]{:S(2)}, u32[]{:S(2)}) collective-permute-start(bf16[4,128,1024]{2,1,0:T(8,128)(2,1)S(1)} %pad_maximum_fusion.2.refs_0_), channel_id=1, source_target_pairs={{0,24},{8,0},{16,8},{24,16},{1,25},{9,1},{17,9},{25,17},{2,26},{10... | collective-permute-start | bytes 3145736 | tf_op jit(solution)/shard_map/ppermute | solution.py:23
  69.9 6.3 %collective-permute-start.18 = (bf16[4,528,256]{2,1,0:T(8,128)(2,1)S(1)}, bf16[4,528,256]{2,1,0:T(8,128)(2,1)S(1)}, u32[]{:S(2)}, u32[]{:S(2)}) collective-permute-start(bf16[4,528,256]{2,1,0:T(8,128)(2,1)S(1)} %pad_maximum_fusion.1), channel_id=1, source_target_pairs={{0,1},{1,0},{2,3},{3,2},{4,5},{5,4},{6,7},{7,6},{8,9},{9,8},{10,11... | collective-permute-start | bytes 3244040 | tf_op jit(solution)/shard_map/ppermute | solution.py:23
  76.1 3.6 %shard_map.120 = (bf16[1024,128]{1,0:T(8,128)(2,1)S(1)}, bf16[512,128]{1,0:T(8,128)(2,1)S(1)}) custom-call(bf16[1024,256]{1,0:T(8,128)(2,1)S(1)} %bitcast.71, bf16[1024,256]{1,0:T(8,128)(2,1)S(1)} %collective-permute-done.refs_1_, bf16[1024,256]{1,0:T(8,128)(2,1)S(1)} %collective-permute-done.1.refs_2_, ...), custom_call_target="tpu_custom_call" | custom-call | flops 800000000 | bytes 5382144 | tf_op jit(solution)/shard_map/pallas_call | solution.py:54
  79.8 3.5 %collective-permute-start.12 = (bf16[512,128]{1,0:T(8,128)(2,1)S(1)}, bf16[512,128]{1,0:T(8,128)(2,1)S(1)}, u32[]{:S(2)}, u32[]{:S(2)}) collective-permute-start(bf16[512,128]{1,0:T(8,128)(2,1)S(1)} %get-tuple-element.27), channel_id=1, source_target_pairs={{0,6},{2,0},{4,2},{6,4},{1,7},{3,1},{5,3},{7,5},{8,14},{10,8},{12,... | collective-permute-start | bytes 393224 | tf_op jit(solution)/shard_map/ppermute | solution.py:23
  84.6 2.4 %collective-permute-done.11.refs_6_ = bf16[512,128]{1,0:T(8,128)(2,1)S(1)} collective-permute-done((bf16[512,128]{1,0:T(8,128)(2,1)S(1)}, bf16[512,128]{1,0:T(8,128)(2,1)S(1)}, u32[]{:S(2)}, u32[]{:S(2)}) %collective-permute-start.11) | collective-permute-done | bytes 131104 | tf_op jit(solution)/shard_map/ppermute | solution.py:23
  87.1 2.7 %collective-permute-start.29 = (bf16[2,128,1024]{2,1,0:T(8,128)(2,1)S(1)}, bf16[2,128,1024]{2,1,0:T(8,128)(2,1)S(1)}, u32[]{:S(2)}, u32[]{:S(2)}) collective-permute-start(bf16[2,128,1024]{2,1,0:T(8,128)(2,1)S(1)} %pad_maximum_fusion.4.refs_1_), channel_id=1, source_target_pairs={{0,224},{32,0},{64,32},{96,64},{128,96},{160,128},{192,160},{224,1... | collective-permute-start | bytes 1572872 | tf_op jit(solution)/shard_map/ppermute | solution.py:23
  90.0 2.4 %collective-permute-start.14 = (bf16[3,512,128]{2,1,0:T(8,128)(2,1)S(1)}, bf16[3,512,128]{2,1,0:T(8,128)(2,1)S(1)}, u32[]{:S(2)}, u32[]{:S(2)}) collective-permute-start(bf16[3,512,128]{2,1,0:T(8,128)(2,1)S(1)} %pad_maximum_fusion.7), channel_id=1, source_target_pairs={{0,1},{1,0},{2,3},{3,2},{4,5},{5,4},{6,7},{7,6},{8,9},{9,8},{10,11... | collective-permute-start | bytes 1179656 | tf_op jit(solution)/shard_map/ppermute | solution.py:23
  92.4 8.7 %collective-permute-done.26.refs_2_ = bf16[2,128,1024]{2,1,0:T(8,128)(2,1)S(1)} collective-permute-done((bf16[2,128,1024]{2,1,0:T(8,128)(2,1)S(1)}, bf16[2,128,1024]{2,1,0:T(8,128)(2,1)S(1)}, u32[]{:S(2)}, u32[]{:S(2)}) %collective-permute-start.26) | collective-permute-done | bytes 524320 | tf_op jit(solution)/shard_map/ppermute | solution.py:23
  101.1 1.2 collective-permute-start.25
  102.8 2.2 %collective-permute-start.28 = (bf16[2,128,1024]{2,1,0:T(8,128)(2,1)S(1)}, bf16[2,128,1024]{2,1,0:T(8,128)(2,1)S(1)}, u32[]{:S(2)}, u32[]{:S(2)}) collective-permute-start(bf16[2,128,1024]{2,1,0:T(8,128)(2,1)S(1)} %pad_maximum_fusion.3.refs_0_), channel_id=1, source_target_pairs={{0,224},{32,0},{64,32},{96,64},{128,96},{160,128},{192,160},{224,1... | collective-permute-start | bytes 1572872 | tf_op jit(solution)/shard_map/ppermute | solution.py:23
  105.0 2.7 %collective-permute-start.31 = (bf16[2,128,1024]{2,1,0:T(8,128)(2,1)S(1)}, bf16[2,128,1024]{2,1,0:T(8,128)(2,1)S(1)}, u32[]{:S(2)}, u32[]{:S(2)}) collective-permute-start(bf16[2,128,1024]{2,1,0:T(8,128)(2,1)S(1)} %collective-permute-done.29.refs_5_), channel_id=1, source_target_pairs={{0,224},{32,0},{64,32},{96,64},{128,96},{160,128},{192,160},{224,1... | collective-permute-start | bytes 1572872 | tf_op jit(solution)/shard_map/ppermute | solution.py:23
  107.7 3.5 %shard_map.121 = (bf16[1024,2048]{1,0:T(8,128)(2,1)S(1)}, bf16[1024,256]{1,0:T(8,128)(2,1)S(1)}, f32[1024,128]{1,0:T(8,128)S(1)}) custom-call(bf16[1024,256]{1,0:T(8,128)(2,1)S(1)} %bitcast.72, bf16[1024,256]{1,0:T(8,128)(2,1)S(1)} %collective-permute-done.refs_1_, bf16[1024,256]{1,0:T(8,128)(2,1)S(1)} %collective-permute-done.1.refs_2_, ...), custom_call_target="tpu_custom_call" | custom-call | flops 2200000000 | bytes 7405568 | tf_op jit(solution)/shard_map/pallas_call | solution.py:54
  111.2 5.1 %shard_map.122.near = f32[1024,1024]{1,0:T(8,128)S(1)} custom-call(bf16[1024,2048]{1,0:T(8,128)(2,1)S(1)} %get-tuple-element.30.mixed, bf16[4,128,1024]{2,1,0:T(8,128)(2,1)S(1)} %pad_maximum_fusion.2.refs_0_, bf16[4,128,1024]{2,1,0:T(8,128)(2,1)S(1)} %collective-permute-done.22.refs_1_, bf16[4,128,1024]{2,1,0:T(8,128)(2,1)S(1)} %collective-permute-done.23.refs_2_), custom_call_target="tpu_custom_call" | custom-call | flops 3200000000 | bytes 7340032 | tf_op jit(solution)/shard_map/pallas_call | solution.py:54
  116.3 2.6 %shard_map.123.hidden = bf16[1024,1024]{1,0:T(8,128)(2,1)S(1)} custom-call(bf16[1024,2048]{1,0:T(8,128)(2,1)S(1)} %get-tuple-element.30.mixed, f32[1024,128]{1,0:T(8,128)S(1)} %get-tuple-element.31.factor, f32[1,1024]{1,0:T(1,128)S(1)} %get-tuple-element.32.s_up, f32[1024,1024]{1,0:T(8,128)S(1)} %shard_map.122.near, ...), custom_call_target="tpu_custom_call" | custom-call | flops 1100000000 | bytes 9965568 | tf_op jit(solution)/shard_map/pallas_call | solution.py:54
  118.9 7.6 %collective-permute-done.30.refs_6_ = bf16[2,128,1024]{2,1,0:T(8,128)(2,1)S(1)} collective-permute-done((bf16[2,128,1024]{2,1,0:T(8,128)(2,1)S(1)}, bf16[2,128,1024]{2,1,0:T(8,128)(2,1)S(1)}, u32[]{:S(2)}, u32[]{:S(2)}) %collective-permute-start.30) | collective-permute-done | bytes 524320 | tf_op jit(solution)/shard_map/ppermute | solution.py:23
  126.5 3.3 %shard_map.125 = (bf16[2,1024,256]{2,1,0:T(8,128)(2,1)S(1)}, bf16[2,1024,256]{2,1,0:T(8,128)(2,1)S(1)}) custom-call(bf16[1024,1024]{1,0:T(8,128)(2,1)S(1)} %shard_map.123.hidden, bf16[2,128,1024]{2,1,0:T(8,128)(2,1)S(1)} %pad_maximum_fusion.3.refs_0_, bf16[2,128,1024]{2,1,0:T(8,128)(2,1)S(1)} %pad_maximum_fusion.4.refs_1_, ...), custom_call_target="tpu_custom_call" | custom-call | flops 2150000128 | bytes 6291456 | tf_op jit(solution)/shard_map/pallas_call | solution.py:54
  129.8 2.7 %collective-permute-start.33 = (bf16[2,1024,256]{2,1,0:T(8,128)(2,1)S(1)}, bf16[2,1024,256]{2,1,0:T(8,128)(2,1)S(1)}, u32[]{:S(2)}, u32[]{:S(2)}) collective-permute-start(bf16[2,1024,256]{2,1,0:T(8,128)(2,1)S(1)} %get-tuple-element.38), channel_id=1, source_target_pairs={{0,1},{1,0},{2,3},{3,2},{4,5},{5,4},{6,7},{7,6},{8,9},{9,8},{10,11... | collective-permute-start | bytes 3145736 | tf_op jit(solution)/shard_map/ppermute | solution.py:23
  132.5 1.6 %shard_map.126 = (bf16[1,1024,256]{2,1,0:T(8,128)(2,1)S(1)}, bf16[1,1024,256]{2,1,0:T(8,128)(2,1)S(1)}) custom-call(bf16[1024,1024]{1,0:T(8,128)(2,1)S(1)} %shard_map.123.hidden, bf16[2,128,1024]{2,1,0:T(8,128)(2,1)S(1)} %pad_maximum_fusion.3.refs_0_, bf16[2,128,1024]{2,1,0:T(8,128)(2,1)S(1)} %pad_maximum_fusion.4.refs_1_, ...), custom_call_target="tpu_custom_call" | custom-call | flops 1075000064 | bytes 6291456 | tf_op jit(solution)/shard_map/pallas_call | solution.py:54
  134.3 1.7 %shard_map.124 = (bf16[1,1024,256]{2,1,0:T(8,128)(2,1)S(1)}, bf16[1,1024,256]{2,1,0:T(8,128)(2,1)S(1)}) custom-call(bf16[1024,1024]{1,0:T(8,128)(2,1)S(1)} %shard_map.123.hidden, bf16[2,128,1024]{2,1,0:T(8,128)(2,1)S(1)} %pad_maximum_fusion.3.refs_0_, bf16[2,128,1024]{2,1,0:T(8,128)(2,1)S(1)} %pad_maximum_fusion.4.refs_1_, ...), custom_call_target="tpu_custom_call" | custom-call | flops 1075000064 | bytes 6291456 | tf_op jit(solution)/shard_map/pallas_call | solution.py:54
  136.7 2.1 %collective-permute-start.37 = (bf16[512,256]{1,0:T(8,128)(2,1)S(1)}, bf16[512,256]{1,0:T(8,128)(2,1)S(1)}, u32[]{:S(2)}, u32[]{:S(2)}) collective-permute-start(bf16[512,256]{1,0:T(8,128)(2,1)S(1)} %get-tuple-element.44), channel_id=1, source_target_pairs={{0,6},{2,0},{4,2},{6,4},{1,7},{3,1},{5,3},{7,5},{8,14},{10,8},{12,... | collective-permute-start | bytes 786440 | tf_op jit(solution)/shard_map/ppermute | solution.py:23
  139.1 5.5 %collective-permute-done.37 = bf16[512,256]{1,0:T(8,128)(2,1)S(1)} collective-permute-done((bf16[512,256]{1,0:T(8,128)(2,1)S(1)}, bf16[512,256]{1,0:T(8,128)(2,1)S(1)}, u32[]{:S(2)}, u32[]{:S(2)}) %collective-permute-start.37) | collective-permute-done | bytes 262176 | tf_op jit(solution)/shard_map/ppermute | solution.py:23
  144.7 3.4 %collective-permute-start.38 = (bf16[1024,256]{1,0:T(8,128)(2,1)S(1)}, bf16[1024,256]{1,0:T(8,128)(2,1)S(1)}, u32[]{:S(2)}, u32[]{:S(2)}) collective-permute-start(bf16[1024,256]{1,0:T(8,128)(2,1)S(1)} %pad_maximum_fusion.6), channel_id=1, source_target_pairs={{0,6},{2,0},{4,2},{6,4},{1,7},{3,1},{5,3},{7,5},{8,14},{10,8},{12,... | collective-permute-start | bytes 1572872 | tf_op jit(solution)/shard_map/ppermute | solution.py:23
  148.3 10.1 %collective-permute-done.38 = bf16[1024,256]{1,0:T(8,128)(2,1)S(1)} collective-permute-done((bf16[1024,256]{1,0:T(8,128)(2,1)S(1)}, bf16[1024,256]{1,0:T(8,128)(2,1)S(1)}, u32[]{:S(2)}, u32[]{:S(2)}) %collective-permute-start.38) | collective-permute-done | bytes 524320 | tf_op jit(solution)/shard_map/ppermute | solution.py:23
  158.4 3.4 %collective-permute-done.36 = bf16[1024,256]{1,0:T(8,128)(2,1)S(1)} collective-permute-done((bf16[1024,256]{1,0:T(8,128)(2,1)S(1)}, bf16[1024,256]{1,0:T(8,128)(2,1)S(1)}, u32[]{:S(2)}, u32[]{:S(2)}) %collective-permute-start.36) | collective-permute-done | bytes 524320 | tf_op jit(solution)/shard_map/ppermute | solution.py:23
  161.7 1.1 fusion.3
  (74 shorter events, 6.5 us)
Async XLA Ops:
  0.0 12.9 %collective-permute-start = (bf16[1024,256]{1,0:T(8,128)(2,1)}, bf16[1024,256]{1,0:T(8,128)(2,1)S(1)}, u32[]{:S(2)}, u32[]{:S(2)}) collective-permute-start(bf16[1024,256]{1,0:T(8,128)(2,1)} %bitcast.68), channel_id=1, source_target_pairs={{0,2},{2,4},{4,6},{6,0},{1,3},{3,5},{5,7},{7,1},{8,10},{10,12},{12... | collective-permute-start | bytes 1572872 | tf_op jit(solution)/shard_map/ppermute | solution.py:23
  2.0 14.3 %collective-permute-start.1 = (bf16[1024,256]{1,0:T(8,128)(2,1)}, bf16[1024,256]{1,0:T(8,128)(2,1)S(1)}, u32[]{:S(2)}, u32[]{:S(2)}) collective-permute-start(bf16[1024,256]{1,0:T(8,128)(2,1)} %bitcast.69), channel_id=1, source_target_pairs={{0,6},{2,0},{4,2},{6,4},{1,7},{3,1},{5,3},{7,5},{8,14},{10,8},{12,... | collective-permute-start | bytes 1572872 | tf_op jit(solution)/shard_map/ppermute | solution.py:23
  3.3 24.0 %collective-permute-start.2 = (bf16[1024,256]{1,0:T(8,128)(2,1)}, bf16[1024,256]{1,0:T(8,128)(2,1)S(1)}, u32[]{:S(2)}, u32[]{:S(2)}) collective-permute-start(bf16[1024,256]{1,0:T(8,128)(2,1)} %bitcast.70), channel_id=1, source_target_pairs={{0,4},{2,6},{4,0},{6,2},{1,5},{3,7},{5,1},{7,3},{8,12},{10,14},{12... | collective-permute-start | bytes 1572872 | tf_op jit(solution)/shard_map/ppermute | solution.py:23
  7.5 22.8 %collective-permute-start.6 = (bf16[152,1024]{1,0:T(8,128)(2,1)}, bf16[152,1024]{1,0:T(8,128)(2,1)S(1)}, u32[]{:S(2)}, u32[]{:S(2)}) collective-permute-start(bf16[152,1024]{1,0:T(8,128)(2,1)} %get-tuple-element.24), channel_id=1, source_target_pairs={{0,16},{8,24},{16,0},{24,8},{1,17},{9,25},{17,1},{25,9},{2,18},{10... | collective-permute-start | bytes 933896 | tf_op jit(solution)/shard_map/ppermute | solution.py:23
  10.5 19.8 %collective-permute-start.5 = (bf16[152,1024]{1,0:T(8,128)(2,1)}, bf16[152,1024]{1,0:T(8,128)(2,1)S(1)}, u32[]{:S(2)}, u32[]{:S(2)}) collective-permute-start(bf16[152,1024]{1,0:T(8,128)(2,1)} %get-tuple-element.24), channel_id=1, source_target_pairs={{0,24},{8,0},{16,8},{24,16},{1,25},{9,1},{17,9},{25,17},{2,26},{10... | collective-permute-start | bytes 933896 | tf_op jit(solution)/shard_map/ppermute | solution.py:23
  12.9 17.3 %collective-permute-start.4 = (bf16[152,1024]{1,0:T(8,128)(2,1)}, bf16[152,1024]{1,0:T(8,128)(2,1)S(1)}, u32[]{:S(2)}, u32[]{:S(2)}) collective-permute-start(bf16[152,1024]{1,0:T(8,128)(2,1)} %get-tuple-element.24), channel_id=1, source_target_pairs={{0,8},{8,16},{16,24},{24,0},{1,9},{9,17},{17,25},{25,1},{2,10},{10... | collective-permute-start | bytes 933896 | tf_op jit(solution)/shard_map/ppermute | solution.py:23
  27.3 3.0 %copy-start.4 = (bf16[24,1024]{1,0:T(8,128)(2,1)S(1)}, bf16[24,1024]{1,0:T(8,128)(2,1)}, u32[]{:S(2)}) copy-start(bf16[24,1024]{1,0:T(8,128)(2,1)} %get-tuple-element.23) | copy-start | bytes 147460
  27.3 8.8 %copy-start.3 = (bf16[128,1024]{1,0:T(8,128)(2,1)S(1)}, bf16[128,1024]{1,0:T(8,128)(2,1)}, u32[]{:S(2)}) copy-start(bf16[128,1024]{1,0:T(8,128)(2,1)} %get-tuple-element.33) | copy-start | bytes 786436
  28.6 47.5 %collective-permute-start.3 = (bf16[4,1024,256]{2,1,0:T(8,128)(2,1)S(1)}, bf16[4,1024,256]{2,1,0:T(8,128)(2,1)S(1)}, u32[]{:S(2)}, u32[]{:S(2)}) collective-permute-start(bf16[4,1024,256]{2,1,0:T(8,128)(2,1)S(1)} %pad_maximum_fusion), channel_id=1, source_target_pairs={{0,1},{1,0},{2,3},{3,2},{4,5},{5,4},{6,7},{7,6},{8,9},{9,8},{10,11... | collective-permute-start | bytes 6291464 | tf_op jit(solution)/shard_map/ppermute | solution.py:23
  30.3 10.9 %collective-permute-start.7 = (bf16[4,24,1024]{2,1,0:T(8,128)(2,1)S(1)}, bf16[4,24,1024]{2,1,0:T(8,128)(2,1)S(1)}, u32[]{:S(2)}, u32[]{:S(2)}) collective-permute-start(bf16[4,24,1024]{2,1,0:T(8,128)(2,1)S(1)} %pad_maximum_fusion.8.m0), channel_id=1, source_target_pairs={{0,32},{32,64},{64,96},{96,128},{128,160},{160,192},{192,224},{224... | collective-permute-start | bytes 589832 | tf_op jit(solution)/shard_map/ppermute | solution.py:23
  32.1 9.2 %collective-permute-start.8 = (bf16[4,24,1024]{2,1,0:T(8,128)(2,1)S(1)}, bf16[4,24,1024]{2,1,0:T(8,128)(2,1)S(1)}, u32[]{:S(2)}, u32[]{:S(2)}) collective-permute-start(bf16[4,24,1024]{2,1,0:T(8,128)(2,1)S(1)} %pad_maximum_fusion.8.m0), channel_id=1, source_target_pairs={{0,224},{32,0},{64,32},{96,64},{128,96},{160,128},{192,160},{224,1... | collective-permute-start | bytes 589832 | tf_op jit(solution)/shard_map/ppermute | solution.py:23
  36.1 19.8 %collective-permute-start.21 = (bf16[128,1024]{1,0:T(8,128)(2,1)S(1)}, bf16[128,1024]{1,0:T(8,128)(2,1)S(1)}, u32[]{:S(2)}, u32[]{:S(2)}) collective-permute-start(bf16[128,1024]{1,0:T(8,128)(2,1)S(1)} %copy-done.3), channel_id=1, source_target_pairs={{0,64},{32,96},{64,128},{96,160},{128,192},{160,224},{192,0},{224,... | collective-permute-start | bytes 786440 | tf_op jit(solution)/shard_map/ppermute | solution.py:23
  36.1 19.8 %collective-permute-start.20 = (bf16[128,1024]{1,0:T(8,128)(2,1)S(1)}, bf16[128,1024]{1,0:T(8,128)(2,1)S(1)}, u32[]{:S(2)}, u32[]{:S(2)}) collective-permute-start(bf16[128,1024]{1,0:T(8,128)(2,1)S(1)} %copy-done.3), channel_id=1, source_target_pairs={{0,224},{32,0},{64,32},{96,64},{128,96},{160,128},{192,160},{224,1... | collective-permute-start | bytes 786440 | tf_op jit(solution)/shard_map/ppermute | solution.py:23
  41.2 16.9 %collective-permute-start.19 = (bf16[128,1024]{1,0:T(8,128)(2,1)S(1)}, bf16[128,1024]{1,0:T(8,128)(2,1)S(1)}, u32[]{:S(2)}, u32[]{:S(2)}) collective-permute-start(bf16[128,1024]{1,0:T(8,128)(2,1)S(1)} %copy-done.3), channel_id=1, source_target_pairs={{0,32},{32,64},{64,96},{96,128},{128,160},{160,192},{192,224},{224... | collective-permute-start | bytes 786440 | tf_op jit(solution)/shard_map/ppermute | solution.py:23
  41.2 13.3 %collective-permute-start.9 = (bf16[4,24,1024]{2,1,0:T(8,128)(2,1)S(1)}, bf16[4,24,1024]{2,1,0:T(8,128)(2,1)S(1)}, u32[]{:S(2)}, u32[]{:S(2)}) collective-permute-start(bf16[4,24,1024]{2,1,0:T(8,128)(2,1)S(1)} %pad_maximum_fusion.8.m0), channel_id=1, source_target_pairs={{0,192},{32,224},{64,0},{96,32},{128,64},{160,96},{192,128},{224,1... | collective-permute-start | bytes 589832 | tf_op jit(solution)/shard_map/ppermute | solution.py:23
  54.9 7.9 %collective-permute-start.15 = (bf16[528,256]{1,0:T(8,128)(2,1)S(1)}, bf16[528,256]{1,0:T(8,128)(2,1)S(1)}, u32[]{:S(2)}, u32[]{:S(2)}) collective-permute-start(bf16[528,256]{1,0:T(8,128)(2,1)S(1)} %get-tuple-element.28.refs_10_), channel_id=1, source_target_pairs={{0,2},{2,4},{4,6},{6,0},{1,3},{3,5},{5,7},{7,1},{8,10},{10,12},{12... | collective-permute-start | bytes 811016 | tf_op jit(solution)/shard_map/ppermute | solution.py:23
  58.2 17.9 %copy-start = (bf16[1,1024,256]{2,1,0:T(8,128)(2,1)S(1)}, bf16[1,1024,256]{2,1,0:T(8,128)(2,1)}, u32[]{:S(2)}) copy-start(bf16[1,1024,256]{2,1,0:T(8,128)(2,1)} %param.12) | copy-start | bytes 1572868
  58.2 17.9 %copy-start.1 = (bf16[4,128,128]{2,1,0:T(8,128)(2,1)S(1)}, bf16[4,128,128]{2,1,0:T(8,128)(2,1)}, u32[]{:S(2)}) copy-start(bf16[4,128,128]{2,1,0:T(8,128)(2,1)} %refs_7_.1) | copy-start | bytes 393220
  58.3 25.5 %collective-permute-start.22 = (bf16[4,128,1024]{2,1,0:T(8,128)(2,1)S(1)}, bf16[4,128,1024]{2,1,0:T(8,128)(2,1)S(1)}, u32[]{:S(2)}, u32[]{:S(2)}) collective-permute-start(bf16[4,128,1024]{2,1,0:T(8,128)(2,1)S(1)} %pad_maximum_fusion.2.refs_0_), channel_id=1, source_target_pairs={{0,8},{8,16},{16,24},{24,0},{1,9},{9,17},{17,25},{25,1},{2,10},{10... | collective-permute-start | bytes 3145736 | tf_op jit(solution)/shard_map/ppermute | solution.py:23
  59.6 7.2 %collective-permute-start.16 = (bf16[528,256]{1,0:T(8,128)(2,1)S(1)}, bf16[528,256]{1,0:T(8,128)(2,1)S(1)}, u32[]{:S(2)}, u32[]{:S(2)}) collective-permute-start(bf16[528,256]{1,0:T(8,128)(2,1)S(1)} %get-tuple-element.28.refs_10_), channel_id=1, source_target_pairs={{0,6},{2,0},{4,2},{6,4},{1,7},{3,1},{5,3},{7,5},{8,14},{10,8},{12,... | collective-permute-start | bytes 811016 | tf_op jit(solution)/shard_map/ppermute | solution.py:23
  61.3 8.4 %collective-permute-start.17 = (bf16[528,256]{1,0:T(8,128)(2,1)S(1)}, bf16[528,256]{1,0:T(8,128)(2,1)S(1)}, u32[]{:S(2)}, u32[]{:S(2)}) collective-permute-start(bf16[528,256]{1,0:T(8,128)(2,1)S(1)} %get-tuple-element.28.refs_10_), channel_id=1, source_target_pairs={{0,4},{2,6},{4,0},{6,2},{1,5},{3,7},{5,1},{7,3},{8,12},{10,14},{12... | collective-permute-start | bytes 811016 | tf_op jit(solution)/shard_map/ppermute | solution.py:23
  62.8 13.3 %collective-permute-start.10 = (bf16[2064,128]{1,0:T(8,128)(2,1)S(1)}, bf16[2064,128]{1,0:T(8,128)(2,1)S(1)}, u32[]{:S(2)}, u32[]{:S(2)}) collective-permute-start(bf16[2064,128]{1,0:T(8,128)(2,1)S(1)} %get-tuple-element.25.refs_5_), channel_id=1, source_target_pairs={{0,1},{1,0},{2,3},{3,2},{4,5},{5,4},{6,7},{7,6},{8,9},{9,8},{10,11... | collective-permute-start | bytes 1585160 | tf_op jit(solution)/shard_map/ppermute | solution.py:23
  66.8 23.2 %collective-permute-start.23 = (bf16[4,128,1024]{2,1,0:T(8,128)(2,1)S(1)}, bf16[4,128,1024]{2,1,0:T(8,128)(2,1)S(1)}, u32[]{:S(2)}, u32[]{:S(2)}) collective-permute-start(bf16[4,128,1024]{2,1,0:T(8,128)(2,1)S(1)} %pad_maximum_fusion.2.refs_0_), channel_id=1, source_target_pairs={{0,24},{8,0},{16,8},{24,16},{1,25},{9,1},{17,9},{25,17},{2,26},{10... | collective-permute-start | bytes 3145736 | tf_op jit(solution)/shard_map/ppermute | solution.py:23
  69.8 14.7 %copy-start.2 = (bf16[128,1024]{1,0:T(8,128)(2,1)S(1)}, bf16[128,1024]{1,0:T(8,128)(2,1)}, u32[]{:S(2)}) copy-start(bf16[128,1024]{1,0:T(8,128)(2,1)} %get-tuple-element.34) | copy-start | bytes 786436
  69.9 35.2 %collective-permute-start.18 = (bf16[4,528,256]{2,1,0:T(8,128)(2,1)S(1)}, bf16[4,528,256]{2,1,0:T(8,128)(2,1)S(1)}, u32[]{:S(2)}, u32[]{:S(2)}) collective-permute-start(bf16[4,528,256]{2,1,0:T(8,128)(2,1)S(1)} %pad_maximum_fusion.1), channel_id=1, source_target_pairs={{0,1},{1,0},{2,3},{3,2},{4,5},{5,4},{6,7},{7,6},{8,9},{9,8},{10,11... | collective-permute-start | bytes 3244040 | tf_op jit(solution)/shard_map/ppermute | solution.py:23
  79.7 7.3 %collective-permute-start.11 = (bf16[512,128]{1,0:T(8,128)(2,1)S(1)}, bf16[512,128]{1,0:T(8,128)(2,1)S(1)}, u32[]{:S(2)}, u32[]{:S(2)}) collective-permute-start(bf16[512,128]{1,0:T(8,128)(2,1)S(1)} %get-tuple-element.27), channel_id=1, source_target_pairs={{0,2},{2,4},{4,6},{6,0},{1,3},{3,5},{5,7},{7,1},{8,10},{10,12},{12... | collective-permute-start | bytes 393224 | tf_op jit(solution)/shard_map/ppermute | solution.py:23
  79.8 7.3 %collective-permute-start.12 = (bf16[512,128]{1,0:T(8,128)(2,1)S(1)}, bf16[512,128]{1,0:T(8,128)(2,1)S(1)}, u32[]{:S(2)}, u32[]{:S(2)}) collective-permute-start(bf16[512,128]{1,0:T(8,128)(2,1)S(1)} %get-tuple-element.27), channel_id=1, source_target_pairs={{0,6},{2,0},{4,2},{6,4},{1,7},{3,1},{5,3},{7,5},{8,14},{10,8},{12,... | collective-permute-start | bytes 393224 | tf_op jit(solution)/shard_map/ppermute | solution.py:23
  83.8 6.1 %collective-permute-start.13 = (bf16[512,128]{1,0:T(8,128)(2,1)S(1)}, bf16[512,128]{1,0:T(8,128)(2,1)S(1)}, u32[]{:S(2)}, u32[]{:S(2)}) collective-permute-start(bf16[512,128]{1,0:T(8,128)(2,1)S(1)} %get-tuple-element.27), channel_id=1, source_target_pairs={{0,4},{2,6},{4,0},{6,2},{1,5},{3,7},{5,1},{7,3},{8,12},{10,14},{12... | collective-permute-start | bytes 393224 | tf_op jit(solution)/shard_map/ppermute | solution.py:23
  87.0 14.1 %collective-permute-start.26 = (bf16[2,128,1024]{2,1,0:T(8,128)(2,1)S(1)}, bf16[2,128,1024]{2,1,0:T(8,128)(2,1)S(1)}, u32[]{:S(2)}, u32[]{:S(2)}) collective-permute-start(bf16[2,128,1024]{2,1,0:T(8,128)(2,1)S(1)} %pad_maximum_fusion.3.refs_0_), channel_id=1, source_target_pairs={{0,32},{32,64},{64,96},{96,128},{128,160},{160,192},{192,224},{224... | collective-permute-start | bytes 1572872 | tf_op jit(solution)/shard_map/ppermute | solution.py:23
  87.1 15.2 %collective-permute-start.29 = (bf16[2,128,1024]{2,1,0:T(8,128)(2,1)S(1)}, bf16[2,128,1024]{2,1,0:T(8,128)(2,1)S(1)}, u32[]{:S(2)}, u32[]{:S(2)}) collective-permute-start(bf16[2,128,1024]{2,1,0:T(8,128)(2,1)S(1)} %pad_maximum_fusion.4.refs_1_), channel_id=1, source_target_pairs={{0,224},{32,0},{64,32},{96,64},{128,96},{160,128},{192,160},{224,1... | collective-permute-start | bytes 1572872 | tf_op jit(solution)/shard_map/ppermute | solution.py:23
  89.9 12.9 %collective-permute-start.24 = (bf16[2,128,1024]{2,1,0:T(8,128)(2,1)S(1)}, bf16[2,128,1024]{2,1,0:T(8,128)(2,1)S(1)}, u32[]{:S(2)}, u32[]{:S(2)}) collective-permute-start(bf16[2,128,1024]{2,1,0:T(8,128)(2,1)S(1)} %slice.97), channel_id=1, source_target_pairs={{0,8},{8,16},{16,24},{24,0},{1,9},{9,17},{17,25},{25,1},{2,10},{10... | collective-permute-start | bytes 1572872 | tf_op jit(solution)/shard_map/ppermute | solution.py:23
  90.0 15.1 %collective-permute-start.14 = (bf16[3,512,128]{2,1,0:T(8,128)(2,1)S(1)}, bf16[3,512,128]{2,1,0:T(8,128)(2,1)S(1)}, u32[]{:S(2)}, u32[]{:S(2)}) collective-permute-start(bf16[3,512,128]{2,1,0:T(8,128)(2,1)S(1)} %pad_maximum_fusion.7), channel_id=1, source_target_pairs={{0,1},{1,0},{2,3},{3,2},{4,5},{5,4},{6,7},{7,6},{8,9},{9,8},{10,11... | collective-permute-start | bytes 1179656 | tf_op jit(solution)/shard_map/ppermute | solution.py:23
  101.1 15.1 %collective-permute-start.25 = (bf16[2,128,1024]{2,1,0:T(8,128)(2,1)S(1)}, bf16[2,128,1024]{2,1,0:T(8,128)(2,1)S(1)}, u32[]{:S(2)}, u32[]{:S(2)}) collective-permute-start(bf16[2,128,1024]{2,1,0:T(8,128)(2,1)S(1)} %slice.98), channel_id=1, source_target_pairs={{0,24},{8,0},{16,8},{24,16},{1,25},{9,1},{17,9},{25,17},{2,26},{10... | collective-permute-start | bytes 1572872 | tf_op jit(solution)/shard_map/ppermute | solution.py:23
  102.3 16.6 %collective-permute-start.27 = (bf16[2,128,1024]{2,1,0:T(8,128)(2,1)S(1)}, bf16[2,128,1024]{2,1,0:T(8,128)(2,1)S(1)}, u32[]{:S(2)}, u32[]{:S(2)}) collective-permute-start(bf16[2,128,1024]{2,1,0:T(8,128)(2,1)S(1)} %pad_maximum_fusion.4.refs_1_), channel_id=1, source_target_pairs={{0,32},{32,64},{64,96},{96,128},{128,160},{160,192},{192,224},{224... | collective-permute-start | bytes 1572872 | tf_op jit(solution)/shard_map/ppermute | solution.py:23
  102.8 16.1 %collective-permute-start.28 = (bf16[2,128,1024]{2,1,0:T(8,128)(2,1)S(1)}, bf16[2,128,1024]{2,1,0:T(8,128)(2,1)S(1)}, u32[]{:S(2)}, u32[]{:S(2)}) collective-permute-start(bf16[2,128,1024]{2,1,0:T(8,128)(2,1)S(1)} %pad_maximum_fusion.3.refs_0_), channel_id=1, source_target_pairs={{0,224},{32,0},{64,32},{96,64},{128,96},{160,128},{192,160},{224,1... | collective-permute-start | bytes 1572872 | tf_op jit(solution)/shard_map/ppermute | solution.py:23
  105.0 21.5 %collective-permute-start.30 = (bf16[2,128,1024]{2,1,0:T(8,128)(2,1)S(1)}, bf16[2,128,1024]{2,1,0:T(8,128)(2,1)S(1)}, u32[]{:S(2)}, u32[]{:S(2)}) collective-permute-start(bf16[2,128,1024]{2,1,0:T(8,128)(2,1)S(1)} %collective-permute-done.26.refs_2_), channel_id=1, source_target_pairs={{0,32},{32,64},{64,96},{96,128},{128,160},{160,192},{192,224},{224... | collective-permute-start | bytes 1572872 | tf_op jit(solution)/shard_map/ppermute | solution.py:23
  105.0 21.5 %collective-permute-start.31 = (bf16[2,128,1024]{2,1,0:T(8,128)(2,1)S(1)}, bf16[2,128,1024]{2,1,0:T(8,128)(2,1)S(1)}, u32[]{:S(2)}, u32[]{:S(2)}) collective-permute-start(bf16[2,128,1024]{2,1,0:T(8,128)(2,1)S(1)} %collective-permute-done.29.refs_5_), channel_id=1, source_target_pairs={{0,224},{32,0},{64,32},{96,64},{128,96},{160,128},{192,160},{224,1... | collective-permute-start | bytes 1572872 | tf_op jit(solution)/shard_map/ppermute | solution.py:23
  129.8 9.0 %collective-permute-start.33 = (bf16[2,1024,256]{2,1,0:T(8,128)(2,1)S(1)}, bf16[2,1024,256]{2,1,0:T(8,128)(2,1)S(1)}, u32[]{:S(2)}, u32[]{:S(2)}) collective-permute-start(bf16[2,1024,256]{2,1,0:T(8,128)(2,1)S(1)} %get-tuple-element.38), channel_id=1, source_target_pairs={{0,1},{1,0},{2,3},{3,2},{4,5},{5,4},{6,7},{7,6},{8,9},{9,8},{10,11... | collective-permute-start | bytes 3145736 | tf_op jit(solution)/shard_map/ppermute | solution.py:23
  134.2 2.3 %collective-permute-start.34 = (bf16[1,1024,256]{2,1,0:T(8,128)(2,1)S(1)}, bf16[1,1024,256]{2,1,0:T(8,128)(2,1)S(1)}, u32[]{:S(2)}, u32[]{:S(2)}) collective-permute-start(bf16[1,1024,256]{2,1,0:T(8,128)(2,1)S(1)} %get-tuple-element.40), channel_id=1, source_target_pairs={{0,1},{1,0},{2,3},{3,2},{4,5},{5,4},{6,7},{7,6},{8,9},{9,8},{10,11... | collective-permute-start | bytes 1572872 | tf_op jit(solution)/shard_map/ppermute | solution.py:23
  136.0 12.3 %collective-permute-start.32 = (bf16[1,1024,256]{2,1,0:T(8,128)(2,1)S(1)}, bf16[1,1024,256]{2,1,0:T(8,128)(2,1)S(1)}, u32[]{:S(2)}, u32[]{:S(2)}) collective-permute-start(bf16[1,1024,256]{2,1,0:T(8,128)(2,1)S(1)} %get-tuple-element.36), channel_id=1, source_target_pairs={{0,1},{1,0},{2,3},{3,2},{4,5},{5,4},{6,7},{7,6},{8,9},{9,8},{10,11... | collective-permute-start | bytes 1572872 | tf_op jit(solution)/shard_map/ppermute | solution.py:23
  136.7 7.9 %collective-permute-start.37 = (bf16[512,256]{1,0:T(8,128)(2,1)S(1)}, bf16[512,256]{1,0:T(8,128)(2,1)S(1)}, u32[]{:S(2)}, u32[]{:S(2)}) collective-permute-start(bf16[512,256]{1,0:T(8,128)(2,1)S(1)} %get-tuple-element.44), channel_id=1, source_target_pairs={{0,6},{2,0},{4,2},{6,4},{1,7},{3,1},{5,3},{7,5},{8,14},{10,8},{12,... | collective-permute-start | bytes 786440 | tf_op jit(solution)/shard_map/ppermute | solution.py:23
  138.8 9.2 %collective-permute-start.35 = (bf16[512,256]{1,0:T(8,128)(2,1)S(1)}, bf16[512,256]{1,0:T(8,128)(2,1)S(1)}, u32[]{:S(2)}, u32[]{:S(2)}) collective-permute-start(bf16[512,256]{1,0:T(8,128)(2,1)S(1)} %get-tuple-element.43), channel_id=1, source_target_pairs={{0,2},{2,4},{4,6},{6,0},{1,3},{3,5},{5,7},{7,1},{8,10},{10,12},{12... | collective-permute-start | bytes 786440 | tf_op jit(solution)/shard_map/ppermute | solution.py:23
  144.7 13.7 %collective-permute-start.38 = (bf16[1024,256]{1,0:T(8,128)(2,1)S(1)}, bf16[1024,256]{1,0:T(8,128)(2,1)S(1)}, u32[]{:S(2)}, u32[]{:S(2)}) collective-permute-start(bf16[1024,256]{1,0:T(8,128)(2,1)S(1)} %pad_maximum_fusion.6), channel_id=1, source_target_pairs={{0,6},{2,0},{4,2},{6,4},{1,7},{3,1},{5,3},{7,5},{8,14},{10,8},{12,... | collective-permute-start | bytes 1572872 | tf_op jit(solution)/shard_map/ppermute | solution.py:23
  148.2 13.6 %collective-permute-start.36 = (bf16[1024,256]{1,0:T(8,128)(2,1)S(1)}, bf16[1024,256]{1,0:T(8,128)(2,1)S(1)}, u32[]{:S(2)}, u32[]{:S(2)}) collective-permute-start(bf16[1024,256]{1,0:T(8,128)(2,1)S(1)} %pad_maximum_fusion.5), channel_id=1, source_target_pairs={{0,2},{2,4},{4,6},{6,0},{1,3},{3,5},{5,7},{7,1},{8,10},{10,12},{12... | collective-permute-start | bytes 1572872 | tf_op jit(solution)/shard_map/ppermute | solution.py:23
